TPU v7x, 32 devices: a whole 2x2x4 slice. The times are simulated.
32 devices in a mesh: fs: 8 (over z, y), tp: 4 (over x, core).
Axes of the slice: x: 2, y: 2, z: 4, core: 2. Of those that a mesh axis runs over, the one named last changes fastest.
Arguments:
- tokens: bfloat16 [1280, 2048], P('fs', 'tp'), may hold values from -6 to 6
- mix_gain: float32 [2048], replicated, may hold values from 0.1 to 1.9
- in_x_w: bfloat16 [2048, 1024], P('fs', 'tp'), may hold values from -0.125 to 0.125
- in_gate_w: bfloat16 [2048, 1024], P('fs', 'tp'), may hold values from -0.125 to 0.125
- conv_taps: float32 [4, 1024], P(None, 'tp'), may hold values from -3 to 3
- gate_x_blocks: bfloat16 [8, 128, 128], P('tp'), may hold values from -0.5 to 0.5
- gate_a_blocks: bfloat16 [8, 128, 128], P('tp'), may hold values from -0.5 to 0.5
- forget_rate: float32 [1024], P('tp'), may hold values from 0.002 to 0.08
- out_w: bfloat16 [1024, 2048], P('tp', 'fs'), may hold values from -0.1875 to 0.1875
- ffn_gain: float32 [2048], replicated, may hold values from 0.1 to 1.9
- ffn_gate_w: bfloat16 [2048, 2816], P('fs', 'tp'), may hold values from -0.125 to 0.125
- ffn_up_w: bfloat16 [2048, 2816], P('fs', 'tp'), may hold values from -0.125 to 0.125
- ffn_down_w: bfloat16 [2816, 2048], P('tp', 'fs'), may hold values from -0.109375 to 0.109375
Outputs:
- layer_out: bfloat16 [1280, 2048], P('fs', 'tp')
All inputs are finite; a program needn't handle non-finite values.
Results may differ from a plain program's by a relative error of at most 0.015.
Values may be sent and summed in bfloat16 or wider, within the bound.
No kernel may reach another device: no remote copies, remote signals or barrier semaphores. Data moves between devices by JAX's collectives and lax.ppermute only.
A program may use at most 64 MiB of HBM per device.

v0:
```python
import jax
import jax.numpy as jnp
from jax import lax
from jax.sharding import PartitionSpec as P

epsilon = 1e-06
gate_power = 8.0


def rms_norm(values, gain):
    wide = values.astype(jnp.float32)
    mean_square = jnp.mean(wide * wide, axis=-1, keepdims=True)
    return (wide * lax.rsqrt(mean_square + epsilon) * gain).astype(jnp.bfloat16)


def full_rows(shard):
    return lax.all_gather(shard, "tp", axis=1, tiled=True)


def pair_folder(left_rows, pieces):
    return (
        jnp.dot(left_rows, pieces[0], preferred_element_type=jnp.float32),
        jnp.dot(left_rows, pieces[1], preferred_element_type=jnp.float32),
    )


def project_out(acts, weight):
    partial_terms = jnp.dot(
        acts, lax.all_gather(weight, "fs", axis=1, tiled=True), preferred_element_type=jnp.float32
    )
    return lax.psum_scatter(
        partial_terms.astype(jnp.bfloat16), "tp", scatter_dimension=1, tiled=True
    ).astype(jnp.float32)


def combine(earlier, later):
    return (earlier[0] * later[0], later[0] * earlier[1] + later[1])


def on_device(
    tokens,
    mix_gain,
    in_x_w,
    in_gate_w,
    conv_taps,
    gate_x_blocks,
    gate_a_blocks,
    forget_rate,
    out_w,
    ffn_gain,
    ffn_gate_w,
    ffn_up_w,
    ffn_down_w,
):
    normed = rms_norm(full_rows(tokens), mix_gain)
    length = normed.shape[0]
    chan_width = in_x_w.shape[1]
    branch_in, branch_gate = pair_folder(
        normed,
        (
            lax.all_gather(in_x_w, "fs", axis=0, tiled=True),
            lax.all_gather(in_gate_w, "fs", axis=0, tiled=True),
        ),
    )
    tap_count = conv_taps.shape[0]
    padded = jnp.pad(branch_in, ((tap_count - 1, 0), (0, 0)))
    conv_sum = padded[0:length] * conv_taps[0]
    for index in range(1, tap_count):
        conv_sum = conv_sum + padded[index : index + length] * conv_taps[index]
    conv_out = conv_sum.astype(jnp.bfloat16)
    blocks = gate_x_blocks.shape[0]
    block_dim = gate_x_blocks.shape[1]
    grouped = conv_out.reshape(length, blocks, block_dim)
    gate_x = jax.nn.sigmoid(
        jnp.einsum(
            "tbi,bij->tbj", grouped, gate_x_blocks, preferred_element_type=jnp.float32
        ).reshape(length, chan_width)
    )
    gate_a = jax.nn.sigmoid(
        jnp.einsum(
            "tbi,bij->tbj", grouped, gate_a_blocks, preferred_element_type=jnp.float32
        ).reshape(length, chan_width)
    )
    log_decay = -gate_power * gate_a * forget_rate
    decay = jnp.exp(log_decay)
    scale = jnp.sqrt(-jnp.expm1(2.0 * log_decay))
    scale = jnp.where((jnp.arange(length) == 0)[:, None], 1.0, scale)
    driven = conv_out.astype(jnp.float32) * gate_x * scale
    _, state = lax.associative_scan(combine, (decay, driven), axis=0)
    mixer_out = (state * jax.nn.gelu(branch_gate)).astype(jnp.bfloat16)
    after_mix = (tokens.astype(jnp.float32) + project_out(mixer_out, out_w)).astype(jnp.bfloat16)
    normed_ffn = rms_norm(full_rows(after_mix), ffn_gain)
    gate_val, up_val = pair_folder(
        normed_ffn,
        (
            lax.all_gather(ffn_gate_w, "fs", axis=0, tiled=True),
            lax.all_gather(ffn_up_w, "fs", axis=0, tiled=True),
        ),
    )
    hidden = (jax.nn.silu(gate_val) * up_val).astype(jnp.bfloat16)
    return (after_mix.astype(jnp.float32) + project_out(hidden, ffn_down_w)).astype(jnp.bfloat16)


def solution(mesh):
    placed = (
        P("fs", "tp"),
        P(),
        P("fs", "tp"),
        P("fs", "tp"),
        P(None, "tp"),
        P("tp", None, None),
        P("tp", None, None),
        P("tp"),
        P("tp", "fs"),
        P(),
        P("fs", "tp"),
        P("fs", "tp"),
        P("tp", "fs"),
    )
    return jax.shard_map(
        on_device, mesh=mesh, in_specs=placed, out_specs=P("fs", "tp"), check_vma=False
    )
```

profile of v0, /device:TPU:0, one launch (start us, length us, event | category | flops | bytes accessed | tf_op | source)
XLA Modules:
  0.0 374.7 jit_solution(2551667740566084442)
XLA Ops:
  6.5 0.0 copy-start
  6.5 0.0 copy-start.3
  6.5 0.0 copy-start.4
  6.5 0.0 copy-start.2
  6.5 0.0 all-gather.7.cloned.1.call-start
  6.6 0.7 all-gather.7.cloned.1.call-update
  7.3 0.0 all-gather.11.cloned.1.call-start
  7.3 0.7 all-gather.11.cloned.1.call-update
  8.0 0.0 all-gather.9.cloned.1.call-start
  8.1 0.7 all-gather.9.cloned.1.call-update
  8.8 0.0 reduce-scatter.3.cloned.1.call-start
  8.8 9.6 %all_gather.24 = bf16[160,2048]{1,0:T(8,128)(2,1)S(1)} all-gather(bf16[160,512]{1,0:T(8,128)(2,1)} %param.13), channel_id=1, replica_groups=mesh['fs'=8,'tp'=4] {'tp'}, dimensions={1}, use_global_device_ids=true | all-gather | bytes 819200 | tf_op jit(solution)/shard_map/all_gather | solution.py:17
  18.4 0.2 fusion
  18.6 0.0 copy-done.3
  18.6 0.0 copy-done.4
  18.7 0.0 copy-start.5
  18.7 33.8 %all-gather.7.cloned.1.call-done = bf16[2048,256]{1,0:T(8,128)(2,1)} async-done(((bf16[256,256]{1,0:T(8,128)(2,1)}), bf16[2048,256]{1,0:T(8,128)(2,1)}) %all-gather.7.cloned.1.call-update) | async-done | bytes 1048592 | tf_op jit(solution)/shard_map/all_gather | solution.py:61
  52.5 0.0 copy-done.2
  52.5 1.6 fusion.27
  54.1 0.1 fusion.83
  54.2 0.0 copy-done
  54.2 0.2 fusion.10
  54.4 0.0 copy-done.5
  54.4 0.2 fusion.14
  54.6 0.2 fusion.49
  56.3 36.3 %all-gather.11.cloned.1.call-done = bf16[256,2048]{1,0:T(8,128)(2,1)} async-done(((bf16[256,256]{1,0:T(8,128)(2,1)}), bf16[256,2048]{1,0:T(8,128)(2,1)}) %all-gather.11.cloned.1.call-update) | async-done | bytes 1048592 | tf_op jit(solution)/shard_map/all_gather | solution.py:29
  92.7 41.5 %all-gather.9.cloned.1.call-done = bf16[2048,256]{1,0:T(8,128)(2,1)} async-done(((bf16[256,256]{1,0:T(8,128)(2,1)}), bf16[2048,256]{1,0:T(8,128)(2,1)}) %all-gather.9.cloned.1.call-update) | async-done | bytes 1048592 | tf_op jit(solution)/shard_map/all_gather | solution.py:62
  134.1 3.4 convolution_convert_fusion.1
  137.5 0.0 copy-start.1
  137.5 0.0 reduce-scatter.3.cloned.1.call-update
  137.6 0.0 all-gather.13.cloned.1.call-start
  137.6 0.5 all-gather.13.cloned.1.call-update
  138.1 0.0 copy-start.6
  138.2 0.0 all-gather.15.cloned.1.call-start
  138.2 0.5 all-gather.15.cloned.1.call-update
  138.7 0.0 all-gather.17.cloned.1.call-start
  138.8 0.7 all-gather.17.cloned.1.call-update
  139.5 0.0 reduce-scatter.5.cloned.1.call-start
  139.5 19.3 %reduce-scatter.3.cloned.1.call-done = bf16[160,512]{1,0:T(8,128)(2,1)} async-done(((bf16[160,2048]{1,0:T(8,128)(2,1)}), bf16[160,512]{1,0:T(8,128)(2,1)}) %reduce-scatter.3.cloned.1.call-update) | async-done | bytes 163856 | tf_op jit(solution)/shard_map/reduce_scatter | solution.py:31
  158.9 0.0 copy-done.1
  158.9 1.0 add_convert_fusion.1
  159.8 7.3 %all_gather.28 = bf16[160,2048]{1,0:T(8,128)(2,1)S(1)} all-gather(bf16[160,512]{1,0:T(8,128)(2,1)S(1)} %add_convert_fusion.1), channel_id=1, replica_groups=mesh['fs'=8,'tp'=4] {'tp'}, dimensions={1}, use_global_device_ids=true | all-gather | bytes 819200 | tf_op jit(solution)/shard_map/all_gather | solution.py:17
  167.1 0.2 fusion.3
  167.4 53.0 %all-gather.13.cloned.1.call-done = bf16[2048,704]{0,1:T(8,128)(2,1)} async-done(((bf16[256,704]{0,1:T(8,128)(2,1)}), bf16[2048,704]{0,1:T(8,128)(2,1)}) %all-gather.13.cloned.1.call-update) | async-done | bytes 2883600 | tf_op jit(solution)/shard_map/all_gather | solution.py:96
  220.4 0.0 copy-done.6
  220.4 2.9 fusion.23
  223.3 56.8 %all-gather.15.cloned.1.call-done = bf16[2048,704]{0,1:T(8,128)(2,1)} async-done(((bf16[256,704]{0,1:T(8,128)(2,1)}), bf16[2048,704]{0,1:T(8,128)(2,1)}) %all-gather.15.cloned.1.call-update) | async-done | bytes 2883600 | tf_op jit(solution)/shard_map/all_gather | solution.py:97
  280.0 59.8 %all-gather.17.cloned.1.call-done = bf16[704,2048]{1,0:T(8,128)(2,1)} async-done(((bf16[704,256]{1,0:T(8,128)(2,1)}), bf16[704,2048]{1,0:T(8,128)(2,1)}) %all-gather.17.cloned.1.call-update) | async-done | bytes 2883600 | tf_op jit(solution)/shard_map/all_gather | solution.py:29
  339.9 5.6 %convolution_convert_fusion = bf16[160,2048]{1,0:T(8,128)(2,1)} fusion(bf16[704,2048]{1,0:T(8,128)(2,1)} %all-gather.17.cloned.1.call-done, bf16[2048,704]{0,1:T(8,128)(2,1)} %all-gather.15.cloned.1.call-done, f32[160,704]{1,0:T(8,128)S(1)} %fusion.23, bf16[160,2048]{1,0:T(8,128)(2,1)S(1)} %all_gather.28, f32[2048]{0:T(1024)S(1)} %copy-done.6, ...), kind=kOutput, calls=%fused_computation | convolution fusion | flops 925061120 | bytes 7537280 | tf_op jit(solution)/shard_map/dot_general | solution.py:28
  345.4 0.0 reduce-scatter.5.cloned.1.call-update
  345.5 20.8 %reduce-scatter.5.cloned.1.call-done = bf16[160,512]{1,0:T(8,128)(2,1)} async-done(((bf16[160,2048]{1,0:T(8,128)(2,1)}), bf16[160,512]{1,0:T(8,128)(2,1)}) %reduce-scatter.5.cloned.1.call-update) | async-done | bytes 163856 | tf_op jit(solution)/shard_map/reduce_scatter | solution.py:31
  366.2 1.6 add_convert_fusion
  (83 shorter events, 1.2 us)
Async XLA Ops:
  6.5 47.7 %copy-start = (bf16[2,128,128]{2,1,0:T(8,128)(2,1)S(1)}, bf16[2,128,128]{2,1,0:T(8,128)(2,1)}, u32[]{:S(2)}) copy-start(bf16[2,128,128]{2,1,0:T(8,128)(2,1)} %param.19) | copy-start | bytes 196612
  6.5 12.1 %copy-start.3 = (f32[4,256]{1,0:T(4,128)S(1)}, f32[4,256]{1,0:T(4,128)}, u32[]{:S(2)}) copy-start(f32[4,256]{1,0:T(4,128)} %param.17) | copy-start | bytes 12292
  6.5 12.1 %copy-start.4 = (f32[256]{0:T(256)S(1)}, f32[256]{0:T(256)}, u32[]{:S(2)}) copy-start(f32[256]{0:T(256)} %param.20) | copy-start | bytes 3076
  6.5 46.0 %copy-start.2 = (f32[2048]{0:T(1024)S(1)}, f32[2048]{0:T(1024)}, u32[]{:S(2)}) copy-start(f32[2048]{0:T(1024)} %param.14) | copy-start | bytes 24580
  6.5 45.9 %all-gather.7.cloned.1.call-start = ((), (), s32[]{:S(2)}) async-start(), calls=%async_computation.2 | async-start | bytes 1179648 | tf_op jit(solution)/shard_map/all_gather | solution.py:61
  7.3 85.4 %all-gather.11.cloned.1.call-start = ((), (), s32[]{:S(2)}) async-start(), calls=%async_computation.4 | async-start | bytes 1179648 | tf_op jit(solution)/shard_map/all_gather | solution.py:29
  8.0 126.1 %all-gather.9.cloned.1.call-start = ((), (), s32[]{:S(2)}) async-start(), calls=%async_computation.3 | async-start | bytes 1179648 | tf_op jit(solution)/shard_map/all_gather | solution.py:62
  8.8 150.1 %reduce-scatter.3.cloned.1.call-start = ((), (), s32[]{:S(2)}) async-start(), calls=%async_computation.5 | async-start | bytes 819200 | tf_op jit(solution)/shard_map/reduce_scatter | solution.py:31
  18.7 35.8 %copy-start.5 = (bf16[2,128,128]{2,1,0:T(8,128)(2,1)S(1)}, bf16[2,128,128]{2,1,0:T(8,128)(2,1)}, u32[]{:S(2)}) copy-start(bf16[2,128,128]{2,1,0:T(8,128)(2,1)} %param.18) | copy-start | bytes 196612
  137.5 21.3 %copy-start.1 = (bf16[160,512]{1,0:T(8,128)(2,1)S(1)}, bf16[160,512]{1,0:T(8,128)(2,1)}, u32[]{:S(2)}) copy-start(bf16[160,512]{1,0:T(8,128)(2,1)} %param.13) | copy-start | bytes 491524
  137.6 82.8 %all-gather.13.cloned.1.call-start = ((), (), s32[]{:S(2)}) async-start(), calls=%async_computation.6 | async-start | bytes 3244032 | tf_op jit(solution)/shard_map/all_gather | solution.py:96
  138.1 82.2 %copy-start.6 = (f32[2048]{0:T(1024)S(1)}, f32[2048]{0:T(1024)}, u32[]{:S(2)}) copy-start(f32[2048]{0:T(1024)} %param.22) | copy-start | bytes 24580
  138.2 141.9 %all-gather.15.cloned.1.call-start = ((), (), s32[]{:S(2)}) async-start(), calls=%async_computation.7 | async-start | bytes 3244032 | tf_op jit(solution)/shard_map/all_gather | solution.py:97
  138.7 201.1 %all-gather.17.cloned.1.call-start = ((), (), s32[]{:S(2)}) async-start(), calls=%async_computation.8 | async-start | bytes 3244032 | tf_op jit(solution)/shard_map/all_gather | solution.py:29
  139.5 226.8 %reduce-scatter.5.cloned.1.call-start = ((), (), s32[]{:S(2)}) async-start(), calls=%async_computation.9 | async-start | bytes 819200 | tf_op jit(solution)/shard_map/reduce_scatter | solution.py:31
Sparse Core Ops, SparseCore 0:
  9.5 42.9 all-gather.6
  54.5 38.0 all-gather.10
  94.8 39.2 all-gather.8
  137.7 21.1 reduce-scatter.2
  160.7 59.5 all-gather.12
  222.3 57.7 all-gather.14
  282.1 57.7 all-gather.16
  345.6 20.6 reduce-scatter.4
where the time goes:
time: 375 us
  waiting for transfers between devices  325 us (87%)
  blocking collectives  16.9 us (5%)
  between operations  14 us (4%)
  matrix products  13.9 us (4%)
    all_gather x2, waiting for transfers between devices, project_out(): lax.all_gather(weight, 'fs', axis=1, tiled=True)  96.2 us
    all_gather x1, waiting for transfers between devices, on_device(): lax.all_gather(ffn_up_w, 'fs', axis=0, tiled=True)  56.8 us
    all_gather x1, waiting for transfers between devices, on_device(): lax.all_gather(ffn_gate_w, 'fs', axis=0, tiled=True)  53 us
    all_gather x1, waiting for transfers between devices, on_device(): lax.all_gather(in_gate_w, 'fs', axis=0, tiled=True)  41.5 us
    reduce_scatter x2, waiting for transfers between devices, project_out(): lax.psum_scatter(partial_terms.astype(jnp.bfloat16), 'tp', scatter_dimens...  40.1 us
    all_gather x1, waiting for transfers between devices, on_device(): lax.all_gather(in_x_w, 'fs', axis=0, tiled=True)  33.8 us
    all_gather x2, blocking collectives, full_rows(): return lax.all_gather(shard, 'tp', axis=1, tiled=True)  16.9 us
    dot_general x2, matrix products, project_out(): jnp.dot(acts, lax.all_gather(weight, 'fs', axis=1, tiled=True), preferred...  8.98 us
  transfers between devices with their start and end apart: 8, of which 8 were waited for; matrix products, arithmetic and copies ran while one was open for 2% of the time, Pallas kernels for 0%

commit v1 on v0

v1 whole, which is shorter than its diff:
```python
import functools

import jax
import jax.numpy as jnp
from jax import lax
from jax.experimental import pallas as pl
from jax.experimental.pallas import tpu as pltpu
from jax.sharding import PartitionSpec as P

epsilon = 1e-06
gate_power = 8.0


def dot(left, right):
    return jnp.dot(left, right, preferred_element_type=jnp.float32)


def rms_norm(values, gain):
    wide = values.astype(jnp.float32)
    mean_square = jnp.mean(wide * wide, axis=-1, keepdims=True)
    return (wide * lax.rsqrt(mean_square + epsilon) * gain).astype(jnp.bfloat16)


def full_rows(shard):
    return lax.all_gather(shard, "tp", axis=1, tiled=True)


def project_out(acts, weight):
    partial_terms = dot(acts, lax.all_gather(weight, "fs", axis=1, tiled=True))
    return lax.psum_scatter(
        partial_terms.astype(jnp.bfloat16), "tp", scatter_dimension=1, tiled=True
    ).astype(jnp.float32)


def combine(earlier, later):
    return (earlier[0] * later[0], later[0] * earlier[1] + later[1])


def gathered_layer(
    tokens,
    mix_gain,
    in_x_w,
    in_gate_w,
    conv_taps,
    gate_x_blocks,
    gate_a_blocks,
    forget_rate,
    out_w,
    ffn_gain,
    ffn_gate_w,
    ffn_up_w,
    ffn_down_w,
):
    normed = rms_norm(full_rows(tokens), mix_gain)
    length = normed.shape[0]
    chan_width = in_x_w.shape[1]
    branch_in = dot(normed, lax.all_gather(in_x_w, "fs", axis=0, tiled=True))
    branch_gate = dot(normed, lax.all_gather(in_gate_w, "fs", axis=0, tiled=True))
    tap_count = conv_taps.shape[0]
    padded = jnp.pad(branch_in, ((tap_count - 1, 0), (0, 0)))
    conv_sum = padded[0:length] * conv_taps[0]
    for index in range(1, tap_count):
        conv_sum = conv_sum + padded[index : index + length] * conv_taps[index]
    conv_out = conv_sum.astype(jnp.bfloat16)
    blocks, block_dim = gate_x_blocks.shape[:2]
    grouped = conv_out.reshape(length, blocks, block_dim)

    def gate(maps):
        mapped = jnp.einsum("tbi,bij->tbj", grouped, maps, preferred_element_type=jnp.float32)
        return jax.nn.sigmoid(mapped.reshape(length, chan_width))

    log_decay = -gate_power * gate(gate_a_blocks) * forget_rate
    scale = jnp.sqrt(-jnp.expm1(2.0 * log_decay))
    scale = jnp.where((jnp.arange(length) == 0)[:, None], 1.0, scale)
    driven = conv_out.astype(jnp.float32) * gate(gate_x_blocks) * scale
    _, state = lax.associative_scan(combine, (jnp.exp(log_decay), driven), axis=0)
    mixer_out = (state * jax.nn.gelu(branch_gate)).astype(jnp.bfloat16)
    after_mix = (tokens.astype(jnp.float32) + project_out(mixer_out, out_w)).astype(jnp.bfloat16)
    normed_ffn = rms_norm(full_rows(after_mix), ffn_gain)
    gate_val = dot(normed_ffn, lax.all_gather(ffn_gate_w, "fs", axis=0, tiled=True))
    up_val = dot(normed_ffn, lax.all_gather(ffn_up_w, "fs", axis=0, tiled=True))
    hidden = (jax.nn.silu(gate_val) * up_val).astype(jnp.bfloat16)
    return (after_mix.astype(jnp.float32) + project_out(hidden, ffn_down_w)).astype(jnp.bfloat16)


MATE = 2
GROUP = 2
KERNEL_BYTES = 16 << 20


def side_of(fs):
    return lax.rem(lax.div(fs, MATE), 2)


def turn_of(tp):
    return (tp & 1) * 4 + ((tp >> 1) ^ (tp & 1))


def block_of(fs, entry, count):
    back = ((fs >> 1) - entry // 2) & (count // 2 - 1)
    return back * 2 + ((fs & 1) ^ (entry & 1))


def at(index, size):
    return pl.ds(pl.multiple_of(index * size, size), size)


def call(kernel, outs, args, scratch=(), space=pltpu.VMEM):
    spec = pl.BlockSpec(memory_space=pltpu.VMEM)
    return pl.pallas_call(
        kernel,
        out_shape=outs,
        in_specs=[spec] * len(args),
        out_specs=jax.tree.map(lambda _: spec, outs),
        scratch_shapes=list(scratch),
        compiler_params=pltpu.CompilerParams(vmem_limit_bytes=KERNEL_BYTES),
    )(*[pltpu.with_memory_space_constraint(arg, space) for arg in args])


def split_in_kernel(x_ref, gate_ref, mine_ref, other_ref):
    side = side_of(lax.axis_index("fs"))
    half = x_ref.shape[1] // 2
    for out, which in ((mine_ref, side), (other_ref, 1 - side)):
        out[:, :half] = x_ref[:, at(which, half)]
        out[:, half:] = gate_ref[:, at(which, half)]


def split_ffn_kernel(gate_ref, up_ref, down_ref, *results):
    side = side_of(lax.axis_index("fs"))
    half = gate_ref.shape[0] // 2
    for turn, which in enumerate((side, 1 - side)):
        up_part, down_part = results[2 * turn : 2 * turn + 2]
        up_part[:half] = gate_ref[at(which, half), :]
        up_part[half:] = up_ref[at(which, half), :]
        down_part[...] = down_ref[at(which, half), :]


def normalize(tp, row_refs, gain_ref, normed_ref):
    length, width = row_refs[0].shape
    slots = len(row_refs) // 2
    features = slots // GROUP * 2 * width
    for far in range(GROUP):
        pieces = []
        squares = 0.0
        for pair in range(slots // GROUP):
            for odd in range(2):
                wide = row_refs[odd * slots + pair * GROUP + far][...].astype(jnp.float32)
                squares = squares + jnp.sum(wide * wide, axis=1, keepdims=True)
                pieces.append((2 * pair + odd, wide))
        norm = lax.rsqrt(squares / features + epsilon)
        for step, wide in pieces:
            lanes = at(tp ^ step, width)
            scaled = wide * norm * gain_ref[:, lanes]
            normed_ref[far * length : (far + 1) * length, lanes] = scaled.astype(jnp.bfloat16)


def minus_expm1(value):
    series = 1.0 / 5040.0
    for factor in (720.0, 120.0, 24.0, 6.0, 2.0, 1.0):
        series = series * value + 1.0 / factor
    return jnp.where(value > -0.25, -value * series, 1.0 - jnp.exp(value))


def mixer_kernel(
    pieces, gain_ref, taps_ref, x_maps_ref, a_maps_ref, rate_ref, *rest
):
    row_refs, weights = rest[:pieces], rest[pieces:-3]
    out_ref, normed_ref, padded_ref = rest[-3:]
    fs = lax.axis_index("fs")
    tp = lax.axis_index("tp")
    side = side_of(fs)
    length = row_refs[0].shape[0]
    normalize(tp, row_refs, gain_ref, normed_ref)
    depth = weights[0].shape[0]
    branches = dot(normed_ref[:, at(fs, depth)], weights[0][...])
    for step in range(1, len(weights)):
        lanes = at(block_of(fs, step, len(weights)), depth)
        branches = branches + dot(normed_ref[:, lanes], weights[step][...])
    chans = out_ref.shape[1]
    tap_count = taps_ref.shape[0]
    taps = taps_ref[:, at(side, chans)]
    rate = rate_ref[:, at(side, chans)]
    maps = x_maps_ref.shape[0] // 2
    size = x_maps_ref.shape[1]
    lead = padded_ref.shape[0] - length
    row = lax.broadcasted_iota(jnp.int32, (length, chans), 0)
    padded_ref[:lead] = jnp.zeros((lead, chans), jnp.float32)
    for far in range(GROUP):
        rows = slice(far * length, (far + 1) * length)
        padded_ref[lead:] = branches[rows, :chans]
        first = lead - tap_count + 1
        conv_sum = padded_ref[first : first + length] * taps[0:1]
        for index in range(1, tap_count):
            start = first + index
            conv_sum = conv_sum + padded_ref[start : start + length] * taps[index : index + 1]
        conv_out = conv_sum.astype(jnp.bfloat16)

        def gate(maps_ref):
            parts = [
                dot(conv_out[:, i * size : (i + 1) * size], maps_ref[side * maps + i])
                for i in range(maps)
            ]
            return jax.nn.sigmoid(jnp.concatenate(parts, axis=1) if maps > 1 else parts[0])

        log_decay = -gate_power * gate(a_maps_ref) * rate
        decay = jnp.exp(log_decay)
        scale = jnp.where(row == 0, 1.0, jnp.sqrt(minus_expm1(2.0 * log_decay)))
        state = conv_out.astype(jnp.float32) * gate(x_maps_ref) * scale
        reach = 1
        while reach < length:
            begun = row >= reach
            state = state + decay * jnp.where(begun, pltpu.roll(state, reach, 0), 0.0)
            decay = decay * jnp.where(begun, pltpu.roll(decay, reach, 0), 1.0)
            reach *= 2
        out_ref[rows, :] = (state * jax.nn.gelu(branches[rows, chans:])).astype(jnp.bfloat16)


def halves_of(ref, far):
    length = ref.shape[0] // GROUP
    return [ref[((slot ^ far) * length) : ((slot ^ far) + 1) * length] for slot in range(GROUP)]


def mix_project_kernel(pieces, *refs):
    mixed, rows, weights = refs[:pieces], refs[pieces : 2 * pieces], refs[2 * pieces : -1]
    out_ref = refs[-1]
    fs = lax.axis_index("fs")
    tp = lax.axis_index("tp")
    side = side_of(fs)
    slots = pieces // 2
    length, width = rows[0].shape
    chans = mixed[0].shape[1]
    columns = weights[0].shape[1]
    block = fs ^ turn_of(tp)
    per_tp = width // columns
    owner = tp ^ lax.div(block, per_tp)
    lanes = at(lax.rem(block, per_tp), columns)
    totals = []
    for slot in range(GROUP):
        base = rows[slot][:, lanes]
        for step in range(1, slots // GROUP * 2):
            source = rows[(step & 1) * slots + step // 2 * GROUP + slot]
            base = jnp.where(owner == step, source[:, lanes], base)
        totals.append(base.astype(jnp.float32))
    for far in range(GROUP):
        which = at(side ^ far, chans)
        for step in range(slots // GROUP * 2):
            source = mixed[(step & 1) * slots + step // 2 * GROUP + far]
            part = dot(source[...], weights[step][which, :])
            for slot in range(GROUP):
                start = (slot ^ far) * length
                totals[slot] = totals[slot] + part[start : start + length]
    for slot in range(GROUP):
        out_ref[slot * length : (slot + 1) * length] = totals[slot].astype(jnp.bfloat16)


def hidden_kernel(pieces, gain_ref, *rest):
    row_refs, weights = rest[:pieces], rest[pieces:-4]
    out_ref, own_ref, normed_ref, whole_ref = rest[-4:]
    fs = lax.axis_index("fs")
    tp = lax.axis_index("tp")
    slots = pieces // 2
    length, width = own_ref.shape
    columns = row_refs[0].shape[1]
    features = columns * pieces
    squares = [0.0] * GROUP
    found = []
    for odd in range(2):
        for pair in range(slots // GROUP):
            for far in range(GROUP):
                source = row_refs[odd * slots + pair * GROUP + far]
                block = fs ^ (MATE * far) ^ turn_of(tp ^ (2 * pair + odd))
                halves = halves_of(source, far)
                whole_ref[:, at(block, columns)] = halves[0]
                wide = [half.astype(jnp.float32) for half in halves]
                for slot in range(GROUP):
                    row_sum = jnp.sum(wide[slot] * wide[slot], axis=1, keepdims=True)
                    squares[slot] = squares[slot] + row_sum
                found.append((at(block, columns), wide))
    norms = [lax.rsqrt(total / features + epsilon) for total in squares]
    for lanes, wide in found:
        for slot in range(GROUP):
            scaled = wide[slot] * norms[slot] * gain_ref[:, lanes]
            normed_ref[slot * length : (slot + 1) * length, lanes] = scaled.astype(jnp.bfloat16)
    own_ref[...] = whole_ref[:, at(tp, width)]
    units = out_ref.shape[1]
    depth = weights[0].shape[1]

    def project(first):
        total = None
        for step, weight in enumerate(weights):
            part = lax.dot_general(
                normed_ref[:, at(block_of(fs, step, len(weights)), depth)],
                weight[first : first + units, :],
                (((1,), (1,)), ((), ())),
                preferred_element_type=jnp.float32,
            )
            total = part if total is None else total + part
        return total

    out_ref[...] = (jax.nn.silu(project(0)) * project(units)).astype(jnp.bfloat16)


def project_out_kernel(acts_ref, *rest):
    *weights, send_ref, keep_ref, whole_ref = rest
    fs = lax.axis_index("fs")
    tp = lax.axis_index("tp")
    slots, length, width = keep_ref.shape
    columns = weights[0].shape[1]
    for step, weight in enumerate(weights):
        whole_ref[:, at(block_of(fs, step, len(weights)), columns)] = weight[...]
    for step in range(slots // GROUP * 2):
        part = dot(acts_ref[...], whole_ref[:, at(tp ^ step, width)]).astype(jnp.bfloat16)
        target = send_ref if step % 2 else keep_ref
        for far in range(GROUP):
            target[step // 2 * GROUP + far] = part[far * length : (far + 1) * length]


def join_kernel(keep_ref, got_ref, own_ref, *sent):
    own_ref[...] = keep_ref[0].astype(jnp.float32) + got_ref[0].astype(jnp.float32)
    for slot, out in enumerate(sent, 1):
        total = keep_ref[slot].astype(jnp.float32) + got_ref[slot].astype(jnp.float32)
        out[...] = total.astype(jnp.bfloat16)


def finish_kernel(base_ref, own_ref, *rest):
    *parts, out_ref = rest
    total = own_ref[...]
    for part in parts:
        total = total + part[...].astype(jnp.float32)
    out_ref[...] = (base_ref[...].astype(jnp.float32) + total).astype(jnp.bfloat16)


def paired_layer(n_fs, n_tp):
    def fs_swap(values, mask):
        return lax.ppermute(values, "fs", [(j, j ^ mask) for j in range(n_fs)])

    def core_swap(values):
        return lax.ppermute(values, "tp", [(j, j ^ 1) for j in range(n_tp)])

    def swap(values, fs_mask, tp_mask):
        pairs = [
            (a * n_tp + b, (a ^ fs_mask) * n_tp + (b ^ tp_mask))
            for a in range(n_fs)
            for b in range(n_tp)
        ]
        return lax.ppermute(values, ("fs", "tp"), pairs)

    def gather(mine, other):
        got = []
        for back in range(n_fs // 2):
            piece = mine
            if back:
                pairs = [(a, (a + 2 * back) % n_fs) for a in range(n_fs)]
                piece = lax.ppermute(other if back % 2 else mine, "fs", pairs)
            got += [piece, fs_swap(piece, 1)]
        return got

    def columns_of(shard):
        blocks = []
        for step in range(n_tp):
            pairs = [
                ((a ^ turn_of(b)) * n_tp + (b ^ step), a * n_tp + b)
                for a in range(n_fs)
                for b in range(n_tp)
            ]
            blocks.append(lax.ppermute(shard, ("fs", "tp"), pairs))
        return blocks

    def whole_rows(own):
        near = [own, swap(own, MATE, 0)]
        for step in range(2, n_tp, 2):
            near += [swap(piece, 0, step) for piece in near[:GROUP]]
        across = [core_swap(piece) for piece in near]
        return near + across

    def on_device(
        tokens,
        mix_gain,
        in_x_w,
        in_gate_w,
        conv_taps,
        gate_x_blocks,
        gate_a_blocks,
        forget_rate,
        out_w,
        ffn_gain,
        ffn_gate_w,
        ffn_up_w,
        ffn_down_w,
    ):
        length, width = tokens.shape
        features = n_tp * width
        slots = n_tp // 2 * GROUP
        rows = GROUP * length
        chans = in_x_w.shape[1] // 2
        units = ffn_down_w.shape[0] // 2
        shard = in_x_w.shape[0]
        bf16, f32 = jnp.bfloat16, jnp.float32
        shape = pltpu.VMEM
        normed_scratch = pltpu.VMEM((rows, features), bf16)

        def reduce_out(acts, weights, base):
            deep = weights[0].shape[0]
            send, keep = call(
                project_out_kernel,
                [shape((slots, length, width), bf16)] * 2,
                [acts, *weights],
                [pltpu.VMEM((deep, features), bf16)],
            )
            got = core_swap(send)
            own, *sent = call(
                join_kernel,
                [shape((length, width), f32)] + [shape((length, width), bf16)] * (slots - 1),
                [keep, got],
            )
            arrived = []
            for slot in range(1, slots):
                step, far = slot // GROUP * 2, slot % GROUP
                arrived.append(swap(sent[slot - 1], MATE * far, step))
            return call(finish_kernel, shape((length, width), bf16), [base, own, *arrived])

        in_parts = call(
            split_in_kernel,
            [shape((shard, 2 * chans), bf16)] * 2,
            [in_x_w, in_gate_w],
            space=pltpu.HBM,
        )
        shares = [shape((2 * units, shard), bf16), shape((units, shard), bf16)]
        ffn_parts = call(
            split_ffn_kernel, shares * 2, [ffn_gate_w.T, ffn_up_w.T, ffn_down_w], space=pltpu.HBM
        )
        pieces = whole_rows(tokens)
        in_w = gather(*in_parts)
        out_blocks = columns_of(out_w)
        up_w = gather(ffn_parts[0], ffn_parts[2])
        down_w = gather(ffn_parts[1], ffn_parts[3])
        mixer_out = call(
            functools.partial(mixer_kernel, len(pieces)),
            shape((rows, chans), bf16),
            [
                mix_gain[None],
                conv_taps,
                gate_x_blocks,
                gate_a_blocks,
                forget_rate[None],
                *pieces,
                *in_w,
            ],
            [normed_scratch, pltpu.VMEM((length + 8, chans), f32)],
        )
        mixed = whole_rows(mixer_out)
        after_mix = call(
            functools.partial(mix_project_kernel, len(pieces)),
            shape((rows, shard), bf16),
            [*mixed, *pieces, *out_blocks],
        )
        hidden, own = call(
            functools.partial(hidden_kernel, len(pieces)),
            [shape((rows, units), bf16), shape((length, width), bf16)],
            [ffn_gain[None], *whole_rows(after_mix), *up_w],
            [normed_scratch, pltpu.VMEM((length, features), bf16)],
        )
        return reduce_out(hidden, down_w, own)

    return on_device


def solution(mesh):
    n_fs, n_tp = mesh.shape["fs"], mesh.shape["tp"]
    placed = (
        P("fs", "tp"),
        P(),
        P("fs", "tp"),
        P("fs", "tp"),
        P(None, "tp"),
        P("tp", None, None),
        P("tp", None, None),
        P("tp"),
        P("tp", "fs"),
        P(),
        P("fs", "tp"),
        P("fs", "tp"),
        P("tp", "fs"),
    )
    made = sorted(turn_of(tp) ^ mate for tp in range(n_tp) for mate in (0, MATE))
    paired = made == list(range(n_fs))
    mapped = functools.partial(
        jax.shard_map, mesh=mesh, in_specs=placed, out_specs=P("fs", "tp"), check_vma=False
    )
    if paired:
        return mapped(paired_layer(n_fs, n_tp))
    return mapped(gathered_layer)
```

time: 375 us -> 151 us (0.40)
  waiting for transfers between devices: 325 us -> 88.9 us
  starting transfers between devices: 0.3 us -> 52 us
  blocking collectives: 16.9 us -> 0 us
  matrix products: 13.9 us -> 0 us
  between operations: 14 us -> 0.16 us
  Pallas kernels: 0 us -> 8.22 us
    all_gather x6 -> x0, waiting for transfers between devices: 281 us -> none  [the longest x2 96.2 us: project_out(): lax.all_gather(weight, 'fs', axis=1, tiled=True)]
    ppermute x0 -> x50, waiting for transfers between devices: none -> 88.9 us  [the longest x9 40 us: gather(): piece = lax.ppermute(other if back % 2 else mine, 'fs', pairs)]
    ppermute x0 -> x50, starting transfers between devices: none -> 52 us  [the longest x12 17.7 us: swap(): return lax.ppermute(values, ('fs', 'tp'), pairs)]
    reduce_scatter x2 -> x0, waiting for transfers between devices: 40.1 us -> none  [project_out(): lax.psum_scatter(partial_terms.astype(jnp.bfloat16), 'tp', scatter_dimens...]
    all_gather x2 -> x0, blocking collectives: 16.9 us -> none  [full_rows(): return lax.all_gather(shard, 'tp', axis=1, tiled=True)]
    dot_general x6 -> x0, matrix products: 13.9 us -> none  [the longest x2 8.98 us: project_out(): jnp.dot(acts, lax.all_gather(weight, 'fs', axis=1, tiled=True), preferred...]
    pallas_call x0 -> x8, Pallas kernels: none -> 8.22 us  [call(): pl.pallas_call(kernel, out_shape=outs, in_specs=[spec] * len(args), out_s...]
    unnamed x8 -> x0, waiting for transfers between devices: 3.84 us -> none
  transfers between devices with their start and end apart: 8 -> 50, of which waited for: 8 -> 20; matrix products, arithmetic and copies ran while one was open for 2% -> 0% of each run, Pallas kernels for 0% -> 4%
where the time goes in v1:
time: 151 us
  waiting for transfers between devices  88.9 us (59%)
  starting transfers between devices  52 us (34%)
  Pallas kernels  8.22 us (5%)
    ppermute x9, waiting for transfers between devices, gather(): piece = lax.ppermute(other if back % 2 else mine, 'fs', pairs)  40 us
    ppermute x12, waiting for transfers between devices, fs_swap(): return lax.ppermute(values, 'fs', [(j, j ^ mask) for j in range(n_fs)])  26 us
    ppermute x12, starting transfers between devices, swap(): return lax.ppermute(values, ('fs', 'tp'), pairs)  17.7 us
    ppermute x12, waiting for transfers between devices, swap(): return lax.ppermute(values, ('fs', 'tp'), pairs)  12.9 us
    ppermute x12, starting transfers between devices, fs_swap(): return lax.ppermute(values, 'fs', [(j, j ^ mask) for j in range(n_fs)])  12.8 us
    ppermute x9, starting transfers between devices, gather(): piece = lax.ppermute(other if back % 2 else mine, 'fs', pairs)  11.6 us
    pallas_call x8, Pallas kernels, call(): pl.pallas_call(kernel, out_shape=outs, in_specs=[spec] * len(args), out_s...  8.22 us
    ppermute x4, starting transfers between devices, columns_of(): blocks.append(lax.ppermute(shard, ('fs', 'tp'), pairs))  6.42 us
  transfers between devices with their start and end apart: 50, of which 20 were waited for; matrix products, arithmetic and copies ran while one was open for 0% of the time, Pallas kernels for 4%

profile of v1, /device:TPU:0, one launch (start us, length us, event | category | flops | bytes accessed | tf_op | source)
XLA Modules:
  0.0 150.6 jit_solution(17904919852184435201)
XLA Ops:
  0.0 1.1 shard_map.127
  1.1 4.1 %collective-permute-start.10 = (bf16[256,256]{1,0:T(8,128)(2,1)S(1)}, bf16[256,256]{1,0:T(8,128)(2,1)S(1)}, u32[]{:S(2)}, u32[]{:S(2)}) collective-permute-start(bf16[256,256]{1,0:T(8,128)(2,1)S(1)} %get-tuple-element.19.rest_8_), channel_id=1, source_target_pairs={{0,16},{4,20},{8,24},{12,28},{16,0},{20,4},{24,8},{28,12},{1,17},{... | collective-permute-start | bytes 393224 | tf_op jit(solution)/shard_map/ppermute | solution.py:354
  5.2 1.3 collective-permute-start.12
  6.5 0.7 collective-permute-start.8
  7.2 1.5 %collective-permute-start.7 = (bf16[256,256]{1,0:T(8,128)(2,1)S(1)}, bf16[256,256]{1,0:T(8,128)(2,1)S(1)}, u32[]{:S(2)}, u32[]{:S(2)}) collective-permute-start(bf16[256,256]{1,0:T(8,128)(2,1)S(1)} %get-tuple-element.19.rest_8_), channel_id=1, source_target_pairs={{0,4},{4,0},{8,12},{12,8},{16,20},{20,16},{24,28},{28,24},{1,5},{5... | collective-permute-start | bytes 393224 | tf_op jit(solution)/shard_map/ppermute | solution.py:335
  8.7 1.6 %collective-permute-start.21 = (bf16[256,256]{1,0:T(8,128)(2,1)}, bf16[256,256]{1,0:T(8,128)(2,1)S(1)}, u32[]{:S(2)}, u32[]{:S(2)}) collective-permute-start(bf16[256,256]{1,0:T(8,128)(2,1)} %param.21), channel_id=1, source_target_pairs={{0,0},{21,1},{6,2},{19,3},{4,4},{17,5},{2,6},{23,7},{8,8},{29,9},{... | collective-permute-start | bytes 393224 | tf_op jit(solution)/shard_map/ppermute | solution.py:366
  10.3 2.9 %collective-permute-done.10.rest_12_ = bf16[256,256]{1,0:T(8,128)(2,1)S(1)} collective-permute-done((bf16[256,256]{1,0:T(8,128)(2,1)S(1)}, bf16[256,256]{1,0:T(8,128)(2,1)S(1)}, u32[]{:S(2)}, u32[]{:S(2)}) %collective-permute-start.10) | collective-permute-done | bytes 131104 | tf_op jit(solution)/shard_map/ppermute | solution.py:354
  13.2 6.9 %collective-permute-start = (bf16[160,512]{1,0:T(8,128)(2,1)S(1)}, bf16[160,512]{1,0:T(8,128)(2,1)S(1)}, u32[]{:S(2)}, u32[]{:S(2)}) collective-permute-start(bf16[160,512]{1,0:T(8,128)(2,1)S(1)} %copy-done), channel_id=1, source_target_pairs={{0,8},{1,9},{2,10},{3,11},{4,12},{5,13},{6,14},{7,15},{8,0},{9,1},... | collective-permute-start | bytes 491528 | tf_op jit(solution)/shard_map/ppermute | solution.py:346
  20.1 2.6 %collective-permute-start.23 = (bf16[256,256]{1,0:T(8,128)(2,1)}, bf16[256,256]{1,0:T(8,128)(2,1)S(1)}, u32[]{:S(2)}, u32[]{:S(2)}) collective-permute-start(bf16[256,256]{1,0:T(8,128)(2,1)} %param.21), channel_id=1, source_target_pairs={{2,0},{23,1},{4,2},{17,3},{6,4},{19,5},{0,6},{21,7},{10,8},{31,9},... | collective-permute-start | bytes 393224 | tf_op jit(solution)/shard_map/ppermute | solution.py:366
  22.7 1.8 %collective-permute-start.3 = (bf16[160,512]{1,0:T(8,128)(2,1)S(1)}, bf16[160,512]{1,0:T(8,128)(2,1)S(1)}, u32[]{:S(2)}, u32[]{:S(2)}) collective-permute-start(bf16[160,512]{1,0:T(8,128)(2,1)S(1)} %copy-done), channel_id=1, source_target_pairs={{0,1},{1,0},{2,3},{3,2},{4,5},{5,4},{6,7},{7,6},{8,9},{9,8},{10,11... | collective-permute-start | bytes 491528 | tf_op jit(solution)/shard_map/ppermute | solution.py:338
  24.5 2.2 %collective-permute-start.24 = (bf16[256,256]{1,0:T(8,128)(2,1)}, bf16[256,256]{1,0:T(8,128)(2,1)S(1)}, u32[]{:S(2)}, u32[]{:S(2)}) collective-permute-start(bf16[256,256]{1,0:T(8,128)(2,1)} %param.21), channel_id=1, source_target_pairs={{3,0},{22,1},{5,2},{16,3},{7,4},{18,5},{1,6},{20,7},{11,8},{30,9},... | collective-permute-start | bytes 393224 | tf_op jit(solution)/shard_map/ppermute | solution.py:366
  26.7 0.7 collective-permute-start.2
  27.4 1.1 collective-permute-start.11
  28.6 5.3 %collective-permute-done.24.refs_19_ = bf16[256,256]{1,0:T(8,128)(2,1)S(1)} collective-permute-done((bf16[256,256]{1,0:T(8,128)(2,1)}, bf16[256,256]{1,0:T(8,128)(2,1)S(1)}, u32[]{:S(2)}, u32[]{:S(2)}) %collective-permute-start.24) | collective-permute-done | bytes 131104 | tf_op jit(solution)/shard_map/ppermute | solution.py:366
  33.8 2.0 %collective-permute-start.13 = (bf16[256,256]{1,0:T(8,128)(2,1)S(1)}, bf16[256,256]{1,0:T(8,128)(2,1)S(1)}, u32[]{:S(2)}, u32[]{:S(2)}) collective-permute-start(bf16[256,256]{1,0:T(8,128)(2,1)S(1)} %collective-permute-done.12.rest_14_), channel_id=1, source_target_pairs={{0,4},{4,0},{8,12},{12,8},{16,20},{20,16},{24,28},{28,24},{1,5},{5... | collective-permute-start | bytes 393224 | tf_op jit(solution)/shard_map/ppermute | solution.py:335
  35.9 0.2 collective-permute-start.5
  36.1 0.3 collective-permute-start.6
  36.4 1.3 shard_map.130
  37.7 2.5 %collective-permute-done.13.rest_15_ = bf16[256,256]{1,0:T(8,128)(2,1)S(1)} collective-permute-done((bf16[256,256]{1,0:T(8,128)(2,1)S(1)}, bf16[256,256]{1,0:T(8,128)(2,1)S(1)}, u32[]{:S(2)}, u32[]{:S(2)}) %collective-permute-start.13) | collective-permute-done | bytes 131104 | tf_op jit(solution)/shard_map/ppermute | solution.py:335
  40.2 1.0 collective-permute-start.35
  41.2 1.6 %collective-permute-done.9.rest_11_ = bf16[256,256]{1,0:T(8,128)(2,1)S(1)} collective-permute-done((bf16[256,256]{1,0:T(8,128)(2,1)S(1)}, bf16[256,256]{1,0:T(8,128)(2,1)S(1)}, u32[]{:S(2)}, u32[]{:S(2)}) %collective-permute-start.9) | collective-permute-done | bytes 131104 | tf_op jit(solution)/shard_map/ppermute | solution.py:335
  42.8 3.8 %collective-permute-start.37 = (bf16[704,256]{1,0:T(8,128)(2,1)S(1)}, bf16[704,256]{1,0:T(8,128)(2,1)S(1)}, u32[]{:S(2)}, u32[]{:S(2)}) collective-permute-start(bf16[704,256]{1,0:T(8,128)(2,1)S(1)} %get-tuple-element.22), channel_id=1, source_target_pairs={{0,24},{4,28},{8,0},{12,4},{16,8},{20,12},{24,16},{28,20},{1,25},{... | collective-permute-start | bytes 1081352 | tf_op jit(solution)/shard_map/ppermute | solution.py:354
  46.6 0.6 collective-permute-start.40
  47.3 0.7 copy-done.6
  47.9 1.7 %shard_map.128.refs_0_ = bf16[320,128]{1,0:T(8,128)(2,1)S(1)} custom-call(f32[1,2048]{1,0:T(1,128)S(1)} %bitcast.5, f32[4,256]{1,0:T(4,128)S(1)} %copy-done.5, bf16[2,128,128]{2,1,0:T(8,128)(2,1)S(1)} %copy-done.1, bf16[2,128,128]{2,1,0:T(8,128)(2,1)S(1)} %copy-done.2, f32[1,256]{1,0:T(1,128)S(1)} %bitcast.7, bf16[160,512]{1,0:T(8,128)(2,1)S(1)} %copy-done, ...), custom_call_target="tpu_custom_call" | custom-call | tf_op jit(solution)/shard_map/pallas_call | solution.py:110
  49.6 35.2 %collective-permute-done.42.rest_4_ = bf16[352,256]{1,0:T(8,128)(2,1)S(1)} collective-permute-done((bf16[352,256]{1,0:T(8,128)(2,1)S(1)}, bf16[352,256]{1,0:T(8,128)(2,1)S(1)}, u32[]{:S(2)}, u32[]{:S(2)}) %collective-permute-start.42) | collective-permute-done | bytes 180256 | tf_op jit(solution)/shard_map/ppermute | solution.py:354
  84.8 0.4 collective-permute-start.32
  85.2 1.6 %collective-permute-start.15 = (bf16[320,128]{1,0:T(8,128)(2,1)S(1)}, bf16[320,128]{1,0:T(8,128)(2,1)S(1)}, u32[]{:S(2)}, u32[]{:S(2)}) collective-permute-start(bf16[320,128]{1,0:T(8,128)(2,1)S(1)} %shard_map.128.refs_0_), channel_id=1, source_target_pairs={{0,2},{1,3},{2,0},{3,1},{4,6},{5,7},{6,4},{7,5},{8,10},{9,11},{10,... | collective-permute-start | bytes 245768 | tf_op jit(solution)/shard_map/ppermute | solution.py:346
  86.8 2.4 %collective-permute-done.14.refs_1_ = bf16[320,128]{1,0:T(8,128)(2,1)S(1)} collective-permute-done((bf16[320,128]{1,0:T(8,128)(2,1)S(1)}, bf16[320,128]{1,0:T(8,128)(2,1)S(1)}, u32[]{:S(2)}, u32[]{:S(2)}) %collective-permute-start.14) | collective-permute-done | bytes 81952 | tf_op jit(solution)/shard_map/ppermute | solution.py:346
  89.2 0.4 collective-permute-start.16
  89.6 0.5 collective-permute-start.19
  90.1 1.6 %collective-permute-start.36 = (bf16[704,256]{1,0:T(8,128)(2,1)S(1)}, bf16[704,256]{1,0:T(8,128)(2,1)S(1)}, u32[]{:S(2)}, u32[]{:S(2)}) collective-permute-start(bf16[704,256]{1,0:T(8,128)(2,1)S(1)} %collective-permute-done.35.rest_12_), channel_id=1, source_target_pairs={{0,4},{4,0},{8,12},{12,8},{16,20},{20,16},{24,28},{28,24},{1,5},{5... | collective-permute-start | bytes 1081352 | tf_op jit(solution)/shard_map/ppermute | solution.py:335
  91.7 1.9 %collective-permute-done.16.refs_3_ = bf16[320,128]{1,0:T(8,128)(2,1)S(1)} collective-permute-done((bf16[320,128]{1,0:T(8,128)(2,1)S(1)}, bf16[320,128]{1,0:T(8,128)(2,1)S(1)}, u32[]{:S(2)}, u32[]{:S(2)}) %collective-permute-start.16) | collective-permute-done | bytes 81952 | tf_op jit(solution)/shard_map/ppermute | solution.py:346
  93.7 0.4 collective-permute-start.34
  94.1 1.3 collective-permute-done.20.refs_7_
  95.4 1.7 %collective-permute-start.38 = (bf16[704,256]{1,0:T(8,128)(2,1)S(1)}, bf16[704,256]{1,0:T(8,128)(2,1)S(1)}, u32[]{:S(2)}, u32[]{:S(2)}) collective-permute-start(bf16[704,256]{1,0:T(8,128)(2,1)S(1)} %collective-permute-done.37.rest_14_), channel_id=1, source_target_pairs={{0,4},{4,0},{8,12},{12,8},{16,20},{20,16},{24,28},{28,24},{1,5},{5... | collective-permute-start | bytes 1081352 | tf_op jit(solution)/shard_map/ppermute | solution.py:335
  97.1 0.5 shard_map.129.rest_0_
  97.6 2.0 %collective-permute-done.44.rest_6_ = bf16[352,256]{1,0:T(8,128)(2,1)S(1)} collective-permute-done((bf16[352,256]{1,0:T(8,128)(2,1)S(1)}, bf16[352,256]{1,0:T(8,128)(2,1)S(1)}, u32[]{:S(2)}, u32[]{:S(2)}) %collective-permute-start.44) | collective-permute-done | bytes 180256 | tf_op jit(solution)/shard_map/ppermute | solution.py:354
  99.5 1.3 collective-permute-start.25
  100.9 1.7 %collective-permute-start.26 = (bf16[320,256]{1,0:T(8,128)(2,1)S(1)}, bf16[320,256]{1,0:T(8,128)(2,1)S(1)}, u32[]{:S(2)}, u32[]{:S(2)}) collective-permute-start(bf16[320,256]{1,0:T(8,128)(2,1)S(1)} %shard_map.129.rest_0_), channel_id=1, source_target_pairs={{0,2},{1,3},{2,0},{3,1},{4,6},{5,7},{6,4},{7,5},{8,10},{9,11},{10,... | collective-permute-start | bytes 491528 | tf_op jit(solution)/shard_map/ppermute | solution.py:346
  102.5 1.3 collective-permute-done.36.rest_13_
  103.8 1.0 collective-permute-done.25.rest_1_
  104.9 1.6 %collective-permute-start.27 = (bf16[320,256]{1,0:T(8,128)(2,1)S(1)}, bf16[320,256]{1,0:T(8,128)(2,1)S(1)}, u32[]{:S(2)}, u32[]{:S(2)}) collective-permute-start(bf16[320,256]{1,0:T(8,128)(2,1)S(1)} %collective-permute-done.25.rest_1_), channel_id=1, source_target_pairs={{0,2},{1,3},{2,0},{3,1},{4,6},{5,7},{6,4},{7,5},{8,10},{9,11},{10,... | collective-permute-start | bytes 491528 | tf_op jit(solution)/shard_map/ppermute | solution.py:346
  106.5 5.1 %collective-permute-done.34.rest_11_ = bf16[704,256]{1,0:T(8,128)(2,1)S(1)} collective-permute-done((bf16[704,256]{1,0:T(8,128)(2,1)S(1)}, bf16[704,256]{1,0:T(8,128)(2,1)S(1)}, u32[]{:S(2)}, u32[]{:S(2)}) %collective-permute-start.34) | collective-permute-done | bytes 360480 | tf_op jit(solution)/shard_map/ppermute | solution.py:335
  111.5 0.5 collective-permute-start.30
  112.0 6.3 %collective-permute-done.38.rest_15_ = bf16[704,256]{1,0:T(8,128)(2,1)S(1)} collective-permute-done((bf16[704,256]{1,0:T(8,128)(2,1)S(1)}, bf16[704,256]{1,0:T(8,128)(2,1)S(1)}, u32[]{:S(2)}, u32[]{:S(2)}) %collective-permute-start.38) | collective-permute-done | bytes 360480 | tf_op jit(solution)/shard_map/ppermute | solution.py:335
  118.3 0.4 collective-permute-start.39
  118.7 1.7 %collective-permute-start.43 = (bf16[352,256]{1,0:T(8,128)(2,1)S(1)}, bf16[352,256]{1,0:T(8,128)(2,1)S(1)}, u32[]{:S(2)}, u32[]{:S(2)}) collective-permute-start(bf16[352,256]{1,0:T(8,128)(2,1)S(1)} %collective-permute-done.42.rest_4_), channel_id=1, source_target_pairs={{0,4},{4,0},{8,12},{12,8},{16,20},{20,16},{24,28},{28,24},{1,5},{5... | collective-permute-start | bytes 540680 | tf_op jit(solution)/shard_map/ppermute | solution.py:335
  120.3 0.4 collective-permute-start.41
  120.7 1.7 %collective-permute-start.45 = (bf16[352,256]{1,0:T(8,128)(2,1)S(1)}, bf16[352,256]{1,0:T(8,128)(2,1)S(1)}, u32[]{:S(2)}, u32[]{:S(2)}) collective-permute-start(bf16[352,256]{1,0:T(8,128)(2,1)S(1)} %collective-permute-done.44.rest_6_), channel_id=1, source_target_pairs={{0,4},{4,0},{8,12},{12,8},{16,20},{20,16},{24,28},{28,24},{1,5},{5... | collective-permute-start | bytes 540680 | tf_op jit(solution)/shard_map/ppermute | solution.py:335
  122.4 1.4 collective-permute-done.31.rest_7_
  123.8 2.4 %shard_map.131 = (bf16[320,352]{1,0:T(8,128)(2,1)S(1)}, bf16[160,512]{1,0:T(8,128)(2,1)S(1)}) custom-call(f32[1,2048]{1,0:T(1,128)S(1)} %bitcast.6, bf16[320,256]{1,0:T(8,128)(2,1)S(1)} %shard_map.129.rest_0_, bf16[320,256]{1,0:T(8,128)(2,1)S(1)} %collective-permute-done.25.rest_1_, bf16[320,256]{1,0:T(8,128)(2,1)S(1)} %collective-permute-done.26.rest_2_, ...), custom_call_target="tpu_custom_call" | custom-call | tf_op jit(solution)/shard_map/pallas_call | solution.py:110
  126.2 3.4 %collective-permute-done.43.rest_5_ = bf16[352,256]{1,0:T(8,128)(2,1)S(1)} collective-permute-done((bf16[352,256]{1,0:T(8,128)(2,1)S(1)}, bf16[352,256]{1,0:T(8,128)(2,1)S(1)}, u32[]{:S(2)}, u32[]{:S(2)}) %collective-permute-start.43) | collective-permute-done | bytes 180256 | tf_op jit(solution)/shard_map/ppermute | solution.py:335
  129.6 3.9 %collective-permute-done.41.rest_3_ = bf16[352,256]{1,0:T(8,128)(2,1)S(1)} collective-permute-done((bf16[352,256]{1,0:T(8,128)(2,1)S(1)}, bf16[352,256]{1,0:T(8,128)(2,1)S(1)}, u32[]{:S(2)}, u32[]{:S(2)}) %collective-permute-start.41) | collective-permute-done | bytes 180256 | tf_op jit(solution)/shard_map/ppermute | solution.py:335
  133.4 2.1 %collective-permute-done.45.rest_7_ = bf16[352,256]{1,0:T(8,128)(2,1)S(1)} collective-permute-done((bf16[352,256]{1,0:T(8,128)(2,1)S(1)}, bf16[352,256]{1,0:T(8,128)(2,1)S(1)}, u32[]{:S(2)}, u32[]{:S(2)}) %collective-permute-start.45) | collective-permute-done | bytes 180256 | tf_op jit(solution)/shard_map/ppermute | solution.py:335
  135.5 1.0 shard_map.132
  136.6 2.1 %collective-permute-done.46.got_ref = bf16[4,160,512]{2,1,0:T(8,128)(2,1)S(1)} collective-permute-done((bf16[4,160,512]{2,1,0:T(8,128)(2,1)S(1)}, bf16[4,160,512]{2,1,0:T(8,128)(2,1)S(1)}, u32[]{:S(2)}, u32[]{:S(2)}) %collective-permute-start.46) | collective-permute-done | bytes 655392 | tf_op jit(solution)/shard_map/ppermute | solution.py:338
  138.7 0.1 shard_map.133
  138.9 1.5 %collective-permute-start.47 = (bf16[160,512]{1,0:T(8,128)(2,1)S(1)}, bf16[160,512]{1,0:T(8,128)(2,1)S(1)}, u32[]{:S(2)}, u32[]{:S(2)}) collective-permute-start(bf16[160,512]{1,0:T(8,128)(2,1)S(1)} %get-tuple-element.30), channel_id=1, source_target_pairs={{0,8},{1,9},{2,10},{3,11},{4,12},{5,13},{6,14},{7,15},{8,0},{9,1},... | collective-permute-start | bytes 491528 | tf_op jit(solution)/shard_map/ppermute | solution.py:346
  140.4 1.2 collective-permute-start.48
  141.6 0.8 collective-permute-start.49
  142.4 3.6 %collective-permute-done.47.rest_0_ = bf16[160,512]{1,0:T(8,128)(2,1)S(1)} collective-permute-done((bf16[160,512]{1,0:T(8,128)(2,1)S(1)}, bf16[160,512]{1,0:T(8,128)(2,1)S(1)}, u32[]{:S(2)}, u32[]{:S(2)}) %collective-permute-start.47) | collective-permute-done | bytes 163872 | tf_op jit(solution)/shard_map/ppermute | solution.py:346
  146.0 3.9 %collective-permute-done.48.rest_1_ = bf16[160,512]{1,0:T(8,128)(2,1)S(1)} collective-permute-done((bf16[160,512]{1,0:T(8,128)(2,1)S(1)}, bf16[160,512]{1,0:T(8,128)(2,1)S(1)}, u32[]{:S(2)}, u32[]{:S(2)}) %collective-permute-start.48) | collective-permute-done | bytes 163872 | tf_op jit(solution)/shard_map/ppermute | solution.py:346
  150.0 0.7 copy.14
  (59 shorter events, 0.5 us)
Async XLA Ops:
  0.0 13.2 %copy-start = (bf16[160,512]{1,0:T(8,128)(2,1)S(1)}, bf16[160,512]{1,0:T(8,128)(2,1)}, u32[]{:S(2)}) copy-start(bf16[160,512]{1,0:T(8,128)(2,1)} %refs_8_.1) | copy-start | bytes 491524
  1.1 12.1 %collective-permute-start.10 = (bf16[256,256]{1,0:T(8,128)(2,1)S(1)}, bf16[256,256]{1,0:T(8,128)(2,1)S(1)}, u32[]{:S(2)}, u32[]{:S(2)}) collective-permute-start(bf16[256,256]{1,0:T(8,128)(2,1)S(1)} %get-tuple-element.19.rest_8_), channel_id=1, source_target_pairs={{0,16},{4,20},{8,24},{12,28},{16,0},{20,4},{24,8},{28,12},{1,17},{... | collective-permute-start | bytes 393224 | tf_op jit(solution)/shard_map/ppermute | solution.py:354
  5.2 8.0 %collective-permute-start.12 = (bf16[256,256]{1,0:T(8,128)(2,1)S(1)}, bf16[256,256]{1,0:T(8,128)(2,1)S(1)}, u32[]{:S(2)}, u32[]{:S(2)}) collective-permute-start(bf16[256,256]{1,0:T(8,128)(2,1)S(1)} %get-tuple-element.20), channel_id=1, source_target_pairs={{0,24},{4,28},{8,0},{12,4},{16,8},{20,12},{24,16},{28,20},{1,25},{... | collective-permute-start | bytes 393224 | tf_op jit(solution)/shard_map/ppermute | solution.py:354
  6.5 13.5 %collective-permute-start.8 = (bf16[256,256]{1,0:T(8,128)(2,1)S(1)}, bf16[256,256]{1,0:T(8,128)(2,1)S(1)}, u32[]{:S(2)}, u32[]{:S(2)}) collective-permute-start(bf16[256,256]{1,0:T(8,128)(2,1)S(1)} %get-tuple-element.20), channel_id=1, source_target_pairs={{0,8},{4,12},{8,16},{12,20},{16,24},{20,28},{24,0},{28,4},{1,9},{5... | collective-permute-start | bytes 393224 | tf_op jit(solution)/shard_map/ppermute | solution.py:354
  7.2 15.5 %collective-permute-start.7 = (bf16[256,256]{1,0:T(8,128)(2,1)S(1)}, bf16[256,256]{1,0:T(8,128)(2,1)S(1)}, u32[]{:S(2)}, u32[]{:S(2)}) collective-permute-start(bf16[256,256]{1,0:T(8,128)(2,1)S(1)} %get-tuple-element.19.rest_8_), channel_id=1, source_target_pairs={{0,4},{4,0},{8,12},{12,8},{16,20},{20,16},{24,28},{28,24},{1,5},{5... | collective-permute-start | bytes 393224 | tf_op jit(solution)/shard_map/ppermute | solution.py:335
  8.7 14.0 %collective-permute-start.21 = (bf16[256,256]{1,0:T(8,128)(2,1)}, bf16[256,256]{1,0:T(8,128)(2,1)S(1)}, u32[]{:S(2)}, u32[]{:S(2)}) collective-permute-start(bf16[256,256]{1,0:T(8,128)(2,1)} %param.21), channel_id=1, source_target_pairs={{0,0},{21,1},{6,2},{19,3},{4,4},{17,5},{2,6},{23,7},{8,8},{29,9},{... | collective-permute-start | bytes 393224 | tf_op jit(solution)/shard_map/ppermute | solution.py:366
  13.2 11.3 %collective-permute-start.22 = (bf16[256,256]{1,0:T(8,128)(2,1)}, bf16[256,256]{1,0:T(8,128)(2,1)S(1)}, u32[]{:S(2)}, u32[]{:S(2)}) collective-permute-start(bf16[256,256]{1,0:T(8,128)(2,1)} %param.21), channel_id=1, source_target_pairs={{1,0},{20,1},{7,2},{18,3},{5,4},{16,5},{3,6},{22,7},{9,8},{28,9},{... | collective-permute-start | bytes 393224 | tf_op jit(solution)/shard_map/ppermute | solution.py:366
  13.2 13.6 %collective-permute-start = (bf16[160,512]{1,0:T(8,128)(2,1)S(1)}, bf16[160,512]{1,0:T(8,128)(2,1)S(1)}, u32[]{:S(2)}, u32[]{:S(2)}) collective-permute-start(bf16[160,512]{1,0:T(8,128)(2,1)S(1)} %copy-done), channel_id=1, source_target_pairs={{0,8},{1,9},{2,10},{3,11},{4,12},{5,13},{6,14},{7,15},{8,0},{9,1},... | collective-permute-start | bytes 491528 | tf_op jit(solution)/shard_map/ppermute | solution.py:346
  20.1 7.4 %collective-permute-start.23 = (bf16[256,256]{1,0:T(8,128)(2,1)}, bf16[256,256]{1,0:T(8,128)(2,1)S(1)}, u32[]{:S(2)}, u32[]{:S(2)}) collective-permute-start(bf16[256,256]{1,0:T(8,128)(2,1)} %param.21), channel_id=1, source_target_pairs={{2,0},{23,1},{4,2},{17,3},{6,4},{19,5},{0,6},{21,7},{10,8},{31,9},... | collective-permute-start | bytes 393224 | tf_op jit(solution)/shard_map/ppermute | solution.py:366
  22.7 11.1 %collective-permute-start.1 = (bf16[160,512]{1,0:T(8,128)(2,1)S(1)}, bf16[160,512]{1,0:T(8,128)(2,1)S(1)}, u32[]{:S(2)}, u32[]{:S(2)}) collective-permute-start(bf16[160,512]{1,0:T(8,128)(2,1)S(1)} %copy-done), channel_id=1, source_target_pairs={{0,2},{1,3},{2,0},{3,1},{4,6},{5,7},{6,4},{7,5},{8,10},{9,11},{10,... | collective-permute-start | bytes 491528 | tf_op jit(solution)/shard_map/ppermute | solution.py:346
  22.7 13.1 %collective-permute-start.3 = (bf16[160,512]{1,0:T(8,128)(2,1)S(1)}, bf16[160,512]{1,0:T(8,128)(2,1)S(1)}, u32[]{:S(2)}, u32[]{:S(2)}) collective-permute-start(bf16[160,512]{1,0:T(8,128)(2,1)S(1)} %copy-done), channel_id=1, source_target_pairs={{0,1},{1,0},{2,3},{3,2},{4,5},{5,4},{6,7},{7,6},{8,9},{9,8},{10,11... | collective-permute-start | bytes 491528 | tf_op jit(solution)/shard_map/ppermute | solution.py:338
  24.5 9.3 %collective-permute-start.24 = (bf16[256,256]{1,0:T(8,128)(2,1)}, bf16[256,256]{1,0:T(8,128)(2,1)S(1)}, u32[]{:S(2)}, u32[]{:S(2)}) collective-permute-start(bf16[256,256]{1,0:T(8,128)(2,1)} %param.21), channel_id=1, source_target_pairs={{3,0},{22,1},{5,2},{16,3},{7,4},{18,5},{1,6},{20,7},{11,8},{30,9},... | collective-permute-start | bytes 393224 | tf_op jit(solution)/shard_map/ppermute | solution.py:366
  26.7 9.4 %collective-permute-start.2 = (bf16[160,512]{1,0:T(8,128)(2,1)S(1)}, bf16[160,512]{1,0:T(8,128)(2,1)S(1)}, u32[]{:S(2)}, u32[]{:S(2)}) collective-permute-start(bf16[160,512]{1,0:T(8,128)(2,1)S(1)} %collective-permute-done.rest_1_.refs_9_), channel_id=1, source_target_pairs={{0,2},{1,3},{2,0},{3,1},{4,6},{5,7},{6,4},{7,5},{8,10},{9,11},{10,... | collective-permute-start | bytes 491528 | tf_op jit(solution)/shard_map/ppermute | solution.py:346
  27.4 8.5 %collective-permute-start.11 = (bf16[256,256]{1,0:T(8,128)(2,1)S(1)}, bf16[256,256]{1,0:T(8,128)(2,1)S(1)}, u32[]{:S(2)}, u32[]{:S(2)}) collective-permute-start(bf16[256,256]{1,0:T(8,128)(2,1)S(1)} %collective-permute-done.10.rest_12_), channel_id=1, source_target_pairs={{0,4},{4,0},{8,12},{12,8},{16,20},{20,16},{24,28},{28,24},{1,5},{5... | collective-permute-start | bytes 393224 | tf_op jit(solution)/shard_map/ppermute | solution.py:335
  33.8 9.0 %collective-permute-start.4 = (bf16[160,512]{1,0:T(8,128)(2,1)S(1)}, bf16[160,512]{1,0:T(8,128)(2,1)S(1)}, u32[]{:S(2)}, u32[]{:S(2)}) collective-permute-start(bf16[160,512]{1,0:T(8,128)(2,1)S(1)} %collective-permute-done.rest_1_.refs_9_), channel_id=1, source_target_pairs={{0,1},{1,0},{2,3},{3,2},{4,5},{5,4},{6,7},{7,6},{8,9},{9,8},{10,11... | collective-permute-start | bytes 491528 | tf_op jit(solution)/shard_map/ppermute | solution.py:338
  33.8 6.4 %collective-permute-start.13 = (bf16[256,256]{1,0:T(8,128)(2,1)S(1)}, bf16[256,256]{1,0:T(8,128)(2,1)S(1)}, u32[]{:S(2)}, u32[]{:S(2)}) collective-permute-start(bf16[256,256]{1,0:T(8,128)(2,1)S(1)} %collective-permute-done.12.rest_14_), channel_id=1, source_target_pairs={{0,4},{4,0},{8,12},{12,8},{16,20},{20,16},{24,28},{28,24},{1,5},{5... | collective-permute-start | bytes 393224 | tf_op jit(solution)/shard_map/ppermute | solution.py:335
  35.8 7.0 %collective-permute-start.9 = (bf16[256,256]{1,0:T(8,128)(2,1)S(1)}, bf16[256,256]{1,0:T(8,128)(2,1)S(1)}, u32[]{:S(2)}, u32[]{:S(2)}) collective-permute-start(bf16[256,256]{1,0:T(8,128)(2,1)S(1)} %collective-permute-done.8.rest_10_), channel_id=1, source_target_pairs={{0,4},{4,0},{8,12},{12,8},{16,20},{20,16},{24,28},{28,24},{1,5},{5... | collective-permute-start | bytes 393224 | tf_op jit(solution)/shard_map/ppermute | solution.py:335
  35.9 10.7 %collective-permute-start.5 = (bf16[160,512]{1,0:T(8,128)(2,1)S(1)}, bf16[160,512]{1,0:T(8,128)(2,1)S(1)}, u32[]{:S(2)}, u32[]{:S(2)}) collective-permute-start(bf16[160,512]{1,0:T(8,128)(2,1)S(1)} %collective-permute-done.1.rest_2_.refs_10_), channel_id=1, source_target_pairs={{0,1},{1,0},{2,3},{3,2},{4,5},{5,4},{6,7},{7,6},{8,9},{9,8},{10,11... | collective-permute-start | bytes 491528 | tf_op jit(solution)/shard_map/ppermute | solution.py:338
  36.1 10.5 %collective-permute-start.6 = (bf16[160,512]{1,0:T(8,128)(2,1)S(1)}, bf16[160,512]{1,0:T(8,128)(2,1)S(1)}, u32[]{:S(2)}, u32[]{:S(2)}) collective-permute-start(bf16[160,512]{1,0:T(8,128)(2,1)S(1)} %collective-permute-done.2.rest_3_.refs_11_), channel_id=1, source_target_pairs={{0,1},{1,0},{2,3},{3,2},{4,5},{5,4},{6,7},{7,6},{8,9},{9,8},{10,11... | collective-permute-start | bytes 491528 | tf_op jit(solution)/shard_map/ppermute | solution.py:338
  36.4 10.8 %copy-start.1 = (bf16[2,128,128]{2,1,0:T(8,128)(2,1)S(1)}, bf16[2,128,128]{2,1,0:T(8,128)(2,1)}, u32[]{:S(2)}) copy-start(bf16[2,128,128]{2,1,0:T(8,128)(2,1)} %x_maps_ref.1) | copy-start | bytes 196612
  36.4 10.8 %copy-start.2 = (bf16[2,128,128]{2,1,0:T(8,128)(2,1)S(1)}, bf16[2,128,128]{2,1,0:T(8,128)(2,1)}, u32[]{:S(2)}) copy-start(bf16[2,128,128]{2,1,0:T(8,128)(2,1)} %a_maps_ref.1) | copy-start | bytes 196612
  36.4 10.8 %copy-start.5 = (f32[4,256]{1,0:T(4,128)S(1)}, f32[4,256]{1,0:T(4,128)}, u32[]{:S(2)}) copy-start(f32[4,256]{1,0:T(4,128)} %taps_ref.1) | copy-start | bytes 12292
  37.7 9.5 %copy-start.3 = (f32[2048]{0:T(1024)S(1)}, f32[2048]{0:T(1024)}, u32[]{:S(2)}) copy-start(f32[2048]{0:T(1024)} %param.14) | copy-start | bytes 24580
  40.2 45.0 %collective-permute-start.35 = (bf16[704,256]{1,0:T(8,128)(2,1)S(1)}, bf16[704,256]{1,0:T(8,128)(2,1)S(1)}, u32[]{:S(2)}, u32[]{:S(2)}) collective-permute-start(bf16[704,256]{1,0:T(8,128)(2,1)S(1)} %get-tuple-element.21.rest_8_), channel_id=1, source_target_pairs={{0,16},{4,20},{8,24},{12,28},{16,0},{20,4},{24,8},{28,12},{1,17},{... | collective-permute-start | bytes 1081352 | tf_op jit(solution)/shard_map/ppermute | solution.py:354
  42.8 44.0 %collective-permute-start.33 = (bf16[704,256]{1,0:T(8,128)(2,1)S(1)}, bf16[704,256]{1,0:T(8,128)(2,1)S(1)}, u32[]{:S(2)}, u32[]{:S(2)}) collective-permute-start(bf16[704,256]{1,0:T(8,128)(2,1)S(1)} %get-tuple-element.22), channel_id=1, source_target_pairs={{0,8},{4,12},{8,16},{12,20},{16,24},{20,28},{24,0},{28,4},{1,9},{5... | collective-permute-start | bytes 1081352 | tf_op jit(solution)/shard_map/ppermute | solution.py:354
  42.8 46.8 %collective-permute-start.37 = (bf16[704,256]{1,0:T(8,128)(2,1)S(1)}, bf16[704,256]{1,0:T(8,128)(2,1)S(1)}, u32[]{:S(2)}, u32[]{:S(2)}) collective-permute-start(bf16[704,256]{1,0:T(8,128)(2,1)S(1)} %get-tuple-element.22), channel_id=1, source_target_pairs={{0,24},{4,28},{8,0},{12,4},{16,8},{20,12},{24,16},{28,20},{1,25},{... | collective-permute-start | bytes 1081352 | tf_op jit(solution)/shard_map/ppermute | solution.py:354
  46.6 38.2 %collective-permute-start.42 = (bf16[352,256]{1,0:T(8,128)(2,1)S(1)}, bf16[352,256]{1,0:T(8,128)(2,1)S(1)}, u32[]{:S(2)}, u32[]{:S(2)}) collective-permute-start(bf16[352,256]{1,0:T(8,128)(2,1)S(1)} %get-tuple-element.25.rest_0_), channel_id=1, source_target_pairs={{0,16},{4,20},{8,24},{12,28},{16,0},{20,4},{24,8},{28,12},{1,17},{... | collective-permute-start | bytes 540680 | tf_op jit(solution)/shard_map/ppermute | solution.py:354
  46.6 38.2 %collective-permute-start.40 = (bf16[352,256]{1,0:T(8,128)(2,1)S(1)}, bf16[352,256]{1,0:T(8,128)(2,1)S(1)}, u32[]{:S(2)}, u32[]{:S(2)}) collective-permute-start(bf16[352,256]{1,0:T(8,128)(2,1)S(1)} %get-tuple-element.26), channel_id=1, source_target_pairs={{0,8},{4,12},{8,16},{12,20},{16,24},{20,28},{24,0},{28,4},{1,9},{5... | collective-permute-start | bytes 540680 | tf_op jit(solution)/shard_map/ppermute | solution.py:354
  47.3 0.7 copy-start.6
  49.6 74.2 %copy-start.4 = (f32[2048]{0:T(1024)S(1)}, f32[2048]{0:T(1024)}, u32[]{:S(2)}) copy-start(f32[2048]{0:T(1024)} %param.22) | copy-start | bytes 24580
  84.8 4.4 %collective-permute-start.14 = (bf16[320,128]{1,0:T(8,128)(2,1)S(1)}, bf16[320,128]{1,0:T(8,128)(2,1)S(1)}, u32[]{:S(2)}, u32[]{:S(2)}) collective-permute-start(bf16[320,128]{1,0:T(8,128)(2,1)S(1)} %shard_map.128.refs_0_), channel_id=1, source_target_pairs={{0,8},{1,9},{2,10},{3,11},{4,12},{5,13},{6,14},{7,15},{8,0},{9,1},... | collective-permute-start | bytes 245768 | tf_op jit(solution)/shard_map/ppermute | solution.py:346
  84.8 16.1 %collective-permute-start.32 = (bf16[704,256]{1,0:T(8,128)(2,1)S(1)}, bf16[704,256]{1,0:T(8,128)(2,1)S(1)}, u32[]{:S(2)}, u32[]{:S(2)}) collective-permute-start(bf16[704,256]{1,0:T(8,128)(2,1)S(1)} %get-tuple-element.21.rest_8_), channel_id=1, source_target_pairs={{0,4},{4,0},{8,12},{12,8},{16,20},{20,16},{24,28},{28,24},{1,5},{5... | collective-permute-start | bytes 1081352 | tf_op jit(solution)/shard_map/ppermute | solution.py:335
  85.2 4.4 %collective-permute-start.15 = (bf16[320,128]{1,0:T(8,128)(2,1)S(1)}, bf16[320,128]{1,0:T(8,128)(2,1)S(1)}, u32[]{:S(2)}, u32[]{:S(2)}) collective-permute-start(bf16[320,128]{1,0:T(8,128)(2,1)S(1)} %shard_map.128.refs_0_), channel_id=1, source_target_pairs={{0,2},{1,3},{2,0},{3,1},{4,6},{5,7},{6,4},{7,5},{8,10},{9,11},{10,... | collective-permute-start | bytes 245768 | tf_op jit(solution)/shard_map/ppermute | solution.py:346
  86.8 3.3 %collective-permute-start.17 = (bf16[320,128]{1,0:T(8,128)(2,1)S(1)}, bf16[320,128]{1,0:T(8,128)(2,1)S(1)}, u32[]{:S(2)}, u32[]{:S(2)}) collective-permute-start(bf16[320,128]{1,0:T(8,128)(2,1)S(1)} %shard_map.128.refs_0_), channel_id=1, source_target_pairs={{0,1},{1,0},{2,3},{3,2},{4,5},{5,4},{6,7},{7,6},{8,9},{9,8},{10,11... | collective-permute-start | bytes 245768 | tf_op jit(solution)/shard_map/ppermute | solution.py:338
  89.2 4.4 %collective-permute-start.16 = (bf16[320,128]{1,0:T(8,128)(2,1)S(1)}, bf16[320,128]{1,0:T(8,128)(2,1)S(1)}, u32[]{:S(2)}, u32[]{:S(2)}) collective-permute-start(bf16[320,128]{1,0:T(8,128)(2,1)S(1)} %collective-permute-done.14.refs_1_), channel_id=1, source_target_pairs={{0,2},{1,3},{2,0},{3,1},{4,6},{5,7},{6,4},{7,5},{8,10},{9,11},{10,... | collective-permute-start | bytes 245768 | tf_op jit(solution)/shard_map/ppermute | solution.py:346
  89.6 4.4 %collective-permute-start.18 = (bf16[320,128]{1,0:T(8,128)(2,1)S(1)}, bf16[320,128]{1,0:T(8,128)(2,1)S(1)}, u32[]{:S(2)}, u32[]{:S(2)}) collective-permute-start(bf16[320,128]{1,0:T(8,128)(2,1)S(1)} %collective-permute-done.14.refs_1_), channel_id=1, source_target_pairs={{0,1},{1,0},{2,3},{3,2},{4,5},{5,4},{6,7},{7,6},{8,9},{9,8},{10,11... | collective-permute-start | bytes 245768 | tf_op jit(solution)/shard_map/ppermute | solution.py:338
  89.6 4.4 %collective-permute-start.19 = (bf16[320,128]{1,0:T(8,128)(2,1)S(1)}, bf16[320,128]{1,0:T(8,128)(2,1)S(1)}, u32[]{:S(2)}, u32[]{:S(2)}) collective-permute-start(bf16[320,128]{1,0:T(8,128)(2,1)S(1)} %collective-permute-done.15.refs_2_), channel_id=1, source_target_pairs={{0,1},{1,0},{2,3},{3,2},{4,5},{5,4},{6,7},{7,6},{8,9},{9,8},{10,11... | collective-permute-start | bytes 245768 | tf_op jit(solution)/shard_map/ppermute | solution.py:338
  90.1 13.7 %collective-permute-start.36 = (bf16[704,256]{1,0:T(8,128)(2,1)S(1)}, bf16[704,256]{1,0:T(8,128)(2,1)S(1)}, u32[]{:S(2)}, u32[]{:S(2)}) collective-permute-start(bf16[704,256]{1,0:T(8,128)(2,1)S(1)} %collective-permute-done.35.rest_12_), channel_id=1, source_target_pairs={{0,4},{4,0},{8,12},{12,8},{16,20},{20,16},{24,28},{28,24},{1,5},{5... | collective-permute-start | bytes 1081352 | tf_op jit(solution)/shard_map/ppermute | solution.py:335
  93.7 17.9 %collective-permute-start.34 = (bf16[704,256]{1,0:T(8,128)(2,1)S(1)}, bf16[704,256]{1,0:T(8,128)(2,1)S(1)}, u32[]{:S(2)}, u32[]{:S(2)}) collective-permute-start(bf16[704,256]{1,0:T(8,128)(2,1)S(1)} %collective-permute-done.33.rest_10_), channel_id=1, source_target_pairs={{0,4},{4,0},{8,12},{12,8},{16,20},{20,16},{24,28},{28,24},{1,5},{5... | collective-permute-start | bytes 1081352 | tf_op jit(solution)/shard_map/ppermute | solution.py:335
  94.0 5.5 %collective-permute-start.44 = (bf16[352,256]{1,0:T(8,128)(2,1)S(1)}, bf16[352,256]{1,0:T(8,128)(2,1)S(1)}, u32[]{:S(2)}, u32[]{:S(2)}) collective-permute-start(bf16[352,256]{1,0:T(8,128)(2,1)S(1)} %get-tuple-element.26), channel_id=1, source_target_pairs={{0,24},{4,28},{8,0},{12,4},{16,8},{20,12},{24,16},{28,20},{1,25},{... | collective-permute-start | bytes 540680 | tf_op jit(solution)/shard_map/ppermute | solution.py:354
  94.0 1.3 collective-permute-start.20
  95.4 22.9 %collective-permute-start.38 = (bf16[704,256]{1,0:T(8,128)(2,1)S(1)}, bf16[704,256]{1,0:T(8,128)(2,1)S(1)}, u32[]{:S(2)}, u32[]{:S(2)}) collective-permute-start(bf16[704,256]{1,0:T(8,128)(2,1)S(1)} %collective-permute-done.37.rest_14_), channel_id=1, source_target_pairs={{0,4},{4,0},{8,12},{12,8},{16,20},{20,16},{24,28},{28,24},{1,5},{5... | collective-permute-start | bytes 1081352 | tf_op jit(solution)/shard_map/ppermute | solution.py:335
  99.5 5.3 %collective-permute-start.25 = (bf16[320,256]{1,0:T(8,128)(2,1)S(1)}, bf16[320,256]{1,0:T(8,128)(2,1)S(1)}, u32[]{:S(2)}, u32[]{:S(2)}) collective-permute-start(bf16[320,256]{1,0:T(8,128)(2,1)S(1)} %shard_map.129.rest_0_), channel_id=1, source_target_pairs={{0,8},{1,9},{2,10},{3,11},{4,12},{5,13},{6,14},{7,15},{8,0},{9,1},... | collective-permute-start | bytes 491528 | tf_op jit(solution)/shard_map/ppermute | solution.py:346
  100.9 10.7 %collective-permute-start.26 = (bf16[320,256]{1,0:T(8,128)(2,1)S(1)}, bf16[320,256]{1,0:T(8,128)(2,1)S(1)}, u32[]{:S(2)}, u32[]{:S(2)}) collective-permute-start(bf16[320,256]{1,0:T(8,128)(2,1)S(1)} %shard_map.129.rest_0_), channel_id=1, source_target_pairs={{0,2},{1,3},{2,0},{3,1},{4,6},{5,7},{6,4},{7,5},{8,10},{9,11},{10,... | collective-permute-start | bytes 491528 | tf_op jit(solution)/shard_map/ppermute | solution.py:346
  103.8 14.9 %collective-permute-start.28 = (bf16[320,256]{1,0:T(8,128)(2,1)S(1)}, bf16[320,256]{1,0:T(8,128)(2,1)S(1)}, u32[]{:S(2)}, u32[]{:S(2)}) collective-permute-start(bf16[320,256]{1,0:T(8,128)(2,1)S(1)} %shard_map.129.rest_0_), channel_id=1, source_target_pairs={{0,1},{1,0},{2,3},{3,2},{4,5},{5,4},{6,7},{7,6},{8,9},{9,8},{10,11... | collective-permute-start | bytes 491528 | tf_op jit(solution)/shard_map/ppermute | solution.py:338
  104.9 15.5 %collective-permute-start.27 = (bf16[320,256]{1,0:T(8,128)(2,1)S(1)}, bf16[320,256]{1,0:T(8,128)(2,1)S(1)}, u32[]{:S(2)}, u32[]{:S(2)}) collective-permute-start(bf16[320,256]{1,0:T(8,128)(2,1)S(1)} %collective-permute-done.25.rest_1_), channel_id=1, source_target_pairs={{0,2},{1,3},{2,0},{3,1},{4,6},{5,7},{6,4},{7,5},{8,10},{9,11},{10,... | collective-permute-start | bytes 491528 | tf_op jit(solution)/shard_map/ppermute | solution.py:346
  111.5 9.2 %collective-permute-start.29 = (bf16[320,256]{1,0:T(8,128)(2,1)S(1)}, bf16[320,256]{1,0:T(8,128)(2,1)S(1)}, u32[]{:S(2)}, u32[]{:S(2)}) collective-permute-start(bf16[320,256]{1,0:T(8,128)(2,1)S(1)} %collective-permute-done.25.rest_1_), channel_id=1, source_target_pairs={{0,1},{1,0},{2,3},{3,2},{4,5},{5,4},{6,7},{7,6},{8,9},{9,8},{10,11... | collective-permute-start | bytes 491528 | tf_op jit(solution)/shard_map/ppermute | solution.py:338
  111.5 10.8 %collective-permute-start.30 = (bf16[320,256]{1,0:T(8,128)(2,1)S(1)}, bf16[320,256]{1,0:T(8,128)(2,1)S(1)}, u32[]{:S(2)}, u32[]{:S(2)}) collective-permute-start(bf16[320,256]{1,0:T(8,128)(2,1)S(1)} %collective-permute-done.26.rest_2_), channel_id=1, source_target_pairs={{0,1},{1,0},{2,3},{3,2},{4,5},{5,4},{6,7},{7,6},{8,9},{9,8},{10,11... | collective-permute-start | bytes 491528 | tf_op jit(solution)/shard_map/ppermute | solution.py:338
  118.3 7.9 %collective-permute-start.39 = (bf16[352,256]{1,0:T(8,128)(2,1)S(1)}, bf16[352,256]{1,0:T(8,128)(2,1)S(1)}, u32[]{:S(2)}, u32[]{:S(2)}) collective-permute-start(bf16[352,256]{1,0:T(8,128)(2,1)S(1)} %get-tuple-element.25.rest_0_), channel_id=1, source_target_pairs={{0,4},{4,0},{8,12},{12,8},{16,20},{20,16},{24,28},{28,24},{1,5},{5... | collective-permute-start | bytes 540680 | tf_op jit(solution)/shard_map/ppermute | solution.py:335
  118.7 10.9 %collective-permute-start.43 = (bf16[352,256]{1,0:T(8,128)(2,1)S(1)}, bf16[352,256]{1,0:T(8,128)(2,1)S(1)}, u32[]{:S(2)}, u32[]{:S(2)}) collective-permute-start(bf16[352,256]{1,0:T(8,128)(2,1)S(1)} %collective-permute-done.42.rest_4_), channel_id=1, source_target_pairs={{0,4},{4,0},{8,12},{12,8},{16,20},{20,16},{24,28},{28,24},{1,5},{5... | collective-permute-start | bytes 540680 | tf_op jit(solution)/shard_map/ppermute | solution.py:335
  120.3 13.1 %collective-permute-start.41 = (bf16[352,256]{1,0:T(8,128)(2,1)S(1)}, bf16[352,256]{1,0:T(8,128)(2,1)S(1)}, u32[]{:S(2)}, u32[]{:S(2)}) collective-permute-start(bf16[352,256]{1,0:T(8,128)(2,1)S(1)} %collective-permute-done.40.rest_2_), channel_id=1, source_target_pairs={{0,4},{4,0},{8,12},{12,8},{16,20},{20,16},{24,28},{28,24},{1,5},{5... | collective-permute-start | bytes 540680 | tf_op jit(solution)/shard_map/ppermute | solution.py:335
  120.7 14.8 %collective-permute-start.45 = (bf16[352,256]{1,0:T(8,128)(2,1)S(1)}, bf16[352,256]{1,0:T(8,128)(2,1)S(1)}, u32[]{:S(2)}, u32[]{:S(2)}) collective-permute-start(bf16[352,256]{1,0:T(8,128)(2,1)S(1)} %collective-permute-done.44.rest_6_), channel_id=1, source_target_pairs={{0,4},{4,0},{8,12},{12,8},{16,20},{20,16},{24,28},{28,24},{1,5},{5... | collective-permute-start | bytes 540680 | tf_op jit(solution)/shard_map/ppermute | solution.py:335
  122.4 1.4 collective-permute-start.31
  136.6 2.2 %collective-permute-start.46 = (bf16[4,160,512]{2,1,0:T(8,128)(2,1)S(1)}, bf16[4,160,512]{2,1,0:T(8,128)(2,1)S(1)}, u32[]{:S(2)}, u32[]{:S(2)}) collective-permute-start(bf16[4,160,512]{2,1,0:T(8,128)(2,1)S(1)} %get-tuple-element.28), channel_id=1, source_target_pairs={{0,1},{1,0},{2,3},{3,2},{4,5},{5,4},{6,7},{7,6},{8,9},{9,8},{10,11... | collective-permute-start | bytes 1966088 | tf_op jit(solution)/shard_map/ppermute | solution.py:338
  138.9 7.1 %collective-permute-start.47 = (bf16[160,512]{1,0:T(8,128)(2,1)S(1)}, bf16[160,512]{1,0:T(8,128)(2,1)S(1)}, u32[]{:S(2)}, u32[]{:S(2)}) collective-permute-start(bf16[160,512]{1,0:T(8,128)(2,1)S(1)} %get-tuple-element.30), channel_id=1, source_target_pairs={{0,8},{1,9},{2,10},{3,11},{4,12},{5,13},{6,14},{7,15},{8,0},{9,1},... | collective-permute-start | bytes 491528 | tf_op jit(solution)/shard_map/ppermute | solution.py:346
  140.4 9.5 %collective-permute-start.48 = (bf16[160,512]{1,0:T(8,128)(2,1)S(1)}, bf16[160,512]{1,0:T(8,128)(2,1)S(1)}, u32[]{:S(2)}, u32[]{:S(2)}) collective-permute-start(bf16[160,512]{1,0:T(8,128)(2,1)S(1)} %get-tuple-element.31), channel_id=1, source_target_pairs={{0,2},{1,3},{2,0},{3,1},{4,6},{5,7},{6,4},{7,5},{8,10},{9,11},{10,... | collective-permute-start | bytes 491528 | tf_op jit(solution)/shard_map/ppermute | solution.py:346
  141.6 8.3 %collective-permute-start.49 = (bf16[160,512]{1,0:T(8,128)(2,1)S(1)}, bf16[160,512]{1,0:T(8,128)(2,1)S(1)}, u32[]{:S(2)}, u32[]{:S(2)}) collective-permute-start(bf16[160,512]{1,0:T(8,128)(2,1)S(1)} %get-tuple-element.32), channel_id=1, source_target_pairs={{0,10},{1,11},{2,8},{3,9},{4,14},{5,15},{6,12},{7,13},{8,2},{9,3},... | collective-permute-start | bytes 491528 | tf_op jit(solution)/shard_map/ppermute | solution.py:346

commit v2 on v1

--- a/solution.py
+++ b/solution.py
@@ -92,10 +92,6 @@
     return lax.rem(lax.div(fs, MATE), 2)
 
 
-def turn_of(tp):
-    return (tp & 1) * 4 + ((tp >> 1) ^ (tp & 1))
-
-
 def block_of(fs, entry, count):
     back = ((fs >> 1) - entry // 2) & (count // 2 - 1)
     return back * 2 + ((fs & 1) ^ (entry & 1))
@@ -117,12 +113,18 @@
     )(*[pltpu.with_memory_space_constraint(arg, space) for arg in args])
 
 
-def split_in_kernel(x_ref, gate_ref, mine_ref, other_ref):
+def split_mix_kernel(x_ref, gate_ref, out_ref, *rest):
+    count = (len(rest) - 2) // 2
+    small, (mine_ref, other_ref), placed = rest[:count], rest[count : count + 2], rest[count + 2 :]
+    for source, target in zip(small, placed):
+        target[...] = source[...]
     side = side_of(lax.axis_index("fs"))
-    half = x_ref.shape[1] // 2
-    for out, which in ((mine_ref, side), (other_ref, 1 - side)):
-        out[:, :half] = x_ref[:, at(which, half)]
-        out[:, half:] = gate_ref[:, at(which, half)]
+    depth, width = x_ref.shape
+    half = width // 2
+    for target, which in ((mine_ref, side), (other_ref, 1 - side)):
+        target[:depth, :half] = x_ref[:, at(which, half)]
+        target[:depth, half:] = gate_ref[:, at(which, half)]
+        target[depth:] = out_ref[at(which, out_ref.shape[0] // 2), :]
 
 
 def split_ffn_kernel(gate_ref, up_ref, down_ref, *results):
@@ -171,11 +173,11 @@
     side = side_of(fs)
     length = row_refs[0].shape[0]
     normalize(tp, row_refs, gain_ref, normed_ref)
-    depth = weights[0].shape[0]
-    branches = dot(normed_ref[:, at(fs, depth)], weights[0][...])
+    depth = normed_ref.shape[1] // len(weights)
+    branches = dot(normed_ref[:, at(fs, depth)], weights[0][:depth])
     for step in range(1, len(weights)):
         lanes = at(block_of(fs, step, len(weights)), depth)
-        branches = branches + dot(normed_ref[:, lanes], weights[step][...])
+        branches = branches + dot(normed_ref[:, lanes], weights[step][:depth])
     chans = out_ref.shape[1]
     tap_count = taps_ref.shape[0]
     taps = taps_ref[:, at(side, chans)]
@@ -215,73 +217,11 @@
         out_ref[rows, :] = (state * jax.nn.gelu(branches[rows, chans:])).astype(jnp.bfloat16)
 
 
-def halves_of(ref, far):
-    length = ref.shape[0] // GROUP
-    return [ref[((slot ^ far) * length) : ((slot ^ far) + 1) * length] for slot in range(GROUP)]
-
-
-def mix_project_kernel(pieces, *refs):
-    mixed, rows, weights = refs[:pieces], refs[pieces : 2 * pieces], refs[2 * pieces : -1]
-    out_ref = refs[-1]
+def hidden_kernel(pieces, gain_ref, *rest):
+    row_refs, weights = rest[:pieces], rest[pieces:-2]
+    out_ref, normed_ref = rest[-2:]
     fs = lax.axis_index("fs")
-    tp = lax.axis_index("tp")
-    side = side_of(fs)
-    slots = pieces // 2
-    length, width = rows[0].shape
-    chans = mixed[0].shape[1]
-    columns = weights[0].shape[1]
-    block = fs ^ turn_of(tp)
-    per_tp = width // columns
-    owner = tp ^ lax.div(block, per_tp)
-    lanes = at(lax.rem(block, per_tp), columns)
-    totals = []
-    for slot in range(GROUP):
-        base = rows[slot][:, lanes]
-        for step in range(1, slots // GROUP * 2):
-            source = rows[(step & 1) * slots + step // 2 * GROUP + slot]
-            base = jnp.where(owner == step, source[:, lanes], base)
-        totals.append(base.astype(jnp.float32))
-    for far in range(GROUP):
-        which = at(side ^ far, chans)
-        for step in range(slots // GROUP * 2):
-            source = mixed[(step & 1) * slots + step // 2 * GROUP + far]
-            part = dot(source[...], weights[step][which, :])
-            for slot in range(GROUP):
-                start = (slot ^ far) * length
-                totals[slot] = totals[slot] + part[start : start + length]
-    for slot in range(GROUP):
-        out_ref[slot * length : (slot + 1) * length] = totals[slot].astype(jnp.bfloat16)
-
-
-def hidden_kernel(pieces, gain_ref, *rest):
-    row_refs, weights = rest[:pieces], rest[pieces:-4]
-    out_ref, own_ref, normed_ref, whole_ref = rest[-4:]
-    fs = lax.axis_index("fs")
-    tp = lax.axis_index("tp")
-    slots = pieces // 2
-    length, width = own_ref.shape
-    columns = row_refs[0].shape[1]
-    features = columns * pieces
-    squares = [0.0] * GROUP
-    found = []
-    for odd in range(2):
-        for pair in range(slots // GROUP):
-            for far in range(GROUP):
-                source = row_refs[odd * slots + pair * GROUP + far]
-                block = fs ^ (MATE * far) ^ turn_of(tp ^ (2 * pair + odd))
-                halves = halves_of(source, far)
-                whole_ref[:, at(block, columns)] = halves[0]
-                wide = [half.astype(jnp.float32) for half in halves]
-                for slot in range(GROUP):
-                    row_sum = jnp.sum(wide[slot] * wide[slot], axis=1, keepdims=True)
-                    squares[slot] = squares[slot] + row_sum
-                found.append((at(block, columns), wide))
-    norms = [lax.rsqrt(total / features + epsilon) for total in squares]
-    for lanes, wide in found:
-        for slot in range(GROUP):
-            scaled = wide[slot] * norms[slot] * gain_ref[:, lanes]
-            normed_ref[slot * length : (slot + 1) * length, lanes] = scaled.astype(jnp.bfloat16)
-    own_ref[...] = whole_ref[:, at(tp, width)]
+    normalize(lax.axis_index("tp"), row_refs, gain_ref, normed_ref)
     units = out_ref.shape[1]
     depth = weights[0].shape[1]
 
@@ -300,32 +240,31 @@
     out_ref[...] = (jax.nn.silu(project(0)) * project(units)).astype(jnp.bfloat16)
 
 
-def project_out_kernel(acts_ref, *rest):
+def project_out_kernel(first_step, acts_ref, *rest):
     *weights, send_ref, keep_ref, whole_ref = rest
     fs = lax.axis_index("fs")
     tp = lax.axis_index("tp")
-    slots, length, width = keep_ref.shape
+    _, length, width = keep_ref.shape
     columns = weights[0].shape[1]
     for step, weight in enumerate(weights):
-        whole_ref[:, at(block_of(fs, step, len(weights)), columns)] = weight[...]
-    for step in range(slots // GROUP * 2):
+        first = weight.shape[0] - whole_ref.shape[0]
+        whole_ref[:, at(block_of(fs, step, len(weights)), columns)] = weight[first:]
+    for step, target in ((first_step + 1, send_ref), (first_step, keep_ref)):
         part = dot(acts_ref[...], whole_ref[:, at(tp ^ step, width)]).astype(jnp.bfloat16)
-        target = send_ref if step % 2 else keep_ref
         for far in range(GROUP):
-            target[step // 2 * GROUP + far] = part[far * length : (far + 1) * length]
-
-
-def join_kernel(keep_ref, got_ref, own_ref, *sent):
-    own_ref[...] = keep_ref[0].astype(jnp.float32) + got_ref[0].astype(jnp.float32)
-    for slot, out in enumerate(sent, 1):
-        total = keep_ref[slot].astype(jnp.float32) + got_ref[slot].astype(jnp.float32)
-        out[...] = total.astype(jnp.bfloat16)
-
-
-def finish_kernel(base_ref, own_ref, *rest):
+            target[far] = part[far * length : (far + 1) * length]
+
+
+def join_kernel(keep_ref, got_ref, *outs):
+    for far, out in enumerate(outs):
+        total = keep_ref[far].astype(jnp.float32) + got_ref[far].astype(jnp.float32)
+        out[...] = total.astype(out.dtype)
+
+
+def finish_kernel(base_ref, *rest):
     *parts, out_ref = rest
-    total = own_ref[...]
-    for part in parts:
+    total = parts[0][...].astype(jnp.float32)
+    for part in parts[1:]:
         total = total + part[...].astype(jnp.float32)
     out_ref[...] = (base_ref[...].astype(jnp.float32) + total).astype(jnp.bfloat16)
 
@@ -354,17 +293,6 @@
                 piece = lax.ppermute(other if back % 2 else mine, "fs", pairs)
             got += [piece, fs_swap(piece, 1)]
         return got
-
-    def columns_of(shard):
-        blocks = []
-        for step in range(n_tp):
-            pairs = [
-                ((a ^ turn_of(b)) * n_tp + (b ^ step), a * n_tp + b)
-                for a in range(n_fs)
-                for b in range(n_tp)
-            ]
-            blocks.append(lax.ppermute(shard, ("fs", "tp"), pairs))
-        return blocks
 
     def whole_rows(own):
         near = [own, swap(own, MATE, 0)]
@@ -390,7 +318,6 @@
     ):
         length, width = tokens.shape
         features = n_tp * width
-        slots = n_tp // 2 * GROUP
         rows = GROUP * length
         chans = in_x_w.shape[1] // 2
         units = ffn_down_w.shape[0] // 2
@@ -399,30 +326,32 @@
         shape = pltpu.VMEM
         normed_scratch = pltpu.VMEM((rows, features), bf16)
 
-        def reduce_out(acts, weights, base):
-            deep = weights[0].shape[0]
-            send, keep = call(
-                project_out_kernel,
-                [shape((slots, length, width), bf16)] * 2,
-                [acts, *weights],
-                [pltpu.VMEM((deep, features), bf16)],
-            )
-            got = core_swap(send)
-            own, *sent = call(
-                join_kernel,
-                [shape((length, width), f32)] + [shape((length, width), bf16)] * (slots - 1),
-                [keep, got],
-            )
+        def reduce_out(acts, weights, base, last):
+            deep = acts.shape[1]
             arrived = []
-            for slot in range(1, slots):
-                step, far = slot // GROUP * 2, slot % GROUP
-                arrived.append(swap(sent[slot - 1], MATE * far, step))
-            return call(finish_kernel, shape((length, width), bf16), [base, own, *arrived])
-
-        in_parts = call(
-            split_in_kernel,
-            [shape((shard, 2 * chans), bf16)] * 2,
-            [in_x_w, in_gate_w],
+            for step in range(n_tp - 2, -1, -2):
+                send, keep = call(
+                    functools.partial(project_out_kernel, step),
+                    [shape((GROUP, length, width), bf16)] * 2,
+                    [acts, *weights],
+                    [pltpu.VMEM((deep, features), bf16)],
+                )
+                parts = call(
+                    join_kernel,
+                    [shape((length, width), bf16 if step + far else f32) for far in range(GROUP)],
+                    [keep, core_swap(send)],
+                )
+                for far, part in enumerate(parts):
+                    moved = swap(part, MATE * far, step) if step + far else part
+                    arrived.append(moved)
+            return call(finish_kernel, last((length, width), bf16), [base, *arrived])
+
+        small = [mix_gain[None], conv_taps, gate_x_blocks, gate_a_blocks, forget_rate[None]]
+        small += [ffn_gain[None], tokens]
+        *mix_parts, mix_gain, conv_taps, gate_x_blocks, gate_a_blocks, forget_rate, ffn_gain, base = call(
+            split_mix_kernel,
+            [shape((shard + chans, 2 * chans), bf16)] * 2 + [shape(x.shape, x.dtype) for x in small],
+            [in_x_w, in_gate_w, out_w, *small],
             space=pltpu.HBM,
         )
         shares = [shape((2 * units, shard), bf16), shape((units, shard), bf16)]
@@ -430,37 +359,33 @@
             split_ffn_kernel, shares * 2, [ffn_gate_w.T, ffn_up_w.T, ffn_down_w], space=pltpu.HBM
         )
         pieces = whole_rows(tokens)
-        in_w = gather(*in_parts)
-        out_blocks = columns_of(out_w)
+        pieces[0] = base
+        mix_w = gather(*mix_parts)
         up_w = gather(ffn_parts[0], ffn_parts[2])
         down_w = gather(ffn_parts[1], ffn_parts[3])
         mixer_out = call(
             functools.partial(mixer_kernel, len(pieces)),
             shape((rows, chans), bf16),
             [
-                mix_gain[None],
+                mix_gain,
                 conv_taps,
                 gate_x_blocks,
                 gate_a_blocks,
-                forget_rate[None],
+                forget_rate,
                 *pieces,
-                *in_w,
+                *mix_w,
             ],
             [normed_scratch, pltpu.VMEM((length + 8, chans), f32)],
         )
-        mixed = whole_rows(mixer_out)
-        after_mix = call(
-            functools.partial(mix_project_kernel, len(pieces)),
-            shape((rows, shard), bf16),
-            [*mixed, *pieces, *out_blocks],
+        after_mix = reduce_out(mixer_out, mix_w, base, shape)
+        pieces = whole_rows(after_mix)
+        hidden = call(
+            functools.partial(hidden_kernel, len(pieces)),
+            shape((rows, units), bf16),
+            [ffn_gain, *pieces, *up_w],
+            [normed_scratch],
         )
-        hidden, own = call(
-            functools.partial(hidden_kernel, len(pieces)),
-            [shape((rows, units), bf16), shape((length, width), bf16)],
-            [ffn_gain[None], *whole_rows(after_mix), *up_w],
-            [normed_scratch, pltpu.VMEM((length, features), bf16)],
-        )
-        return reduce_out(hidden, down_w, own)
+        return reduce_out(hidden, down_w, after_mix, jax.ShapeDtypeStruct)
 
     return on_device
 
@@ -482,8 +407,7 @@
         P("fs", "tp"),
         P("tp", "fs"),
     )
-    made = sorted(turn_of(tp) ^ mate for tp in range(n_tp) for mate in (0, MATE))
-    paired = made == list(range(n_fs))
+    paired = n_fs == GROUP * n_tp and n_tp % 2 == 0 and 2 * MATE < n_fs
     mapped = functools.partial(
         jax.shard_map, mesh=mesh, in_specs=placed, out_specs=P("fs", "tp"), check_vma=False
     )

time: 151 us -> 152 us (level)
  Pallas kernels: 8.22 us -> 9.76 us
    ppermute x9, waiting for transfers between devices: 40 us -> 49.7 us  [gather(): piece = lax.ppermute(other if back % 2 else mine, 'fs', pairs)]
    ppermute x4 -> x0, starting transfers between devices: 6.42 us -> none  [columns_of(): blocks.append(lax.ppermute(shard, ('fs', 'tp'), pairs))]
    ppermute x4 -> x0, waiting for transfers between devices: 5.27 us -> none  [columns_of(): blocks.append(lax.ppermute(shard, ('fs', 'tp'), pairs))]
    ppermute x12, starting transfers between devices: 17.7 us -> 22.2 us  [swap(): return lax.ppermute(values, ('fs', 'tp'), pairs)]
    ppermute x9, starting transfers between devices: 11.6 us -> 15.2 us  [gather(): piece = lax.ppermute(other if back % 2 else mine, 'fs', pairs)]
    ppermute x13 -> x12, waiting for transfers between devices: 4.77 us -> 2.64 us  [core_swap(): return lax.ppermute(values, 'tp', [(j, j ^ 1) for j in range(n_tp)])]
    ppermute x13 -> x12, starting transfers between devices: 3.46 us -> 1.36 us  [core_swap(): return lax.ppermute(values, 'tp', [(j, j ^ 1) for j in range(n_tp)])]
    ppermute x12, waiting for transfers between devices: 26 us -> 24.2 us  [fs_swap(): return lax.ppermute(values, 'fs', [(j, j ^ mask) for j in range(n_fs)])]
  transfers between devices with their start and end apart: 50 -> 45, of which waited for: 20 -> 21; matrix products, arithmetic and copies ran while one was open for 0% -> 0% of each run, Pallas kernels for 4% -> 4%
where the time goes in v2:
time: 152 us; the launch traced here: 151 us
  waiting for transfers between devices  89.5 us (59%)
  starting transfers between devices  51.9 us (34%)
  Pallas kernels  9.76 us (6%)
    ppermute x9, waiting for transfers between devices, gather(): piece = lax.ppermute(other if back % 2 else mine, 'fs', pairs)  49.7 us
    ppermute x12, waiting for transfers between devices, fs_swap(): return lax.ppermute(values, 'fs', [(j, j ^ mask) for j in range(n_fs)])  24.2 us
    ppermute x12, starting transfers between devices, swap(): return lax.ppermute(values, ('fs', 'tp'), pairs)  22.2 us
    ppermute x9, starting transfers between devices, gather(): piece = lax.ppermute(other if back % 2 else mine, 'fs', pairs)  15.2 us
    ppermute x12, starting transfers between devices, fs_swap(): return lax.ppermute(values, 'fs', [(j, j ^ mask) for j in range(n_fs)])  13.2 us
    ppermute x12, waiting for transfers between devices, swap(): return lax.ppermute(values, ('fs', 'tp'), pairs)  12.9 us
    pallas_call x14, Pallas kernels, call(): pl.pallas_call(kernel, out_shape=outs, in_specs=[spec] * len(args), out_s...  9.76 us
  transfers between devices with their start and end apart: 45, of which 21 were waited for; matrix products, arithmetic and copies ran while one was open for 0% of the time, Pallas kernels for 4%

profile of v2, /device:TPU:0, one launch (start us, length us, event | category | flops | bytes accessed | tf_op | source)
XLA Modules:
  0.0 151.4 jit_solution(14702613008417883905)
XLA Ops:
  0.0 3.1 %collective-permute-start = (bf16[160,512]{1,0:T(8,128)(2,1)}, bf16[160,512]{1,0:T(8,128)(2,1)S(1)}, u32[]{:S(2)}, u32[]{:S(2)}) collective-permute-start(bf16[160,512]{1,0:T(8,128)(2,1)} %rest_6_.1), channel_id=1, source_target_pairs={{0,8},{1,9},{2,10},{3,11},{4,12},{5,13},{6,14},{7,15},{8,0},{9,1},... | collective-permute-start | bytes 491528 | tf_op jit(solution)/shard_map/ppermute | solution.py:285
  3.1 1.5 collective-permute-start.1
  4.5 1.3 shard_map.127
  5.9 2.7 %collective-permute-start.10 = (bf16[384,256]{1,0:T(8,128)(2,1)S(1)}, bf16[384,256]{1,0:T(8,128)(2,1)S(1)}, u32[]{:S(2)}, u32[]{:S(2)}) collective-permute-start(bf16[384,256]{1,0:T(8,128)(2,1)S(1)} %get-tuple-element.40.rest_8_.rest_0_), channel_id=1, source_target_pairs={{0,16},{4,20},{8,24},{12,28},{16,0},{20,4},{24,8},{28,12},{1,17},{... | collective-permute-start | bytes 589832 | tf_op jit(solution)/shard_map/ppermute | solution.py:293
  8.5 0.2 collective-permute-start.12
  8.8 1.8 %collective-permute-start.8 = (bf16[384,256]{1,0:T(8,128)(2,1)S(1)}, bf16[384,256]{1,0:T(8,128)(2,1)S(1)}, u32[]{:S(2)}, u32[]{:S(2)}) collective-permute-start(bf16[384,256]{1,0:T(8,128)(2,1)S(1)} %get-tuple-element.41), channel_id=1, source_target_pairs={{0,8},{4,12},{8,16},{12,20},{16,24},{20,28},{24,0},{28,4},{1,9},{5... | collective-permute-start | bytes 589832 | tf_op jit(solution)/shard_map/ppermute | solution.py:293
  10.6 1.5 %collective-permute-start.7 = (bf16[384,256]{1,0:T(8,128)(2,1)S(1)}, bf16[384,256]{1,0:T(8,128)(2,1)S(1)}, u32[]{:S(2)}, u32[]{:S(2)}) collective-permute-start(bf16[384,256]{1,0:T(8,128)(2,1)S(1)} %get-tuple-element.40.rest_8_.rest_0_), channel_id=1, source_target_pairs={{0,4},{4,0},{8,12},{12,8},{16,20},{20,16},{24,28},{28,24},{1,5},{5... | collective-permute-start | bytes 589832 | tf_op jit(solution)/shard_map/ppermute | solution.py:274
  12.1 0.5 collective-permute-start.2
  12.6 6.2 %collective-permute-done.10.rest_12_.rest_4_ = bf16[384,256]{1,0:T(8,128)(2,1)S(1)} collective-permute-done((bf16[384,256]{1,0:T(8,128)(2,1)S(1)}, bf16[384,256]{1,0:T(8,128)(2,1)S(1)}, u32[]{:S(2)}, u32[]{:S(2)}) %collective-permute-start.10) | collective-permute-done | bytes 196640 | tf_op jit(solution)/shard_map/ppermute | solution.py:293
  18.9 4.3 %collective-permute-done.12.rest_14_.rest_6_ = bf16[384,256]{1,0:T(8,128)(2,1)S(1)} collective-permute-done((bf16[384,256]{1,0:T(8,128)(2,1)S(1)}, bf16[384,256]{1,0:T(8,128)(2,1)S(1)}, u32[]{:S(2)}, u32[]{:S(2)}) %collective-permute-start.12) | collective-permute-done | bytes 196640 | tf_op jit(solution)/shard_map/ppermute | solution.py:293
  23.2 1.5 %collective-permute-start.11 = (bf16[384,256]{1,0:T(8,128)(2,1)S(1)}, bf16[384,256]{1,0:T(8,128)(2,1)S(1)}, u32[]{:S(2)}, u32[]{:S(2)}) collective-permute-start(bf16[384,256]{1,0:T(8,128)(2,1)S(1)} %collective-permute-done.10.rest_12_.rest_4_), channel_id=1, source_target_pairs={{0,4},{4,0},{8,12},{12,8},{16,20},{20,16},{24,28},{28,24},{1,5},{5... | collective-permute-start | bytes 589832 | tf_op jit(solution)/shard_map/ppermute | solution.py:274
  24.7 0.5 collective-permute-start.13
  25.2 1.5 %collective-permute-start.9 = (bf16[384,256]{1,0:T(8,128)(2,1)S(1)}, bf16[384,256]{1,0:T(8,128)(2,1)S(1)}, u32[]{:S(2)}, u32[]{:S(2)}) collective-permute-start(bf16[384,256]{1,0:T(8,128)(2,1)S(1)} %collective-permute-done.8.rest_10_.rest_2_), channel_id=1, source_target_pairs={{0,4},{4,0},{8,12},{12,8},{16,20},{20,16},{24,28},{28,24},{1,5},{5... | collective-permute-start | bytes 589832 | tf_op jit(solution)/shard_map/ppermute | solution.py:274
  26.8 0.5 collective-permute-start.6
  27.3 0.9 collective-permute-done.5.rest_6_
  28.2 2.8 %collective-permute-done.11.rest_13_.rest_5_ = bf16[384,256]{1,0:T(8,128)(2,1)S(1)} collective-permute-done((bf16[384,256]{1,0:T(8,128)(2,1)S(1)}, bf16[384,256]{1,0:T(8,128)(2,1)S(1)}, u32[]{:S(2)}, u32[]{:S(2)}) %collective-permute-start.11) | collective-permute-done | bytes 196640 | tf_op jit(solution)/shard_map/ppermute | solution.py:274
  31.0 4.2 %collective-permute-done.13.rest_15_.rest_7_ = bf16[384,256]{1,0:T(8,128)(2,1)S(1)} collective-permute-done((bf16[384,256]{1,0:T(8,128)(2,1)S(1)}, bf16[384,256]{1,0:T(8,128)(2,1)S(1)}, u32[]{:S(2)}, u32[]{:S(2)}) %collective-permute-start.13) | collective-permute-done | bytes 196640 | tf_op jit(solution)/shard_map/ppermute | solution.py:274
  35.2 2.9 %collective-permute-done.9.rest_11_.rest_3_ = bf16[384,256]{1,0:T(8,128)(2,1)S(1)} collective-permute-done((bf16[384,256]{1,0:T(8,128)(2,1)S(1)}, bf16[384,256]{1,0:T(8,128)(2,1)S(1)}, u32[]{:S(2)}, u32[]{:S(2)}) %collective-permute-start.9) | collective-permute-done | bytes 196640 | tf_op jit(solution)/shard_map/ppermute | solution.py:274
  38.1 1.7 %shard_map.128.acts_ref = bf16[320,128]{1,0:T(8,128)(2,1)S(1)} custom-call(f32[1,2048]{1,0:T(1,128)S(1)} %get-tuple-element.35.gain_ref, f32[4,256]{1,0:T(4,128)S(1)} %get-tuple-element.36.taps_ref, bf16[2,128,128]{2,1,0:T(8,128)(2,1)S(1)} %get-tuple-element.37.x_maps_ref, bf16[2,128,128]{2,1,0:T(8,128)(2,1)S(1)} %get-tuple-element.38.a_maps_ref, ...), custom_call_target="tpu_custom_call" | custom-call | tf_op jit(solution)/shard_map/pallas_call | solution.py:106
  39.8 0.4 shard_map.131
  40.2 1.3 shard_map.134
  41.5 1.6 %collective-permute-start.36 = (bf16[352,256]{1,0:T(8,128)(2,1)S(1)}, bf16[352,256]{1,0:T(8,128)(2,1)S(1)}, u32[]{:S(2)}, u32[]{:S(2)}) collective-permute-start(bf16[352,256]{1,0:T(8,128)(2,1)S(1)} %get-tuple-element.53.rest_0_), channel_id=1, source_target_pairs={{0,16},{4,20},{8,24},{12,28},{16,0},{20,4},{24,8},{28,12},{1,17},{... | collective-permute-start | bytes 540680 | tf_op jit(solution)/shard_map/ppermute | solution.py:293
  43.1 1.4 collective-permute-start.29
  44.5 0.4 shard_map.129
  45.0 2.6 %collective-permute-start.27 = (bf16[704,256]{1,0:T(8,128)(2,1)S(1)}, bf16[704,256]{1,0:T(8,128)(2,1)S(1)}, u32[]{:S(2)}, u32[]{:S(2)}) collective-permute-start(bf16[704,256]{1,0:T(8,128)(2,1)S(1)} %get-tuple-element.52), channel_id=1, source_target_pairs={{0,8},{4,12},{8,16},{12,20},{16,24},{20,28},{24,0},{28,4},{1,9},{5... | collective-permute-start | bytes 1081352 | tf_op jit(solution)/shard_map/ppermute | solution.py:293
  47.6 21.6 %collective-permute-done.36.rest_4_ = bf16[352,256]{1,0:T(8,128)(2,1)S(1)} collective-permute-done((bf16[352,256]{1,0:T(8,128)(2,1)S(1)}, bf16[352,256]{1,0:T(8,128)(2,1)S(1)}, u32[]{:S(2)}, u32[]{:S(2)}) %collective-permute-start.36) | collective-permute-done | bytes 180256 | tf_op jit(solution)/shard_map/ppermute | solution.py:293
  69.2 2.0 %collective-permute-start.34 = (bf16[352,256]{1,0:T(8,128)(2,1)S(1)}, bf16[352,256]{1,0:T(8,128)(2,1)S(1)}, u32[]{:S(2)}, u32[]{:S(2)}) collective-permute-start(bf16[352,256]{1,0:T(8,128)(2,1)S(1)} %get-tuple-element.54), channel_id=1, source_target_pairs={{0,8},{4,12},{8,16},{12,20},{16,24},{20,28},{24,0},{28,4},{1,9},{5... | collective-permute-start | bytes 540680 | tf_op jit(solution)/shard_map/ppermute | solution.py:293
  71.4 0.1 shard_map.130
  71.5 11.8 %collective-permute-done.34.rest_2_ = bf16[352,256]{1,0:T(8,128)(2,1)S(1)} collective-permute-done((bf16[352,256]{1,0:T(8,128)(2,1)S(1)}, bf16[352,256]{1,0:T(8,128)(2,1)S(1)}, u32[]{:S(2)}, u32[]{:S(2)}) %collective-permute-start.34) | collective-permute-done | bytes 180256 | tf_op jit(solution)/shard_map/ppermute | solution.py:293
  83.3 1.5 %collective-permute-start.26 = (bf16[704,256]{1,0:T(8,128)(2,1)S(1)}, bf16[704,256]{1,0:T(8,128)(2,1)S(1)}, u32[]{:S(2)}, u32[]{:S(2)}) collective-permute-start(bf16[704,256]{1,0:T(8,128)(2,1)S(1)} %get-tuple-element.51.rest_8_), channel_id=1, source_target_pairs={{0,4},{4,0},{8,12},{12,8},{16,20},{20,16},{24,28},{28,24},{1,5},{5... | collective-permute-start | bytes 1081352 | tf_op jit(solution)/shard_map/ppermute | solution.py:274
  84.8 5.8 %collective-permute-start.16 = (bf16[160,512]{1,0:T(8,128)(2,1)S(1)}, bf16[160,512]{1,0:T(8,128)(2,1)S(1)}, u32[]{:S(2)}, u32[]{:S(2)}) collective-permute-start(bf16[160,512]{1,0:T(8,128)(2,1)S(1)} %get-tuple-element.45), channel_id=1, source_target_pairs={{0,10},{1,11},{2,8},{3,9},{4,14},{5,15},{6,12},{7,13},{8,2},{9,3},... | collective-permute-start | bytes 491528 | tf_op jit(solution)/shard_map/ppermute | solution.py:285
  90.7 0.5 collective-permute-start.30
  91.2 0.5 collective-permute-done.18.rest_3_
  91.7 1.5 %collective-permute-start.28 = (bf16[704,256]{1,0:T(8,128)(2,1)S(1)}, bf16[704,256]{1,0:T(8,128)(2,1)S(1)}, u32[]{:S(2)}, u32[]{:S(2)}) collective-permute-start(bf16[704,256]{1,0:T(8,128)(2,1)S(1)} %collective-permute-done.27.rest_10_), channel_id=1, source_target_pairs={{0,4},{4,0},{8,12},{12,8},{16,20},{20,16},{24,28},{28,24},{1,5},{5... | collective-permute-start | bytes 1081352 | tf_op jit(solution)/shard_map/ppermute | solution.py:274
  93.2 2.9 %collective-permute-start.38 = (bf16[352,256]{1,0:T(8,128)(2,1)S(1)}, bf16[352,256]{1,0:T(8,128)(2,1)S(1)}, u32[]{:S(2)}, u32[]{:S(2)}) collective-permute-start(bf16[352,256]{1,0:T(8,128)(2,1)S(1)} %get-tuple-element.54), channel_id=1, source_target_pairs={{0,24},{4,28},{8,0},{12,4},{16,8},{20,12},{24,16},{28,20},{1,25},{... | collective-permute-start | bytes 540680 | tf_op jit(solution)/shard_map/ppermute | solution.py:293
  96.1 0.5 collective-permute-start.32
  96.6 0.1 shard_map.133.rest_0_.base_ref
  96.7 5.7 %collective-permute-done.38.rest_6_ = bf16[352,256]{1,0:T(8,128)(2,1)S(1)} collective-permute-done((bf16[352,256]{1,0:T(8,128)(2,1)S(1)}, bf16[352,256]{1,0:T(8,128)(2,1)S(1)}, u32[]{:S(2)}, u32[]{:S(2)}) %collective-permute-start.38) | collective-permute-done | bytes 180256 | tf_op jit(solution)/shard_map/ppermute | solution.py:293
  102.3 2.5 %collective-permute-start.19 = (bf16[160,512]{1,0:T(8,128)(2,1)S(1)}, bf16[160,512]{1,0:T(8,128)(2,1)S(1)}, u32[]{:S(2)}, u32[]{:S(2)}) collective-permute-start(bf16[160,512]{1,0:T(8,128)(2,1)S(1)} %shard_map.133.rest_0_.base_ref), channel_id=1, source_target_pairs={{0,8},{1,9},{2,10},{3,11},{4,12},{5,13},{6,14},{7,15},{8,0},{9,1},... | collective-permute-start | bytes 491528 | tf_op jit(solution)/shard_map/ppermute | solution.py:285
  104.9 3.2 %collective-permute-done.19.rest_1_ = bf16[160,512]{1,0:T(8,128)(2,1)S(1)} collective-permute-done((bf16[160,512]{1,0:T(8,128)(2,1)S(1)}, bf16[160,512]{1,0:T(8,128)(2,1)S(1)}, u32[]{:S(2)}, u32[]{:S(2)}) %collective-permute-start.19) | collective-permute-done | bytes 163872 | tf_op jit(solution)/shard_map/ppermute | solution.py:285
  108.1 1.6 %collective-permute-done.28.rest_11_ = bf16[704,256]{1,0:T(8,128)(2,1)S(1)} collective-permute-done((bf16[704,256]{1,0:T(8,128)(2,1)S(1)}, bf16[704,256]{1,0:T(8,128)(2,1)S(1)}, u32[]{:S(2)}, u32[]{:S(2)}) %collective-permute-start.28) | collective-permute-done | bytes 360480 | tf_op jit(solution)/shard_map/ppermute | solution.py:274
  109.7 2.0 %collective-permute-done.20.rest_2_ = bf16[160,512]{1,0:T(8,128)(2,1)S(1)} collective-permute-done((bf16[160,512]{1,0:T(8,128)(2,1)S(1)}, bf16[160,512]{1,0:T(8,128)(2,1)S(1)}, u32[]{:S(2)}, u32[]{:S(2)}) %collective-permute-start.20) | collective-permute-done | bytes 163872 | tf_op jit(solution)/shard_map/ppermute | solution.py:285
  111.7 4.0 %collective-permute-done.32.rest_15_ = bf16[704,256]{1,0:T(8,128)(2,1)S(1)} collective-permute-done((bf16[704,256]{1,0:T(8,128)(2,1)S(1)}, bf16[704,256]{1,0:T(8,128)(2,1)S(1)}, u32[]{:S(2)}, u32[]{:S(2)}) %collective-permute-start.32) | collective-permute-done | bytes 360480 | tf_op jit(solution)/shard_map/ppermute | solution.py:274
  115.7 0.5 collective-permute-start.33
  116.2 1.5 %collective-permute-start.37 = (bf16[352,256]{1,0:T(8,128)(2,1)S(1)}, bf16[352,256]{1,0:T(8,128)(2,1)S(1)}, u32[]{:S(2)}, u32[]{:S(2)}) collective-permute-start(bf16[352,256]{1,0:T(8,128)(2,1)S(1)} %collective-permute-done.36.rest_4_), channel_id=1, source_target_pairs={{0,4},{4,0},{8,12},{12,8},{16,20},{20,16},{24,28},{28,24},{1,5},{5... | collective-permute-start | bytes 540680 | tf_op jit(solution)/shard_map/ppermute | solution.py:274
  117.7 0.5 collective-permute-start.35
  118.2 1.5 %collective-permute-start.39 = (bf16[352,256]{1,0:T(8,128)(2,1)S(1)}, bf16[352,256]{1,0:T(8,128)(2,1)S(1)}, u32[]{:S(2)}, u32[]{:S(2)}) collective-permute-start(bf16[352,256]{1,0:T(8,128)(2,1)S(1)} %collective-permute-done.38.rest_6_), channel_id=1, source_target_pairs={{0,4},{4,0},{8,12},{12,8},{16,20},{20,16},{24,28},{28,24},{1,5},{5... | collective-permute-start | bytes 540680 | tf_op jit(solution)/shard_map/ppermute | solution.py:274
  119.7 1.4 collective-permute-done.25.rest_7_
  121.1 2.1 %shard_map.135.acts_ref = bf16[320,352]{1,0:T(8,128)(2,1)S(1)} custom-call(f32[1,2048]{1,0:T(1,128)S(1)} %get-tuple-element.50.gain_ref, bf16[160,512]{1,0:T(8,128)(2,1)S(1)} %shard_map.133.rest_0_.base_ref, bf16[160,512]{1,0:T(8,128)(2,1)S(1)} %collective-permute-done.19.rest_1_, bf16[160,512]{1,0:T(8,128)(2,1)S(1)} %collective-permute-done.20.rest_2_, ...), custom_call_target="tpu_custom_call" | custom-call | tf_op jit(solution)/shard_map/pallas_call | solution.py:106
  123.3 3.7 %collective-permute-done.37.rest_5_ = bf16[352,256]{1,0:T(8,128)(2,1)S(1)} collective-permute-done((bf16[352,256]{1,0:T(8,128)(2,1)S(1)}, bf16[352,256]{1,0:T(8,128)(2,1)S(1)}, u32[]{:S(2)}, u32[]{:S(2)}) %collective-permute-start.37) | collective-permute-done | bytes 180256 | tf_op jit(solution)/shard_map/ppermute | solution.py:274
  126.9 3.2 %collective-permute-done.35.rest_3_ = bf16[352,256]{1,0:T(8,128)(2,1)S(1)} collective-permute-done((bf16[352,256]{1,0:T(8,128)(2,1)S(1)}, bf16[352,256]{1,0:T(8,128)(2,1)S(1)}, u32[]{:S(2)}, u32[]{:S(2)}) %collective-permute-start.35) | collective-permute-done | bytes 180256 | tf_op jit(solution)/shard_map/ppermute | solution.py:274
  130.1 1.9 %collective-permute-done.39.rest_7_ = bf16[352,256]{1,0:T(8,128)(2,1)S(1)} collective-permute-done((bf16[352,256]{1,0:T(8,128)(2,1)S(1)}, bf16[352,256]{1,0:T(8,128)(2,1)S(1)}, u32[]{:S(2)}, u32[]{:S(2)}) %collective-permute-start.39) | collective-permute-done | bytes 180256 | tf_op jit(solution)/shard_map/ppermute | solution.py:274
  132.0 0.7 shard_map.138
  132.8 0.7 shard_map.136
  133.5 0.6 collective-permute-start.40
  134.1 0.3 collective-permute-done.43.got_ref
  134.5 0.1 shard_map.139
  134.5 6.5 %collective-permute-start.44 = (bf16[160,512]{1,0:T(8,128)(2,1)S(1)}, bf16[160,512]{1,0:T(8,128)(2,1)S(1)}, u32[]{:S(2)}, u32[]{:S(2)}) collective-permute-start(bf16[160,512]{1,0:T(8,128)(2,1)S(1)} %get-tuple-element.62), channel_id=1, source_target_pairs={{0,8},{1,9},{2,10},{3,11},{4,12},{5,13},{6,14},{7,15},{8,0},{9,1},... | collective-permute-start | bytes 491528 | tf_op jit(solution)/shard_map/ppermute | solution.py:285
  141.0 0.1 shard_map.137
  141.1 0.2 collective-permute-start.41
  141.3 2.1 %collective-permute-start.42 = (bf16[160,512]{1,0:T(8,128)(2,1)S(1)}, bf16[160,512]{1,0:T(8,128)(2,1)S(1)}, u32[]{:S(2)}, u32[]{:S(2)}) collective-permute-start(bf16[160,512]{1,0:T(8,128)(2,1)S(1)} %get-tuple-element.58), channel_id=1, source_target_pairs={{0,10},{1,11},{2,8},{3,9},{4,14},{5,15},{6,12},{7,13},{8,2},{9,3},... | collective-permute-start | bytes 491528 | tf_op jit(solution)/shard_map/ppermute | solution.py:285
  143.4 2.7 %collective-permute-done.44.rest_3_ = bf16[160,512]{1,0:T(8,128)(2,1)S(1)} collective-permute-done((bf16[160,512]{1,0:T(8,128)(2,1)S(1)}, bf16[160,512]{1,0:T(8,128)(2,1)S(1)}, u32[]{:S(2)}, u32[]{:S(2)}) %collective-permute-start.44) | collective-permute-done | bytes 163872 | tf_op jit(solution)/shard_map/ppermute | solution.py:285
  146.0 4.6 %collective-permute-done.41.rest_0_ = bf16[160,512]{1,0:T(8,128)(2,1)S(1)} collective-permute-done((bf16[160,512]{1,0:T(8,128)(2,1)S(1)}, bf16[160,512]{1,0:T(8,128)(2,1)S(1)}, u32[]{:S(2)}, u32[]{:S(2)}) %collective-permute-start.41) | collective-permute-done | bytes 163872 | tf_op jit(solution)/shard_map/ppermute | solution.py:285
  150.6 0.8 shard_map.140
  (42 shorter events, 0.5 us)
Async XLA Ops:
  0.0 8.8 %collective-permute-start = (bf16[160,512]{1,0:T(8,128)(2,1)}, bf16[160,512]{1,0:T(8,128)(2,1)S(1)}, u32[]{:S(2)}, u32[]{:S(2)}) collective-permute-start(bf16[160,512]{1,0:T(8,128)(2,1)} %rest_6_.1), channel_id=1, source_target_pairs={{0,8},{1,9},{2,10},{3,11},{4,12},{5,13},{6,14},{7,15},{8,0},{9,1},... | collective-permute-start | bytes 491528 | tf_op jit(solution)/shard_map/ppermute | solution.py:285
  3.1 7.5 %collective-permute-start.1 = (bf16[160,512]{1,0:T(8,128)(2,1)}, bf16[160,512]{1,0:T(8,128)(2,1)S(1)}, u32[]{:S(2)}, u32[]{:S(2)}) collective-permute-start(bf16[160,512]{1,0:T(8,128)(2,1)} %rest_6_.1), channel_id=1, source_target_pairs={{0,2},{1,3},{2,0},{3,1},{4,6},{5,7},{6,4},{7,5},{8,10},{9,11},{10,... | collective-permute-start | bytes 491528 | tf_op jit(solution)/shard_map/ppermute | solution.py:285
  4.5 4.0 %copy-start = (bf16[160,512]{1,0:T(8,128)(2,1)S(1)}, bf16[160,512]{1,0:T(8,128)(2,1)}, u32[]{:S(2)}) copy-start(bf16[160,512]{1,0:T(8,128)(2,1)} %rest_6_.1) | copy-start | bytes 491524
  5.9 13.0 %collective-permute-start.10 = (bf16[384,256]{1,0:T(8,128)(2,1)S(1)}, bf16[384,256]{1,0:T(8,128)(2,1)S(1)}, u32[]{:S(2)}, u32[]{:S(2)}) collective-permute-start(bf16[384,256]{1,0:T(8,128)(2,1)S(1)} %get-tuple-element.40.rest_8_.rest_0_), channel_id=1, source_target_pairs={{0,16},{4,20},{8,24},{12,28},{16,0},{20,4},{24,8},{28,12},{1,17},{... | collective-permute-start | bytes 589832 | tf_op jit(solution)/shard_map/ppermute | solution.py:293
  8.5 3.6 %collective-permute-start.3 = (bf16[160,512]{1,0:T(8,128)(2,1)S(1)}, bf16[160,512]{1,0:T(8,128)(2,1)S(1)}, u32[]{:S(2)}, u32[]{:S(2)}) collective-permute-start(bf16[160,512]{1,0:T(8,128)(2,1)S(1)} %copy-done), channel_id=1, source_target_pairs={{0,1},{1,0},{2,3},{3,2},{4,5},{5,4},{6,7},{7,6},{8,9},{9,8},{10,11... | collective-permute-start | bytes 491528 | tf_op jit(solution)/shard_map/ppermute | solution.py:277
  8.5 14.7 %collective-permute-start.12 = (bf16[384,256]{1,0:T(8,128)(2,1)S(1)}, bf16[384,256]{1,0:T(8,128)(2,1)S(1)}, u32[]{:S(2)}, u32[]{:S(2)}) collective-permute-start(bf16[384,256]{1,0:T(8,128)(2,1)S(1)} %get-tuple-element.41), channel_id=1, source_target_pairs={{0,24},{4,28},{8,0},{12,4},{16,8},{20,12},{24,16},{28,20},{1,25},{... | collective-permute-start | bytes 589832 | tf_op jit(solution)/shard_map/ppermute | solution.py:293
  8.8 16.0 %collective-permute-start.8 = (bf16[384,256]{1,0:T(8,128)(2,1)S(1)}, bf16[384,256]{1,0:T(8,128)(2,1)S(1)}, u32[]{:S(2)}, u32[]{:S(2)}) collective-permute-start(bf16[384,256]{1,0:T(8,128)(2,1)S(1)} %get-tuple-element.41), channel_id=1, source_target_pairs={{0,8},{4,12},{8,16},{12,20},{16,24},{20,28},{24,0},{28,4},{1,9},{5... | collective-permute-start | bytes 589832 | tf_op jit(solution)/shard_map/ppermute | solution.py:293
  10.6 14.7 %collective-permute-start.7 = (bf16[384,256]{1,0:T(8,128)(2,1)S(1)}, bf16[384,256]{1,0:T(8,128)(2,1)S(1)}, u32[]{:S(2)}, u32[]{:S(2)}) collective-permute-start(bf16[384,256]{1,0:T(8,128)(2,1)S(1)} %get-tuple-element.40.rest_8_.rest_0_), channel_id=1, source_target_pairs={{0,4},{4,0},{8,12},{12,8},{16,20},{20,16},{24,28},{28,24},{1,5},{5... | collective-permute-start | bytes 589832 | tf_op jit(solution)/shard_map/ppermute | solution.py:274
  12.1 14.7 %collective-permute-start.2 = (bf16[160,512]{1,0:T(8,128)(2,1)S(1)}, bf16[160,512]{1,0:T(8,128)(2,1)S(1)}, u32[]{:S(2)}, u32[]{:S(2)}) collective-permute-start(bf16[160,512]{1,0:T(8,128)(2,1)S(1)} %collective-permute-done.rest_1_), channel_id=1, source_target_pairs={{0,2},{1,3},{2,0},{3,1},{4,6},{5,7},{6,4},{7,5},{8,10},{9,11},{10,... | collective-permute-start | bytes 491528 | tf_op jit(solution)/shard_map/ppermute | solution.py:285
  18.9 7.9 %collective-permute-start.4 = (bf16[160,512]{1,0:T(8,128)(2,1)S(1)}, bf16[160,512]{1,0:T(8,128)(2,1)S(1)}, u32[]{:S(2)}, u32[]{:S(2)}) collective-permute-start(bf16[160,512]{1,0:T(8,128)(2,1)S(1)} %collective-permute-done.rest_1_), channel_id=1, source_target_pairs={{0,1},{1,0},{2,3},{3,2},{4,5},{5,4},{6,7},{7,6},{8,9},{9,8},{10,11... | collective-permute-start | bytes 491528 | tf_op jit(solution)/shard_map/ppermute | solution.py:277
  23.2 7.8 %collective-permute-start.11 = (bf16[384,256]{1,0:T(8,128)(2,1)S(1)}, bf16[384,256]{1,0:T(8,128)(2,1)S(1)}, u32[]{:S(2)}, u32[]{:S(2)}) collective-permute-start(bf16[384,256]{1,0:T(8,128)(2,1)S(1)} %collective-permute-done.10.rest_12_.rest_4_), channel_id=1, source_target_pairs={{0,4},{4,0},{8,12},{12,8},{16,20},{20,16},{24,28},{28,24},{1,5},{5... | collective-permute-start | bytes 589832 | tf_op jit(solution)/shard_map/ppermute | solution.py:274
  24.7 10.5 %collective-permute-start.13 = (bf16[384,256]{1,0:T(8,128)(2,1)S(1)}, bf16[384,256]{1,0:T(8,128)(2,1)S(1)}, u32[]{:S(2)}, u32[]{:S(2)}) collective-permute-start(bf16[384,256]{1,0:T(8,128)(2,1)S(1)} %collective-permute-done.12.rest_14_.rest_6_), channel_id=1, source_target_pairs={{0,4},{4,0},{8,12},{12,8},{16,20},{20,16},{24,28},{28,24},{1,5},{5... | collective-permute-start | bytes 589832 | tf_op jit(solution)/shard_map/ppermute | solution.py:274
  25.2 12.8 %collective-permute-start.9 = (bf16[384,256]{1,0:T(8,128)(2,1)S(1)}, bf16[384,256]{1,0:T(8,128)(2,1)S(1)}, u32[]{:S(2)}, u32[]{:S(2)}) collective-permute-start(bf16[384,256]{1,0:T(8,128)(2,1)S(1)} %collective-permute-done.8.rest_10_.rest_2_), channel_id=1, source_target_pairs={{0,4},{4,0},{8,12},{12,8},{16,20},{20,16},{24,28},{28,24},{1,5},{5... | collective-permute-start | bytes 589832 | tf_op jit(solution)/shard_map/ppermute | solution.py:274
  26.8 1.4 collective-permute-start.5
  26.8 11.3 %collective-permute-start.6 = (bf16[160,512]{1,0:T(8,128)(2,1)S(1)}, bf16[160,512]{1,0:T(8,128)(2,1)S(1)}, u32[]{:S(2)}, u32[]{:S(2)}) collective-permute-start(bf16[160,512]{1,0:T(8,128)(2,1)S(1)} %collective-permute-done.2.rest_3_), channel_id=1, source_target_pairs={{0,1},{1,0},{2,3},{3,2},{4,5},{5,4},{6,7},{7,6},{8,9},{9,8},{10,11... | collective-permute-start | bytes 491528 | tf_op jit(solution)/shard_map/ppermute | solution.py:277
  40.2 29.1 %collective-permute-start.17 = (bf16[2,160,512]{2,1,0:T(8,128)(2,1)S(1)}, bf16[2,160,512]{2,1,0:T(8,128)(2,1)S(1)}, u32[]{:S(2)}, u32[]{:S(2)}) collective-permute-start(bf16[2,160,512]{2,1,0:T(8,128)(2,1)S(1)} %get-tuple-element.47), channel_id=1, source_target_pairs={{0,1},{1,0},{2,3},{3,2},{4,5},{5,4},{6,7},{7,6},{8,9},{9,8},{10,11... | collective-permute-start | bytes 983048 | tf_op jit(solution)/shard_map/ppermute | solution.py:277
  41.5 27.7 %collective-permute-start.36 = (bf16[352,256]{1,0:T(8,128)(2,1)S(1)}, bf16[352,256]{1,0:T(8,128)(2,1)S(1)}, u32[]{:S(2)}, u32[]{:S(2)}) collective-permute-start(bf16[352,256]{1,0:T(8,128)(2,1)S(1)} %get-tuple-element.53.rest_0_), channel_id=1, source_target_pairs={{0,16},{4,20},{8,24},{12,28},{16,0},{20,4},{24,8},{28,12},{1,17},{... | collective-permute-start | bytes 540680 | tf_op jit(solution)/shard_map/ppermute | solution.py:293
  43.1 41.7 %collective-permute-start.29 = (bf16[704,256]{1,0:T(8,128)(2,1)S(1)}, bf16[704,256]{1,0:T(8,128)(2,1)S(1)}, u32[]{:S(2)}, u32[]{:S(2)}) collective-permute-start(bf16[704,256]{1,0:T(8,128)(2,1)S(1)} %get-tuple-element.51.rest_8_), channel_id=1, source_target_pairs={{0,16},{4,20},{8,24},{12,28},{16,0},{20,4},{24,8},{28,12},{1,17},{... | collective-permute-start | bytes 1081352 | tf_op jit(solution)/shard_map/ppermute | solution.py:293
  44.9 26.4 %collective-permute-start.14 = (bf16[2,160,512]{2,1,0:T(8,128)(2,1)S(1)}, bf16[2,160,512]{2,1,0:T(8,128)(2,1)S(1)}, u32[]{:S(2)}, u32[]{:S(2)}) collective-permute-start(bf16[2,160,512]{2,1,0:T(8,128)(2,1)S(1)} %get-tuple-element.43), channel_id=1, source_target_pairs={{0,1},{1,0},{2,3},{3,2},{4,5},{5,4},{6,7},{7,6},{8,9},{9,8},{10,11... | collective-permute-start | bytes 983048 | tf_op jit(solution)/shard_map/ppermute | solution.py:277
  45.0 39.9 %collective-permute-start.27 = (bf16[704,256]{1,0:T(8,128)(2,1)S(1)}, bf16[704,256]{1,0:T(8,128)(2,1)S(1)}, u32[]{:S(2)}, u32[]{:S(2)}) collective-permute-start(bf16[704,256]{1,0:T(8,128)(2,1)S(1)} %get-tuple-element.52), channel_id=1, source_target_pairs={{0,8},{4,12},{8,16},{12,20},{16,24},{20,28},{24,0},{28,4},{1,9},{5... | collective-permute-start | bytes 1081352 | tf_op jit(solution)/shard_map/ppermute | solution.py:293
  69.2 21.5 %collective-permute-start.31 = (bf16[704,256]{1,0:T(8,128)(2,1)S(1)}, bf16[704,256]{1,0:T(8,128)(2,1)S(1)}, u32[]{:S(2)}, u32[]{:S(2)}) collective-permute-start(bf16[704,256]{1,0:T(8,128)(2,1)S(1)} %get-tuple-element.52), channel_id=1, source_target_pairs={{0,24},{4,28},{8,0},{12,4},{16,8},{20,12},{24,16},{28,20},{1,25},{... | collective-permute-start | bytes 1081352 | tf_op jit(solution)/shard_map/ppermute | solution.py:293
  69.2 14.1 %collective-permute-start.34 = (bf16[352,256]{1,0:T(8,128)(2,1)S(1)}, bf16[352,256]{1,0:T(8,128)(2,1)S(1)}, u32[]{:S(2)}, u32[]{:S(2)}) collective-permute-start(bf16[352,256]{1,0:T(8,128)(2,1)S(1)} %get-tuple-element.54), channel_id=1, source_target_pairs={{0,8},{4,12},{8,16},{12,20},{16,24},{20,28},{24,0},{28,4},{1,9},{5... | collective-permute-start | bytes 540680 | tf_op jit(solution)/shard_map/ppermute | solution.py:293
  71.3 20.3 %collective-permute-start.18 = (bf16[160,512]{1,0:T(8,128)(2,1)S(1)}, bf16[160,512]{1,0:T(8,128)(2,1)S(1)}, u32[]{:S(2)}, u32[]{:S(2)}) collective-permute-start(bf16[160,512]{1,0:T(8,128)(2,1)S(1)} %get-tuple-element.49), channel_id=1, source_target_pairs={{0,8},{1,9},{2,10},{3,11},{4,12},{5,13},{6,14},{7,15},{8,0},{9,1},... | collective-permute-start | bytes 491528 | tf_op jit(solution)/shard_map/ppermute | solution.py:285
  83.3 21.5 %collective-permute-start.26 = (bf16[704,256]{1,0:T(8,128)(2,1)S(1)}, bf16[704,256]{1,0:T(8,128)(2,1)S(1)}, u32[]{:S(2)}, u32[]{:S(2)}) collective-permute-start(bf16[704,256]{1,0:T(8,128)(2,1)S(1)} %get-tuple-element.51.rest_8_), channel_id=1, source_target_pairs={{0,4},{4,0},{8,12},{12,8},{16,20},{20,16},{24,28},{28,24},{1,5},{5... | collective-permute-start | bytes 1081352 | tf_op jit(solution)/shard_map/ppermute | solution.py:274
  84.8 8.4 %collective-permute-start.15 = (bf16[160,512]{1,0:T(8,128)(2,1)S(1)}, bf16[160,512]{1,0:T(8,128)(2,1)S(1)}, u32[]{:S(2)}, u32[]{:S(2)}) collective-permute-start(bf16[160,512]{1,0:T(8,128)(2,1)S(1)} %get-tuple-element.44), channel_id=1, source_target_pairs={{0,2},{1,3},{2,0},{3,1},{4,6},{5,7},{6,4},{7,5},{8,10},{9,11},{10,... | collective-permute-start | bytes 491528 | tf_op jit(solution)/shard_map/ppermute | solution.py:285
  84.8 11.2 %collective-permute-start.16 = (bf16[160,512]{1,0:T(8,128)(2,1)S(1)}, bf16[160,512]{1,0:T(8,128)(2,1)S(1)}, u32[]{:S(2)}, u32[]{:S(2)}) collective-permute-start(bf16[160,512]{1,0:T(8,128)(2,1)S(1)} %get-tuple-element.45), channel_id=1, source_target_pairs={{0,10},{1,11},{2,8},{3,9},{4,14},{5,15},{6,12},{7,13},{8,2},{9,3},... | collective-permute-start | bytes 491528 | tf_op jit(solution)/shard_map/ppermute | solution.py:285
  90.7 14.2 %collective-permute-start.30 = (bf16[704,256]{1,0:T(8,128)(2,1)S(1)}, bf16[704,256]{1,0:T(8,128)(2,1)S(1)}, u32[]{:S(2)}, u32[]{:S(2)}) collective-permute-start(bf16[704,256]{1,0:T(8,128)(2,1)S(1)} %collective-permute-done.29.rest_12_), channel_id=1, source_target_pairs={{0,4},{4,0},{8,12},{12,8},{16,20},{20,16},{24,28},{28,24},{1,5},{5... | collective-permute-start | bytes 1081352 | tf_op jit(solution)/shard_map/ppermute | solution.py:274
  91.7 18.0 %collective-permute-start.28 = (bf16[704,256]{1,0:T(8,128)(2,1)S(1)}, bf16[704,256]{1,0:T(8,128)(2,1)S(1)}, u32[]{:S(2)}, u32[]{:S(2)}) collective-permute-start(bf16[704,256]{1,0:T(8,128)(2,1)S(1)} %collective-permute-done.27.rest_10_), channel_id=1, source_target_pairs={{0,4},{4,0},{8,12},{12,8},{16,20},{20,16},{24,28},{28,24},{1,5},{5... | collective-permute-start | bytes 1081352 | tf_op jit(solution)/shard_map/ppermute | solution.py:274
  93.2 9.2 %collective-permute-start.38 = (bf16[352,256]{1,0:T(8,128)(2,1)S(1)}, bf16[352,256]{1,0:T(8,128)(2,1)S(1)}, u32[]{:S(2)}, u32[]{:S(2)}) collective-permute-start(bf16[352,256]{1,0:T(8,128)(2,1)S(1)} %get-tuple-element.54), channel_id=1, source_target_pairs={{0,24},{4,28},{8,0},{12,4},{16,8},{20,12},{24,16},{28,20},{1,25},{... | collective-permute-start | bytes 540680 | tf_op jit(solution)/shard_map/ppermute | solution.py:293
  96.1 19.6 %collective-permute-start.32 = (bf16[704,256]{1,0:T(8,128)(2,1)S(1)}, bf16[704,256]{1,0:T(8,128)(2,1)S(1)}, u32[]{:S(2)}, u32[]{:S(2)}) collective-permute-start(bf16[704,256]{1,0:T(8,128)(2,1)S(1)} %collective-permute-done.31.rest_14_), channel_id=1, source_target_pairs={{0,4},{4,0},{8,12},{12,8},{16,20},{20,16},{24,28},{28,24},{1,5},{5... | collective-permute-start | bytes 1081352 | tf_op jit(solution)/shard_map/ppermute | solution.py:274
  102.3 5.8 %collective-permute-start.19 = (bf16[160,512]{1,0:T(8,128)(2,1)S(1)}, bf16[160,512]{1,0:T(8,128)(2,1)S(1)}, u32[]{:S(2)}, u32[]{:S(2)}) collective-permute-start(bf16[160,512]{1,0:T(8,128)(2,1)S(1)} %shard_map.133.rest_0_.base_ref), channel_id=1, source_target_pairs={{0,8},{1,9},{2,10},{3,11},{4,12},{5,13},{6,14},{7,15},{8,0},{9,1},... | collective-permute-start | bytes 491528 | tf_op jit(solution)/shard_map/ppermute | solution.py:285
  104.8 6.9 %collective-permute-start.20 = (bf16[160,512]{1,0:T(8,128)(2,1)S(1)}, bf16[160,512]{1,0:T(8,128)(2,1)S(1)}, u32[]{:S(2)}, u32[]{:S(2)}) collective-permute-start(bf16[160,512]{1,0:T(8,128)(2,1)S(1)} %shard_map.133.rest_0_.base_ref), channel_id=1, source_target_pairs={{0,2},{1,3},{2,0},{3,1},{4,6},{5,7},{6,4},{7,5},{8,10},{9,11},{10,... | collective-permute-start | bytes 491528 | tf_op jit(solution)/shard_map/ppermute | solution.py:285
  104.8 11.3 %collective-permute-start.22 = (bf16[160,512]{1,0:T(8,128)(2,1)S(1)}, bf16[160,512]{1,0:T(8,128)(2,1)S(1)}, u32[]{:S(2)}, u32[]{:S(2)}) collective-permute-start(bf16[160,512]{1,0:T(8,128)(2,1)S(1)} %shard_map.133.rest_0_.base_ref), channel_id=1, source_target_pairs={{0,1},{1,0},{2,3},{3,2},{4,5},{5,4},{6,7},{7,6},{8,9},{9,8},{10,11... | collective-permute-start | bytes 491528 | tf_op jit(solution)/shard_map/ppermute | solution.py:277
  108.1 9.6 %collective-permute-start.21 = (bf16[160,512]{1,0:T(8,128)(2,1)S(1)}, bf16[160,512]{1,0:T(8,128)(2,1)S(1)}, u32[]{:S(2)}, u32[]{:S(2)}) collective-permute-start(bf16[160,512]{1,0:T(8,128)(2,1)S(1)} %collective-permute-done.19.rest_1_), channel_id=1, source_target_pairs={{0,2},{1,3},{2,0},{3,1},{4,6},{5,7},{6,4},{7,5},{8,10},{9,11},{10,... | collective-permute-start | bytes 491528 | tf_op jit(solution)/shard_map/ppermute | solution.py:285
  109.7 8.5 %collective-permute-start.23 = (bf16[160,512]{1,0:T(8,128)(2,1)S(1)}, bf16[160,512]{1,0:T(8,128)(2,1)S(1)}, u32[]{:S(2)}, u32[]{:S(2)}) collective-permute-start(bf16[160,512]{1,0:T(8,128)(2,1)S(1)} %collective-permute-done.19.rest_1_), channel_id=1, source_target_pairs={{0,1},{1,0},{2,3},{3,2},{4,5},{5,4},{6,7},{7,6},{8,9},{9,8},{10,11... | collective-permute-start | bytes 491528 | tf_op jit(solution)/shard_map/ppermute | solution.py:277
  111.7 8.0 %collective-permute-start.24 = (bf16[160,512]{1,0:T(8,128)(2,1)S(1)}, bf16[160,512]{1,0:T(8,128)(2,1)S(1)}, u32[]{:S(2)}, u32[]{:S(2)}) collective-permute-start(bf16[160,512]{1,0:T(8,128)(2,1)S(1)} %collective-permute-done.20.rest_2_), channel_id=1, source_target_pairs={{0,1},{1,0},{2,3},{3,2},{4,5},{5,4},{6,7},{7,6},{8,9},{9,8},{10,11... | collective-permute-start | bytes 491528 | tf_op jit(solution)/shard_map/ppermute | solution.py:277
  115.7 7.6 %collective-permute-start.33 = (bf16[352,256]{1,0:T(8,128)(2,1)S(1)}, bf16[352,256]{1,0:T(8,128)(2,1)S(1)}, u32[]{:S(2)}, u32[]{:S(2)}) collective-permute-start(bf16[352,256]{1,0:T(8,128)(2,1)S(1)} %get-tuple-element.53.rest_0_), channel_id=1, source_target_pairs={{0,4},{4,0},{8,12},{12,8},{16,20},{20,16},{24,28},{28,24},{1,5},{5... | collective-permute-start | bytes 540680 | tf_op jit(solution)/shard_map/ppermute | solution.py:274
  116.2 10.8 %collective-permute-start.37 = (bf16[352,256]{1,0:T(8,128)(2,1)S(1)}, bf16[352,256]{1,0:T(8,128)(2,1)S(1)}, u32[]{:S(2)}, u32[]{:S(2)}) collective-permute-start(bf16[352,256]{1,0:T(8,128)(2,1)S(1)} %collective-permute-done.36.rest_4_), channel_id=1, source_target_pairs={{0,4},{4,0},{8,12},{12,8},{16,20},{20,16},{24,28},{28,24},{1,5},{5... | collective-permute-start | bytes 540680 | tf_op jit(solution)/shard_map/ppermute | solution.py:274
  117.7 12.4 %collective-permute-start.35 = (bf16[352,256]{1,0:T(8,128)(2,1)S(1)}, bf16[352,256]{1,0:T(8,128)(2,1)S(1)}, u32[]{:S(2)}, u32[]{:S(2)}) collective-permute-start(bf16[352,256]{1,0:T(8,128)(2,1)S(1)} %collective-permute-done.34.rest_2_), channel_id=1, source_target_pairs={{0,4},{4,0},{8,12},{12,8},{16,20},{20,16},{24,28},{28,24},{1,5},{5... | collective-permute-start | bytes 540680 | tf_op jit(solution)/shard_map/ppermute | solution.py:274
  118.2 13.8 %collective-permute-start.39 = (bf16[352,256]{1,0:T(8,128)(2,1)S(1)}, bf16[352,256]{1,0:T(8,128)(2,1)S(1)}, u32[]{:S(2)}, u32[]{:S(2)}) collective-permute-start(bf16[352,256]{1,0:T(8,128)(2,1)S(1)} %collective-permute-done.38.rest_6_), channel_id=1, source_target_pairs={{0,4},{4,0},{8,12},{12,8},{16,20},{20,16},{24,28},{28,24},{1,5},{5... | collective-permute-start | bytes 540680 | tf_op jit(solution)/shard_map/ppermute | solution.py:274
  119.7 1.4 collective-permute-start.25
  132.8 1.7 %collective-permute-start.43 = (bf16[2,160,512]{2,1,0:T(8,128)(2,1)S(1)}, bf16[2,160,512]{2,1,0:T(8,128)(2,1)S(1)}, u32[]{:S(2)}, u32[]{:S(2)}) collective-permute-start(bf16[2,160,512]{2,1,0:T(8,128)(2,1)S(1)} %get-tuple-element.60), channel_id=1, source_target_pairs={{0,1},{1,0},{2,3},{3,2},{4,5},{5,4},{6,7},{7,6},{8,9},{9,8},{10,11... | collective-permute-start | bytes 983048 | tf_op jit(solution)/shard_map/ppermute | solution.py:277
  133.5 7.4 %collective-permute-start.40 = (bf16[2,160,512]{2,1,0:T(8,128)(2,1)S(1)}, bf16[2,160,512]{2,1,0:T(8,128)(2,1)S(1)}, u32[]{:S(2)}, u32[]{:S(2)}) collective-permute-start(bf16[2,160,512]{2,1,0:T(8,128)(2,1)S(1)} %get-tuple-element.56), channel_id=1, source_target_pairs={{0,1},{1,0},{2,3},{3,2},{4,5},{5,4},{6,7},{7,6},{8,9},{9,8},{10,11... | collective-permute-start | bytes 983048 | tf_op jit(solution)/shard_map/ppermute | solution.py:277
  134.5 11.5 %collective-permute-start.44 = (bf16[160,512]{1,0:T(8,128)(2,1)S(1)}, bf16[160,512]{1,0:T(8,128)(2,1)S(1)}, u32[]{:S(2)}, u32[]{:S(2)}) collective-permute-start(bf16[160,512]{1,0:T(8,128)(2,1)S(1)} %get-tuple-element.62), channel_id=1, source_target_pairs={{0,8},{1,9},{2,10},{3,11},{4,12},{5,13},{6,14},{7,15},{8,0},{9,1},... | collective-permute-start | bytes 491528 | tf_op jit(solution)/shard_map/ppermute | solution.py:285
  141.1 9.5 %collective-permute-start.41 = (bf16[160,512]{1,0:T(8,128)(2,1)S(1)}, bf16[160,512]{1,0:T(8,128)(2,1)S(1)}, u32[]{:S(2)}, u32[]{:S(2)}) collective-permute-start(bf16[160,512]{1,0:T(8,128)(2,1)S(1)} %get-tuple-element.57), channel_id=1, source_target_pairs={{0,2},{1,3},{2,0},{3,1},{4,6},{5,7},{6,4},{7,5},{8,10},{9,11},{10,... | collective-permute-start | bytes 491528 | tf_op jit(solution)/shard_map/ppermute | solution.py:285
  141.3 9.3 %collective-permute-start.42 = (bf16[160,512]{1,0:T(8,128)(2,1)S(1)}, bf16[160,512]{1,0:T(8,128)(2,1)S(1)}, u32[]{:S(2)}, u32[]{:S(2)}) collective-permute-start(bf16[160,512]{1,0:T(8,128)(2,1)S(1)} %get-tuple-element.58), channel_id=1, source_target_pairs={{0,10},{1,11},{2,8},{3,9},{4,14},{5,15},{6,12},{7,13},{8,2},{9,3},... | collective-permute-start | bytes 491528 | tf_op jit(solution)/shard_map/ppermute | solution.py:285

commit v3 on v2

--- a/solution.py
+++ b/solution.py
@@ -217,27 +217,35 @@
         out_ref[rows, :] = (state * jax.nn.gelu(branches[rows, chans:])).astype(jnp.bfloat16)
 
 
-def hidden_kernel(pieces, gain_ref, *rest):
-    row_refs, weights = rest[:pieces], rest[pieces:-2]
-    out_ref, normed_ref = rest[-2:]
-    fs = lax.axis_index("fs")
+def project_rows(normed_ref, weights, entries, count, first, units):
+    total = None
+    for entry, weight in zip(entries, weights):
+        depth = weight.shape[1]
+        part = lax.dot_general(
+            normed_ref[:, at(block_of(lax.axis_index("fs"), entry, count), depth)],
+            weight[first : first + units, :],
+            (((1,), (1,)), ((), ())),
+            preferred_element_type=jnp.float32,
+        )
+        total = part if total is None else total + part
+    return total
+
+
+def early_kernel(pieces, entries, count, gain_ref, *rest):
+    row_refs, weights = rest[:pieces], rest[pieces:-3]
+    gate_ref, up_ref, normed_ref = rest[-3:]
     normalize(lax.axis_index("tp"), row_refs, gain_ref, normed_ref)
+    units = gate_ref.shape[1]
+    gate_ref[...] = project_rows(normed_ref, weights, entries, count, 0, units)
+    up_ref[...] = project_rows(normed_ref, weights, entries, count, units, units)
+
+
+def hidden_kernel(entries, count, gate_ref, up_ref, normed_ref, *rest):
+    *weights, out_ref = rest
     units = out_ref.shape[1]
-    depth = weights[0].shape[1]
-
-    def project(first):
-        total = None
-        for step, weight in enumerate(weights):
-            part = lax.dot_general(
-                normed_ref[:, at(block_of(fs, step, len(weights)), depth)],
-                weight[first : first + units, :],
-                (((1,), (1,)), ((), ())),
-                preferred_element_type=jnp.float32,
-            )
-            total = part if total is None else total + part
-        return total
-
-    out_ref[...] = (jax.nn.silu(project(0)) * project(units)).astype(jnp.bfloat16)
+    gate = gate_ref[...] + project_rows(normed_ref, weights, entries, count, 0, units)
+    up = up_ref[...] + project_rows(normed_ref, weights, entries, count, units, units)
+    out_ref[...] = (jax.nn.silu(gate) * up).astype(jnp.bfloat16)
 
 
 def project_out_kernel(first_step, acts_ref, *rest):
@@ -261,6 +269,21 @@
         out[...] = total.astype(out.dtype)
 
 
+def gather_sum_kernel(*refs):
+    *parts, out_ref = refs
+    for far in range(GROUP):
+        total = parts[far][...].astype(jnp.float32)
+        for part in parts[GROUP + far :: GROUP]:
+            total = total + part[...].astype(jnp.float32)
+        out_ref[far] = total.astype(jnp.bfloat16)
+
+
+def add_pair_kernel(own_ref, mate_ref, made_ref, got_ref, *outs):
+    for far, (base_ref, out) in enumerate(zip((own_ref, mate_ref), outs)):
+        total = made_ref[far].astype(jnp.float32) + got_ref[far ^ 1].astype(jnp.float32)
+        out[...] = (base_ref[...].astype(jnp.float32) + total).astype(jnp.bfloat16)
+
+
 def finish_kernel(base_ref, *rest):
     *parts, out_ref = rest
     total = parts[0][...].astype(jnp.float32)
@@ -294,12 +317,11 @@
             got += [piece, fs_swap(piece, 1)]
         return got
 
-    def whole_rows(own):
-        near = [own, swap(own, MATE, 0)]
+    def whole_rows(near):
+        near = list(near)
         for step in range(2, n_tp, 2):
             near += [swap(piece, 0, step) for piece in near[:GROUP]]
-        across = [core_swap(piece) for piece in near]
-        return near + across
+        return near + [core_swap(piece) for piece in near]
 
     def on_device(
         tokens,
@@ -326,9 +348,8 @@
         shape = pltpu.VMEM
         normed_scratch = pltpu.VMEM((rows, features), bf16)
 
-        def reduce_out(acts, weights, base, last):
+        def core_sums(acts, weights, kinds):
             deep = acts.shape[1]
-            arrived = []
             for step in range(n_tp - 2, -1, -2):
                 send, keep = call(
                     functools.partial(project_out_kernel, step),
@@ -338,13 +359,30 @@
                 )
                 parts = call(
                     join_kernel,
-                    [shape((length, width), bf16 if step + far else f32) for far in range(GROUP)],
+                    [shape((length, width), bf16 if step else kind) for kind in kinds],
                     [keep, core_swap(send)],
                 )
+                yield step, parts
+
+        def reduce_both(acts, weights, bases):
+            found = []
+            for step, parts in core_sums(acts, weights, (f32, f32)):
+                for part in parts:
+                    found.append(swap(part, 0, step) if step else part)
+            made = call(gather_sum_kernel, shape((GROUP, length, width), bf16), found)
+            return call(
+                add_pair_kernel,
+                [shape((length, width), bf16)] * GROUP,
+                [*bases, made, swap(made, MATE, 0)],
+            )
+
+        def reduce_own(acts, weights, base):
+            found = []
+            for step, parts in core_sums(acts, weights, (f32, bf16)):
                 for far, part in enumerate(parts):
-                    moved = swap(part, MATE * far, step) if step + far else part
-                    arrived.append(moved)
-            return call(finish_kernel, last((length, width), bf16), [base, *arrived])
+                    moved = step + far
+                    found.append(swap(part, MATE * far, step) if moved else part)
+            return call(finish_kernel, jax.ShapeDtypeStruct((length, width), bf16), [base, *found])
 
         small = [mix_gain[None], conv_taps, gate_x_blocks, gate_a_blocks, forget_rate[None]]
         small += [ffn_gain[None], tokens]
@@ -358,8 +396,8 @@
         ffn_parts = call(
             split_ffn_kernel, shares * 2, [ffn_gate_w.T, ffn_up_w.T, ffn_down_w], space=pltpu.HBM
         )
-        pieces = whole_rows(tokens)
-        pieces[0] = base
+        bases = [base, swap(tokens, MATE, 0)]
+        pieces = whole_rows(bases)
         mix_w = gather(*mix_parts)
         up_w = gather(ffn_parts[0], ffn_parts[2])
         down_w = gather(ffn_parts[1], ffn_parts[3])
@@ -377,15 +415,21 @@
             ],
             [normed_scratch, pltpu.VMEM((length + 8, chans), f32)],
         )
-        after_mix = reduce_out(mixer_out, mix_w, base, shape)
+        after_mix = reduce_both(mixer_out, mix_w, bases)
         pieces = whole_rows(after_mix)
+        late = [entry for entry in range(n_fs) if entry // 2 == n_fs // 4]
+        early = [entry for entry in range(n_fs) if entry not in late]
+        sums = call(
+            functools.partial(early_kernel, len(pieces), early, n_fs),
+            [shape((rows, units), f32)] * 2 + [shape((rows, features), bf16)],
+            [ffn_gain, *pieces, *[up_w[entry] for entry in early]],
+        )
         hidden = call(
-            functools.partial(hidden_kernel, len(pieces)),
+            functools.partial(hidden_kernel, late, n_fs),
             shape((rows, units), bf16),
-            [ffn_gain, *pieces, *up_w],
-            [normed_scratch],
-        )
-        return reduce_out(hidden, down_w, after_mix, jax.ShapeDtypeStruct)
+            [*sums, *[up_w[entry] for entry in late]],
+        )
+        return reduce_own(hidden, down_w, after_mix[0])
 
     return on_device
 

time: 152 us -> 140 us (0.921)
  waiting for transfers between devices: 89.5 us -> 82.1 us
  starting transfers between devices: 51.9 us -> 48.1 us
    ppermute x9, waiting for transfers between devices: 49.7 us -> 41.7 us  [gather(): piece = lax.ppermute(other if back % 2 else mine, 'fs', pairs)]
    ppermute x12 -> x11, starting transfers between devices: 22.2 us -> 19.3 us  [swap(): return lax.ppermute(values, ('fs', 'tp'), pairs)]
    ppermute x9, starting transfers between devices: 15.2 us -> 12.3 us  [gather(): piece = lax.ppermute(other if back % 2 else mine, 'fs', pairs)]
    ppermute x12 -> x11, waiting for transfers between devices: 12.9 us -> 14.1 us  [swap(): return lax.ppermute(values, ('fs', 'tp'), pairs)]
    pallas_call x14 -> x16, Pallas kernels: 9.76 us -> 9.97 us  [call(): pl.pallas_call(kernel, out_shape=outs, in_specs=[spec] * len(args), out_s...]
  transfers between devices with their start and end apart: 45 -> 44, of which waited for: 21 -> 22; matrix products, arithmetic and copies ran while one was open for 0% -> 0% of each run, Pallas kernels for 4% -> 4%
where the time goes in v3:
time: 140 us
  waiting for transfers between devices  82.1 us (59%)
  starting transfers between devices  48.1 us (34%)
  Pallas kernels  9.97 us (7%)
    ppermute x9, waiting for transfers between devices, gather(): piece = lax.ppermute(other if back % 2 else mine, 'fs', pairs)  41.7 us
    ppermute x12, waiting for transfers between devices, fs_swap(): return lax.ppermute(values, 'fs', [(j, j ^ mask) for j in range(n_fs)])  24.1 us
    ppermute x11, starting transfers between devices, swap(): return lax.ppermute(values, ('fs', 'tp'), pairs)  19.3 us
    ppermute x12, starting transfers between devices, fs_swap(): return lax.ppermute(values, 'fs', [(j, j ^ mask) for j in range(n_fs)])  14.2 us
    ppermute x11, waiting for transfers between devices, swap(): return lax.ppermute(values, ('fs', 'tp'), pairs)  14.1 us
    ppermute x9, starting transfers between devices, gather(): piece = lax.ppermute(other if back % 2 else mine, 'fs', pairs)  12.3 us
    pallas_call x16, Pallas kernels, call(): pl.pallas_call(kernel, out_shape=outs, in_specs=[spec] * len(args), out_s...  9.97 us
  transfers between devices with their start and end apart: 44, of which 22 were waited for; matrix products, arithmetic and copies ran while one was open for 0% of the time, Pallas kernels for 4%

profile of v3, /device:TPU:0, one launch (start us, length us, event | category | flops | bytes accessed | tf_op | source)
XLA Modules:
  0.0 140.3 jit_solution(6943080649587811982)
XLA Ops:
  0.0 1.3 shard_map.127
  1.3 3.0 %collective-permute-start.1 = (bf16[160,512]{1,0:T(8,128)(2,1)S(1)}, bf16[160,512]{1,0:T(8,128)(2,1)S(1)}, u32[]{:S(2)}, u32[]{:S(2)}) collective-permute-start(bf16[160,512]{1,0:T(8,128)(2,1)S(1)} %get-tuple-element.39.rest_0_.own_ref), channel_id=1, source_target_pairs={{0,2},{1,3},{2,0},{3,1},{4,6},{5,7},{6,4},{7,5},{8,10},{9,11},{10,... | collective-permute-start | bytes 491528 | tf_op jit(solution)/shard_map/ppermute | solution.py:308
  4.3 2.6 %collective-permute-start.10 = (bf16[384,256]{1,0:T(8,128)(2,1)S(1)}, bf16[384,256]{1,0:T(8,128)(2,1)S(1)}, u32[]{:S(2)}, u32[]{:S(2)}) collective-permute-start(bf16[384,256]{1,0:T(8,128)(2,1)S(1)} %get-tuple-element.45.rest_8_.rest_0_), channel_id=1, source_target_pairs={{0,16},{4,20},{8,24},{12,28},{16,0},{20,4},{24,8},{28,12},{1,17},{... | collective-permute-start | bytes 589832 | tf_op jit(solution)/shard_map/ppermute | solution.py:316
  6.9 1.6 %collective-permute-start = (bf16[160,512]{1,0:T(8,128)(2,1)}, bf16[160,512]{1,0:T(8,128)(2,1)S(1)}, u32[]{:S(2)}, u32[]{:S(2)}) collective-permute-start(bf16[160,512]{1,0:T(8,128)(2,1)} %rest_6_.1), channel_id=1, source_target_pairs={{0,8},{1,9},{2,10},{3,11},{4,12},{5,13},{6,14},{7,15},{8,0},{9,1},... | collective-permute-start | bytes 491528 | tf_op jit(solution)/shard_map/ppermute | solution.py:308
  8.7 1.8 %collective-permute-start.8 = (bf16[384,256]{1,0:T(8,128)(2,1)S(1)}, bf16[384,256]{1,0:T(8,128)(2,1)S(1)}, u32[]{:S(2)}, u32[]{:S(2)}) collective-permute-start(bf16[384,256]{1,0:T(8,128)(2,1)S(1)} %get-tuple-element.46), channel_id=1, source_target_pairs={{0,8},{4,12},{8,16},{12,20},{16,24},{20,28},{24,0},{28,4},{1,9},{5... | collective-permute-start | bytes 589832 | tf_op jit(solution)/shard_map/ppermute | solution.py:316
  10.5 1.5 %collective-permute-start.7 = (bf16[384,256]{1,0:T(8,128)(2,1)S(1)}, bf16[384,256]{1,0:T(8,128)(2,1)S(1)}, u32[]{:S(2)}, u32[]{:S(2)}) collective-permute-start(bf16[384,256]{1,0:T(8,128)(2,1)S(1)} %get-tuple-element.45.rest_8_.rest_0_), channel_id=1, source_target_pairs={{0,4},{4,0},{8,12},{12,8},{16,20},{20,16},{24,28},{28,24},{1,5},{5... | collective-permute-start | bytes 589832 | tf_op jit(solution)/shard_map/ppermute | solution.py:297
  12.1 5.3 %collective-permute-done.rest_1_.mate_ref = bf16[160,512]{1,0:T(8,128)(2,1)S(1)} collective-permute-done((bf16[160,512]{1,0:T(8,128)(2,1)}, bf16[160,512]{1,0:T(8,128)(2,1)S(1)}, u32[]{:S(2)}, u32[]{:S(2)}) %collective-permute-start) | collective-permute-done | bytes 163872 | tf_op jit(solution)/shard_map/ppermute | solution.py:308
  17.3 0.5 collective-permute-start.2
  17.8 3.0 %collective-permute-done.12.rest_14_.rest_6_ = bf16[384,256]{1,0:T(8,128)(2,1)S(1)} collective-permute-done((bf16[384,256]{1,0:T(8,128)(2,1)S(1)}, bf16[384,256]{1,0:T(8,128)(2,1)S(1)}, u32[]{:S(2)}, u32[]{:S(2)}) %collective-permute-start.12) | collective-permute-done | bytes 196640 | tf_op jit(solution)/shard_map/ppermute | solution.py:316
  20.8 1.5 %collective-permute-start.11 = (bf16[384,256]{1,0:T(8,128)(2,1)S(1)}, bf16[384,256]{1,0:T(8,128)(2,1)S(1)}, u32[]{:S(2)}, u32[]{:S(2)}) collective-permute-start(bf16[384,256]{1,0:T(8,128)(2,1)S(1)} %collective-permute-done.10.rest_12_.rest_4_), channel_id=1, source_target_pairs={{0,4},{4,0},{8,12},{12,8},{16,20},{20,16},{24,28},{28,24},{1,5},{5... | collective-permute-start | bytes 589832 | tf_op jit(solution)/shard_map/ppermute | solution.py:297
  22.3 3.2 %collective-permute-done.8.rest_10_.rest_2_ = bf16[384,256]{1,0:T(8,128)(2,1)S(1)} collective-permute-done((bf16[384,256]{1,0:T(8,128)(2,1)S(1)}, bf16[384,256]{1,0:T(8,128)(2,1)S(1)}, u32[]{:S(2)}, u32[]{:S(2)}) %collective-permute-start.8) | collective-permute-done | bytes 196640 | tf_op jit(solution)/shard_map/ppermute | solution.py:316
  25.6 1.5 %collective-permute-start.13 = (bf16[384,256]{1,0:T(8,128)(2,1)S(1)}, bf16[384,256]{1,0:T(8,128)(2,1)S(1)}, u32[]{:S(2)}, u32[]{:S(2)}) collective-permute-start(bf16[384,256]{1,0:T(8,128)(2,1)S(1)} %collective-permute-done.12.rest_14_.rest_6_), channel_id=1, source_target_pairs={{0,4},{4,0},{8,12},{12,8},{16,20},{20,16},{24,28},{28,24},{1,5},{5... | collective-permute-start | bytes 589832 | tf_op jit(solution)/shard_map/ppermute | solution.py:297
  27.1 0.5 collective-permute-start.9
  27.6 0.5 collective-permute-start.6
  28.1 0.9 collective-permute-done.4.rest_5_
  29.0 4.3 %collective-permute-done.13.rest_15_.rest_7_ = bf16[384,256]{1,0:T(8,128)(2,1)S(1)} collective-permute-done((bf16[384,256]{1,0:T(8,128)(2,1)S(1)}, bf16[384,256]{1,0:T(8,128)(2,1)S(1)}, u32[]{:S(2)}, u32[]{:S(2)}) %collective-permute-start.13) | collective-permute-done | bytes 196640 | tf_op jit(solution)/shard_map/ppermute | solution.py:297
  33.3 2.9 %collective-permute-done.9.rest_11_.rest_3_ = bf16[384,256]{1,0:T(8,128)(2,1)S(1)} collective-permute-done((bf16[384,256]{1,0:T(8,128)(2,1)S(1)}, bf16[384,256]{1,0:T(8,128)(2,1)S(1)}, u32[]{:S(2)}, u32[]{:S(2)}) %collective-permute-start.9) | collective-permute-done | bytes 196640 | tf_op jit(solution)/shard_map/ppermute | solution.py:297
  36.2 1.7 %shard_map.128.acts_ref = bf16[320,128]{1,0:T(8,128)(2,1)S(1)} custom-call(f32[1,2048]{1,0:T(1,128)S(1)} %get-tuple-element.40.gain_ref, f32[4,256]{1,0:T(4,128)S(1)} %get-tuple-element.41.taps_ref, bf16[2,128,128]{2,1,0:T(8,128)(2,1)S(1)} %get-tuple-element.42.x_maps_ref, bf16[2,128,128]{2,1,0:T(8,128)(2,1)S(1)} %get-tuple-element.43.a_maps_ref, ...), custom_call_target="tpu_custom_call" | custom-call | tf_op jit(solution)/shard_map/pallas_call | solution.py:106
  37.9 0.4 shard_map.129
  38.4 0.4 shard_map.131
  38.8 0.6 collective-permute-start.17
  39.3 0.7 collective-permute-done.14.got_ref
  40.1 0.6 collective-permute-start.15
  40.7 1.5 %collective-permute-start.16 = (bf16[160,512]{1,0:T(8,128)(2,1)S(1)}, bf16[160,512]{1,0:T(8,128)(2,1)S(1)}, u32[]{:S(2)}, u32[]{:S(2)}) collective-permute-start(bf16[160,512]{1,0:T(8,128)(2,1)S(1)} %get-tuple-element.50), channel_id=1, source_target_pairs={{0,2},{1,3},{2,0},{3,1},{4,6},{5,7},{6,4},{7,5},{8,10},{9,11},{10,... | collective-permute-start | bytes 491528 | tf_op jit(solution)/shard_map/ppermute | solution.py:308
  42.2 1.3 shard_map.135
  43.4 0.8 collective-permute-start.26
  44.3 3.1 %collective-permute-start.28 = (bf16[704,256]{1,0:T(8,128)(2,1)S(1)}, bf16[704,256]{1,0:T(8,128)(2,1)S(1)}, u32[]{:S(2)}, u32[]{:S(2)}) collective-permute-start(bf16[704,256]{1,0:T(8,128)(2,1)S(1)} %get-tuple-element.59), channel_id=1, source_target_pairs={{0,24},{4,28},{8,0},{12,4},{16,8},{20,12},{24,16},{28,20},{1,25},{... | collective-permute-start | bytes 1081352 | tf_op jit(solution)/shard_map/ppermute | solution.py:316
  47.4 0.8 collective-permute-start.35
  48.3 1.6 %collective-permute-done.16.refs_1_ = bf16[160,512]{1,0:T(8,128)(2,1)S(1)} collective-permute-done((bf16[160,512]{1,0:T(8,128)(2,1)S(1)}, bf16[160,512]{1,0:T(8,128)(2,1)S(1)}, u32[]{:S(2)}, u32[]{:S(2)}) %collective-permute-start.16) | collective-permute-done | bytes 163872 | tf_op jit(solution)/shard_map/ppermute | solution.py:308
  49.9 0.9 collective-permute-start.18
  50.8 1.2 collective-permute-start.33
  52.0 19.0 %collective-permute-done.35.rest_4_ = bf16[352,256]{1,0:T(8,128)(2,1)S(1)} collective-permute-done((bf16[352,256]{1,0:T(8,128)(2,1)S(1)}, bf16[352,256]{1,0:T(8,128)(2,1)S(1)}, u32[]{:S(2)}, u32[]{:S(2)}) %collective-permute-start.35) | collective-permute-done | bytes 180256 | tf_op jit(solution)/shard_map/ppermute | solution.py:316
  71.1 1.5 %collective-permute-start.25 = (bf16[704,256]{1,0:T(8,128)(2,1)S(1)}, bf16[704,256]{1,0:T(8,128)(2,1)S(1)}, u32[]{:S(2)}, u32[]{:S(2)}) collective-permute-start(bf16[704,256]{1,0:T(8,128)(2,1)S(1)} %get-tuple-element.58.rest_8_), channel_id=1, source_target_pairs={{0,4},{4,0},{8,12},{12,8},{16,20},{20,16},{24,28},{28,24},{1,5},{5... | collective-permute-start | bytes 1081352 | tf_op jit(solution)/shard_map/ppermute | solution.py:297
  72.6 5.5 %collective-permute-done.33.rest_2_ = bf16[352,256]{1,0:T(8,128)(2,1)S(1)} collective-permute-done((bf16[352,256]{1,0:T(8,128)(2,1)S(1)}, bf16[352,256]{1,0:T(8,128)(2,1)S(1)}, u32[]{:S(2)}, u32[]{:S(2)}) %collective-permute-start.33) | collective-permute-done | bytes 180256 | tf_op jit(solution)/shard_map/ppermute | solution.py:316
  78.1 1.5 %collective-permute-start.27 = (bf16[704,256]{1,0:T(8,128)(2,1)S(1)}, bf16[704,256]{1,0:T(8,128)(2,1)S(1)}, u32[]{:S(2)}, u32[]{:S(2)}) collective-permute-start(bf16[704,256]{1,0:T(8,128)(2,1)S(1)} %collective-permute-done.26.rest_10_), channel_id=1, source_target_pairs={{0,4},{4,0},{8,12},{12,8},{16,20},{20,16},{24,28},{28,24},{1,5},{5... | collective-permute-start | bytes 1081352 | tf_op jit(solution)/shard_map/ppermute | solution.py:297
  79.6 0.5 collective-permute-start.29
  80.1 1.7 %collective-permute-start.37 = (bf16[352,256]{1,0:T(8,128)(2,1)S(1)}, bf16[352,256]{1,0:T(8,128)(2,1)S(1)}, u32[]{:S(2)}, u32[]{:S(2)}) collective-permute-start(bf16[352,256]{1,0:T(8,128)(2,1)S(1)} %get-tuple-element.64), channel_id=1, source_target_pairs={{0,24},{4,28},{8,0},{12,4},{16,8},{20,12},{24,16},{28,20},{1,25},{... | collective-permute-start | bytes 540680 | tf_op jit(solution)/shard_map/ppermute | solution.py:316
  81.9 7.2 %collective-permute-done.37.rest_6_ = bf16[352,256]{1,0:T(8,128)(2,1)S(1)} collective-permute-done((bf16[352,256]{1,0:T(8,128)(2,1)S(1)}, bf16[352,256]{1,0:T(8,128)(2,1)S(1)}, u32[]{:S(2)}, u32[]{:S(2)}) %collective-permute-start.37) | collective-permute-done | bytes 180256 | tf_op jit(solution)/shard_map/ppermute | solution.py:316
  89.1 1.5 %collective-permute-start.19 = (bf16[160,512]{1,0:T(8,128)(2,1)S(1)}, bf16[160,512]{1,0:T(8,128)(2,1)S(1)}, u32[]{:S(2)}, u32[]{:S(2)}) collective-permute-start(bf16[160,512]{1,0:T(8,128)(2,1)S(1)} %get-tuple-element.55.rest_0_.base_ref), channel_id=1, source_target_pairs={{0,2},{1,3},{2,0},{3,1},{4,6},{5,7},{6,4},{7,5},{8,10},{9,11},{10,... | collective-permute-start | bytes 491528 | tf_op jit(solution)/shard_map/ppermute | solution.py:308
  90.6 0.5 collective-permute-start.20
  91.1 3.7 %collective-permute-done.30.rest_0_ = bf16[704,256]{1,0:T(8,128)(2,1)S(1)} collective-permute-done((bf16[704,256]{1,0:T(8,128)(2,1)S(1)}, bf16[704,256]{1,0:T(8,128)(2,1)S(1)}, u32[]{:S(2)}, u32[]{:S(2)}) %collective-permute-start.30) | collective-permute-done | bytes 360480 | tf_op jit(solution)/shard_map/ppermute | solution.py:316
  94.8 1.5 %collective-permute-start.31 = (bf16[704,256]{1,0:T(8,128)(2,1)S(1)}, bf16[704,256]{1,0:T(8,128)(2,1)S(1)}, u32[]{:S(2)}, u32[]{:S(2)}) collective-permute-start(bf16[704,256]{1,0:T(8,128)(2,1)S(1)} %collective-permute-done.30.rest_0_), channel_id=1, source_target_pairs={{0,4},{4,0},{8,12},{12,8},{16,20},{20,16},{24,28},{28,24},{1,5},{5... | collective-permute-start | bytes 1081352 | tf_op jit(solution)/shard_map/ppermute | solution.py:297
  96.4 0.4 collective-permute-done.29.rest_13_
  96.9 0.4 collective-permute-start.23
  97.7 1.1 collective-permute-start.32
  98.9 0.9 collective-permute-start.36
  99.8 1.1 collective-permute-start.34
  100.9 0.9 collective-permute-start.38
  101.8 1.8 %shard_map.136 = (f32[320,352]{1,0:T(8,128)S(1)}, f32[320,352]{1,0:T(8,128)S(1)}, bf16[320,2048]{1,0:T(8,128)(2,1)S(1)}) custom-call(f32[1,2048]{1,0:T(1,128)S(1)} %get-tuple-element.56.gain_ref, bf16[160,512]{1,0:T(8,128)(2,1)S(1)} %get-tuple-element.55.rest_0_.base_ref, bf16[160,512]{1,0:T(8,128)(2,1)S(1)} %get-tuple-element.57.rest_1_, ...), custom_call_target="tpu_custom_call" | custom-call | tf_op jit(solution)/shard_map/pallas_call | solution.py:106
  103.6 2.5 %collective-permute-done.31.rest_1_ = bf16[704,256]{1,0:T(8,128)(2,1)S(1)} collective-permute-done((bf16[704,256]{1,0:T(8,128)(2,1)S(1)}, bf16[704,256]{1,0:T(8,128)(2,1)S(1)}, u32[]{:S(2)}, u32[]{:S(2)}) %collective-permute-start.31) | collective-permute-done | bytes 360480 | tf_op jit(solution)/shard_map/ppermute | solution.py:297
  106.1 0.5 shard_map.137.acts_ref
  106.7 3.3 %collective-permute-done.32.rest_1_ = bf16[352,256]{1,0:T(8,128)(2,1)S(1)} collective-permute-done((bf16[352,256]{1,0:T(8,128)(2,1)S(1)}, bf16[352,256]{1,0:T(8,128)(2,1)S(1)}, u32[]{:S(2)}, u32[]{:S(2)}) %collective-permute-start.32) | collective-permute-done | bytes 180256 | tf_op jit(solution)/shard_map/ppermute | solution.py:297
  110.0 3.9 %collective-permute-done.36.rest_5_ = bf16[352,256]{1,0:T(8,128)(2,1)S(1)} collective-permute-done((bf16[352,256]{1,0:T(8,128)(2,1)S(1)}, bf16[352,256]{1,0:T(8,128)(2,1)S(1)}, u32[]{:S(2)}, u32[]{:S(2)}) %collective-permute-start.36) | collective-permute-done | bytes 180256 | tf_op jit(solution)/shard_map/ppermute | solution.py:297
  113.8 3.9 %collective-permute-done.34.rest_3_ = bf16[352,256]{1,0:T(8,128)(2,1)S(1)} collective-permute-done((bf16[352,256]{1,0:T(8,128)(2,1)S(1)}, bf16[352,256]{1,0:T(8,128)(2,1)S(1)}, u32[]{:S(2)}, u32[]{:S(2)}) %collective-permute-start.34) | collective-permute-done | bytes 180256 | tf_op jit(solution)/shard_map/ppermute | solution.py:297
  117.7 2.8 %collective-permute-done.38.rest_7_ = bf16[352,256]{1,0:T(8,128)(2,1)S(1)} collective-permute-done((bf16[352,256]{1,0:T(8,128)(2,1)S(1)}, bf16[352,256]{1,0:T(8,128)(2,1)S(1)}, u32[]{:S(2)}, u32[]{:S(2)}) %collective-permute-start.38) | collective-permute-done | bytes 180256 | tf_op jit(solution)/shard_map/ppermute | solution.py:297
  120.5 0.7 shard_map.140
  121.3 0.7 shard_map.138
  122.0 0.6 collective-permute-start.39
  123.0 6.9 %collective-permute-start.43 = (bf16[160,512]{1,0:T(8,128)(2,1)S(1)}, bf16[160,512]{1,0:T(8,128)(2,1)S(1)}, u32[]{:S(2)}, u32[]{:S(2)}) collective-permute-start(bf16[160,512]{1,0:T(8,128)(2,1)S(1)} %get-tuple-element.72), channel_id=1, source_target_pairs={{0,8},{1,9},{2,10},{3,11},{4,12},{5,13},{6,14},{7,15},{8,0},{9,1},... | collective-permute-start | bytes 491528 | tf_op jit(solution)/shard_map/ppermute | solution.py:308
  130.0 1.6 %collective-permute-start.40 = (bf16[160,512]{1,0:T(8,128)(2,1)S(1)}, bf16[160,512]{1,0:T(8,128)(2,1)S(1)}, u32[]{:S(2)}, u32[]{:S(2)}) collective-permute-start(bf16[160,512]{1,0:T(8,128)(2,1)S(1)} %get-tuple-element.67), channel_id=1, source_target_pairs={{0,2},{1,3},{2,0},{3,1},{4,6},{5,7},{6,4},{7,5},{8,10},{9,11},{10,... | collective-permute-start | bytes 491528 | tf_op jit(solution)/shard_map/ppermute | solution.py:308
  131.5 0.7 collective-permute-start.41
  132.3 2.7 %collective-permute-done.43.rest_3_ = bf16[160,512]{1,0:T(8,128)(2,1)S(1)} collective-permute-done((bf16[160,512]{1,0:T(8,128)(2,1)S(1)}, bf16[160,512]{1,0:T(8,128)(2,1)S(1)}, u32[]{:S(2)}, u32[]{:S(2)}) %collective-permute-start.43) | collective-permute-done | bytes 163872 | tf_op jit(solution)/shard_map/ppermute | solution.py:308
  134.9 4.6 %collective-permute-done.40.rest_0_ = bf16[160,512]{1,0:T(8,128)(2,1)S(1)} collective-permute-done((bf16[160,512]{1,0:T(8,128)(2,1)S(1)}, bf16[160,512]{1,0:T(8,128)(2,1)S(1)}, u32[]{:S(2)}, u32[]{:S(2)}) %collective-permute-start.40) | collective-permute-done | bytes 163872 | tf_op jit(solution)/shard_map/ppermute | solution.py:308
  139.5 0.8 shard_map.142
  (40 shorter events, 1.8 us)
Async XLA Ops:
  1.3 7.4 %collective-permute-start.1 = (bf16[160,512]{1,0:T(8,128)(2,1)S(1)}, bf16[160,512]{1,0:T(8,128)(2,1)S(1)}, u32[]{:S(2)}, u32[]{:S(2)}) collective-permute-start(bf16[160,512]{1,0:T(8,128)(2,1)S(1)} %get-tuple-element.39.rest_0_.own_ref), channel_id=1, source_target_pairs={{0,2},{1,3},{2,0},{3,1},{4,6},{5,7},{6,4},{7,5},{8,10},{9,11},{10,... | collective-permute-start | bytes 491528 | tf_op jit(solution)/shard_map/ppermute | solution.py:308
  4.3 6.2 %collective-permute-start.3 = (bf16[160,512]{1,0:T(8,128)(2,1)S(1)}, bf16[160,512]{1,0:T(8,128)(2,1)S(1)}, u32[]{:S(2)}, u32[]{:S(2)}) collective-permute-start(bf16[160,512]{1,0:T(8,128)(2,1)S(1)} %get-tuple-element.39.rest_0_.own_ref), channel_id=1, source_target_pairs={{0,1},{1,0},{2,3},{3,2},{4,5},{5,4},{6,7},{7,6},{8,9},{9,8},{10,11... | collective-permute-start | bytes 491528 | tf_op jit(solution)/shard_map/ppermute | solution.py:300
  4.3 13.0 %collective-permute-start.10 = (bf16[384,256]{1,0:T(8,128)(2,1)S(1)}, bf16[384,256]{1,0:T(8,128)(2,1)S(1)}, u32[]{:S(2)}, u32[]{:S(2)}) collective-permute-start(bf16[384,256]{1,0:T(8,128)(2,1)S(1)} %get-tuple-element.45.rest_8_.rest_0_), channel_id=1, source_target_pairs={{0,16},{4,20},{8,24},{12,28},{16,0},{20,4},{24,8},{28,12},{1,17},{... | collective-permute-start | bytes 589832 | tf_op jit(solution)/shard_map/ppermute | solution.py:316
  6.9 10.4 %collective-permute-start = (bf16[160,512]{1,0:T(8,128)(2,1)}, bf16[160,512]{1,0:T(8,128)(2,1)S(1)}, u32[]{:S(2)}, u32[]{:S(2)}) collective-permute-start(bf16[160,512]{1,0:T(8,128)(2,1)} %rest_6_.1), channel_id=1, source_target_pairs={{0,8},{1,9},{2,10},{3,11},{4,12},{5,13},{6,14},{7,15},{8,0},{9,1},... | collective-permute-start | bytes 491528 | tf_op jit(solution)/shard_map/ppermute | solution.py:308
  8.5 12.3 %collective-permute-start.12 = (bf16[384,256]{1,0:T(8,128)(2,1)S(1)}, bf16[384,256]{1,0:T(8,128)(2,1)S(1)}, u32[]{:S(2)}, u32[]{:S(2)}) collective-permute-start(bf16[384,256]{1,0:T(8,128)(2,1)S(1)} %get-tuple-element.46), channel_id=1, source_target_pairs={{0,24},{4,28},{8,0},{12,4},{16,8},{20,12},{24,16},{28,20},{1,25},{... | collective-permute-start | bytes 589832 | tf_op jit(solution)/shard_map/ppermute | solution.py:316
  8.7 16.8 %collective-permute-start.8 = (bf16[384,256]{1,0:T(8,128)(2,1)S(1)}, bf16[384,256]{1,0:T(8,128)(2,1)S(1)}, u32[]{:S(2)}, u32[]{:S(2)}) collective-permute-start(bf16[384,256]{1,0:T(8,128)(2,1)S(1)} %get-tuple-element.46), channel_id=1, source_target_pairs={{0,8},{4,12},{8,16},{12,20},{16,24},{20,28},{24,0},{28,4},{1,9},{5... | collective-permute-start | bytes 589832 | tf_op jit(solution)/shard_map/ppermute | solution.py:316
  10.5 16.5 %collective-permute-start.7 = (bf16[384,256]{1,0:T(8,128)(2,1)S(1)}, bf16[384,256]{1,0:T(8,128)(2,1)S(1)}, u32[]{:S(2)}, u32[]{:S(2)}) collective-permute-start(bf16[384,256]{1,0:T(8,128)(2,1)S(1)} %get-tuple-element.45.rest_8_.rest_0_), channel_id=1, source_target_pairs={{0,4},{4,0},{8,12},{12,8},{16,20},{20,16},{24,28},{28,24},{1,5},{5... | collective-permute-start | bytes 589832 | tf_op jit(solution)/shard_map/ppermute | solution.py:297
  17.3 10.3 %collective-permute-start.5 = (bf16[160,512]{1,0:T(8,128)(2,1)S(1)}, bf16[160,512]{1,0:T(8,128)(2,1)S(1)}, u32[]{:S(2)}, u32[]{:S(2)}) collective-permute-start(bf16[160,512]{1,0:T(8,128)(2,1)S(1)} %collective-permute-done.1.rest_2_), channel_id=1, source_target_pairs={{0,1},{1,0},{2,3},{3,2},{4,5},{5,4},{6,7},{7,6},{8,9},{9,8},{10,11... | collective-permute-start | bytes 491528 | tf_op jit(solution)/shard_map/ppermute | solution.py:300
  17.3 10.3 %collective-permute-start.2 = (bf16[160,512]{1,0:T(8,128)(2,1)S(1)}, bf16[160,512]{1,0:T(8,128)(2,1)S(1)}, u32[]{:S(2)}, u32[]{:S(2)}) collective-permute-start(bf16[160,512]{1,0:T(8,128)(2,1)S(1)} %collective-permute-done.rest_1_.mate_ref), channel_id=1, source_target_pairs={{0,2},{1,3},{2,0},{3,1},{4,6},{5,7},{6,4},{7,5},{8,10},{9,11},{10,... | collective-permute-start | bytes 491528 | tf_op jit(solution)/shard_map/ppermute | solution.py:308
  20.8 8.2 %collective-permute-start.11 = (bf16[384,256]{1,0:T(8,128)(2,1)S(1)}, bf16[384,256]{1,0:T(8,128)(2,1)S(1)}, u32[]{:S(2)}, u32[]{:S(2)}) collective-permute-start(bf16[384,256]{1,0:T(8,128)(2,1)S(1)} %collective-permute-done.10.rest_12_.rest_4_), channel_id=1, source_target_pairs={{0,4},{4,0},{8,12},{12,8},{16,20},{20,16},{24,28},{28,24},{1,5},{5... | collective-permute-start | bytes 589832 | tf_op jit(solution)/shard_map/ppermute | solution.py:297
  25.6 7.8 %collective-permute-start.13 = (bf16[384,256]{1,0:T(8,128)(2,1)S(1)}, bf16[384,256]{1,0:T(8,128)(2,1)S(1)}, u32[]{:S(2)}, u32[]{:S(2)}) collective-permute-start(bf16[384,256]{1,0:T(8,128)(2,1)S(1)} %collective-permute-done.12.rest_14_.rest_6_), channel_id=1, source_target_pairs={{0,4},{4,0},{8,12},{12,8},{16,20},{20,16},{24,28},{28,24},{1,5},{5... | collective-permute-start | bytes 589832 | tf_op jit(solution)/shard_map/ppermute | solution.py:297
  27.1 9.1 %collective-permute-start.9 = (bf16[384,256]{1,0:T(8,128)(2,1)S(1)}, bf16[384,256]{1,0:T(8,128)(2,1)S(1)}, u32[]{:S(2)}, u32[]{:S(2)}) collective-permute-start(bf16[384,256]{1,0:T(8,128)(2,1)S(1)} %collective-permute-done.8.rest_10_.rest_2_), channel_id=1, source_target_pairs={{0,4},{4,0},{8,12},{12,8},{16,20},{20,16},{24,28},{28,24},{1,5},{5... | collective-permute-start | bytes 589832 | tf_op jit(solution)/shard_map/ppermute | solution.py:297
  27.6 1.4 collective-permute-start.4
  27.6 8.6 %collective-permute-start.6 = (bf16[160,512]{1,0:T(8,128)(2,1)S(1)}, bf16[160,512]{1,0:T(8,128)(2,1)S(1)}, u32[]{:S(2)}, u32[]{:S(2)}) collective-permute-start(bf16[160,512]{1,0:T(8,128)(2,1)S(1)} %collective-permute-done.2.rest_3_), channel_id=1, source_target_pairs={{0,1},{1,0},{2,3},{3,2},{4,5},{5,4},{6,7},{7,6},{8,9},{9,8},{10,11... | collective-permute-start | bytes 491528 | tf_op jit(solution)/shard_map/ppermute | solution.py:300
  38.3 1.7 %collective-permute-start.14 = (bf16[2,160,512]{2,1,0:T(8,128)(2,1)S(1)}, bf16[2,160,512]{2,1,0:T(8,128)(2,1)S(1)}, u32[]{:S(2)}, u32[]{:S(2)}) collective-permute-start(bf16[2,160,512]{2,1,0:T(8,128)(2,1)S(1)} %get-tuple-element.48), channel_id=1, source_target_pairs={{0,1},{1,0},{2,3},{3,2},{4,5},{5,4},{6,7},{7,6},{8,9},{9,8},{10,11... | collective-permute-start | bytes 983048 | tf_op jit(solution)/shard_map/ppermute | solution.py:300
  38.8 8.7 %collective-permute-start.17 = (bf16[2,160,512]{2,1,0:T(8,128)(2,1)S(1)}, bf16[2,160,512]{2,1,0:T(8,128)(2,1)S(1)}, u32[]{:S(2)}, u32[]{:S(2)}) collective-permute-start(bf16[2,160,512]{2,1,0:T(8,128)(2,1)S(1)} %get-tuple-element.52), channel_id=1, source_target_pairs={{0,1},{1,0},{2,3},{3,2},{4,5},{5,4},{6,7},{7,6},{8,9},{9,8},{10,11... | collective-permute-start | bytes 983048 | tf_op jit(solution)/shard_map/ppermute | solution.py:300
  40.1 8.2 %collective-permute-start.15 = (bf16[160,512]{1,0:T(8,128)(2,1)S(1)}, bf16[160,512]{1,0:T(8,128)(2,1)S(1)}, u32[]{:S(2)}, u32[]{:S(2)}) collective-permute-start(bf16[160,512]{1,0:T(8,128)(2,1)S(1)} %get-tuple-element.49), channel_id=1, source_target_pairs={{0,2},{1,3},{2,0},{3,1},{4,6},{5,7},{6,4},{7,5},{8,10},{9,11},{10,... | collective-permute-start | bytes 491528 | tf_op jit(solution)/shard_map/ppermute | solution.py:308
  40.7 9.2 %collective-permute-start.16 = (bf16[160,512]{1,0:T(8,128)(2,1)S(1)}, bf16[160,512]{1,0:T(8,128)(2,1)S(1)}, u32[]{:S(2)}, u32[]{:S(2)}) collective-permute-start(bf16[160,512]{1,0:T(8,128)(2,1)S(1)} %get-tuple-element.50), channel_id=1, source_target_pairs={{0,2},{1,3},{2,0},{3,1},{4,6},{5,7},{6,4},{7,5},{8,10},{9,11},{10,... | collective-permute-start | bytes 491528 | tf_op jit(solution)/shard_map/ppermute | solution.py:308
  43.4 34.6 %collective-permute-start.26 = (bf16[704,256]{1,0:T(8,128)(2,1)S(1)}, bf16[704,256]{1,0:T(8,128)(2,1)S(1)}, u32[]{:S(2)}, u32[]{:S(2)}) collective-permute-start(bf16[704,256]{1,0:T(8,128)(2,1)S(1)} %get-tuple-element.59), channel_id=1, source_target_pairs={{0,8},{4,12},{8,16},{12,20},{16,24},{20,28},{24,0},{28,4},{1,9},{5... | collective-permute-start | bytes 1081352 | tf_op jit(solution)/shard_map/ppermute | solution.py:316
  44.3 35.3 %collective-permute-start.28 = (bf16[704,256]{1,0:T(8,128)(2,1)S(1)}, bf16[704,256]{1,0:T(8,128)(2,1)S(1)}, u32[]{:S(2)}, u32[]{:S(2)}) collective-permute-start(bf16[704,256]{1,0:T(8,128)(2,1)S(1)} %get-tuple-element.59), channel_id=1, source_target_pairs={{0,24},{4,28},{8,0},{12,4},{16,8},{20,12},{24,16},{28,20},{1,25},{... | collective-permute-start | bytes 1081352 | tf_op jit(solution)/shard_map/ppermute | solution.py:316
  47.4 23.6 %collective-permute-start.35 = (bf16[352,256]{1,0:T(8,128)(2,1)S(1)}, bf16[352,256]{1,0:T(8,128)(2,1)S(1)}, u32[]{:S(2)}, u32[]{:S(2)}) collective-permute-start(bf16[352,256]{1,0:T(8,128)(2,1)S(1)} %get-tuple-element.63.rest_0_), channel_id=1, source_target_pairs={{0,16},{4,20},{8,24},{12,28},{16,0},{20,4},{24,8},{28,12},{1,17},{... | collective-permute-start | bytes 540680 | tf_op jit(solution)/shard_map/ppermute | solution.py:316
  49.9 30.2 %collective-permute-start.18 = (bf16[2,160,512]{2,1,0:T(8,128)(2,1)S(1)}, bf16[2,160,512]{2,1,0:T(8,128)(2,1)S(1)}, u32[]{:S(2)}, u32[]{:S(2)}) collective-permute-start(bf16[2,160,512]{2,1,0:T(8,128)(2,1)S(1)} %shard_map.133.made_ref), channel_id=1, source_target_pairs={{0,8},{1,9},{2,10},{3,11},{4,12},{5,13},{6,14},{7,15},{8,0},{9,1},... | collective-permute-start | bytes 983048 | tf_op jit(solution)/shard_map/ppermute | solution.py:308
  50.8 27.3 %collective-permute-start.33 = (bf16[352,256]{1,0:T(8,128)(2,1)S(1)}, bf16[352,256]{1,0:T(8,128)(2,1)S(1)}, u32[]{:S(2)}, u32[]{:S(2)}) collective-permute-start(bf16[352,256]{1,0:T(8,128)(2,1)S(1)} %get-tuple-element.64), channel_id=1, source_target_pairs={{0,8},{4,12},{8,16},{12,20},{16,24},{20,28},{24,0},{28,4},{1,9},{5... | collective-permute-start | bytes 540680 | tf_op jit(solution)/shard_map/ppermute | solution.py:316
  71.1 19.5 %collective-permute-start.25 = (bf16[704,256]{1,0:T(8,128)(2,1)S(1)}, bf16[704,256]{1,0:T(8,128)(2,1)S(1)}, u32[]{:S(2)}, u32[]{:S(2)}) collective-permute-start(bf16[704,256]{1,0:T(8,128)(2,1)S(1)} %get-tuple-element.58.rest_8_), channel_id=1, source_target_pairs={{0,4},{4,0},{8,12},{12,8},{16,20},{20,16},{24,28},{28,24},{1,5},{5... | collective-permute-start | bytes 1081352 | tf_op jit(solution)/shard_map/ppermute | solution.py:297
  78.1 16.8 %collective-permute-start.30 = (bf16[704,256]{1,0:T(8,128)(2,1)S(1)}, bf16[704,256]{1,0:T(8,128)(2,1)S(1)}, u32[]{:S(2)}, u32[]{:S(2)}) collective-permute-start(bf16[704,256]{1,0:T(8,128)(2,1)S(1)} %get-tuple-element.58.rest_8_), channel_id=1, source_target_pairs={{0,16},{4,20},{8,24},{12,28},{16,0},{20,4},{24,8},{28,12},{1,17},{... | collective-permute-start | bytes 1081352 | tf_op jit(solution)/shard_map/ppermute | solution.py:316
  78.1 18.3 %collective-permute-start.27 = (bf16[704,256]{1,0:T(8,128)(2,1)S(1)}, bf16[704,256]{1,0:T(8,128)(2,1)S(1)}, u32[]{:S(2)}, u32[]{:S(2)}) collective-permute-start(bf16[704,256]{1,0:T(8,128)(2,1)S(1)} %collective-permute-done.26.rest_10_), channel_id=1, source_target_pairs={{0,4},{4,0},{8,12},{12,8},{16,20},{20,16},{24,28},{28,24},{1,5},{5... | collective-permute-start | bytes 1081352 | tf_op jit(solution)/shard_map/ppermute | solution.py:297
  79.6 17.2 %collective-permute-start.29 = (bf16[704,256]{1,0:T(8,128)(2,1)S(1)}, bf16[704,256]{1,0:T(8,128)(2,1)S(1)}, u32[]{:S(2)}, u32[]{:S(2)}) collective-permute-start(bf16[704,256]{1,0:T(8,128)(2,1)S(1)} %collective-permute-done.28.rest_12_), channel_id=1, source_target_pairs={{0,4},{4,0},{8,12},{12,8},{16,20},{20,16},{24,28},{28,24},{1,5},{5... | collective-permute-start | bytes 1081352 | tf_op jit(solution)/shard_map/ppermute | solution.py:297
  80.1 9.0 %collective-permute-start.37 = (bf16[352,256]{1,0:T(8,128)(2,1)S(1)}, bf16[352,256]{1,0:T(8,128)(2,1)S(1)}, u32[]{:S(2)}, u32[]{:S(2)}) collective-permute-start(bf16[352,256]{1,0:T(8,128)(2,1)S(1)} %get-tuple-element.64), channel_id=1, source_target_pairs={{0,24},{4,28},{8,0},{12,4},{16,8},{20,12},{24,16},{28,20},{1,25},{... | collective-permute-start | bytes 540680 | tf_op jit(solution)/shard_map/ppermute | solution.py:316
  89.1 7.8 %collective-permute-start.19 = (bf16[160,512]{1,0:T(8,128)(2,1)S(1)}, bf16[160,512]{1,0:T(8,128)(2,1)S(1)}, u32[]{:S(2)}, u32[]{:S(2)}) collective-permute-start(bf16[160,512]{1,0:T(8,128)(2,1)S(1)} %get-tuple-element.55.rest_0_.base_ref), channel_id=1, source_target_pairs={{0,2},{1,3},{2,0},{3,1},{4,6},{5,7},{6,4},{7,5},{8,10},{9,11},{10,... | collective-permute-start | bytes 491528 | tf_op jit(solution)/shard_map/ppermute | solution.py:308
  90.6 6.7 %collective-permute-start.20 = (bf16[160,512]{1,0:T(8,128)(2,1)S(1)}, bf16[160,512]{1,0:T(8,128)(2,1)S(1)}, u32[]{:S(2)}, u32[]{:S(2)}) collective-permute-start(bf16[160,512]{1,0:T(8,128)(2,1)S(1)} %get-tuple-element.57.rest_1_), channel_id=1, source_target_pairs={{0,2},{1,3},{2,0},{3,1},{4,6},{5,7},{6,4},{7,5},{8,10},{9,11},{10,... | collective-permute-start | bytes 491528 | tf_op jit(solution)/shard_map/ppermute | solution.py:308
  94.8 11.3 %collective-permute-start.31 = (bf16[704,256]{1,0:T(8,128)(2,1)S(1)}, bf16[704,256]{1,0:T(8,128)(2,1)S(1)}, u32[]{:S(2)}, u32[]{:S(2)}) collective-permute-start(bf16[704,256]{1,0:T(8,128)(2,1)S(1)} %collective-permute-done.30.rest_0_), channel_id=1, source_target_pairs={{0,4},{4,0},{8,12},{12,8},{16,20},{20,16},{24,28},{28,24},{1,5},{5... | collective-permute-start | bytes 1081352 | tf_op jit(solution)/shard_map/ppermute | solution.py:297
  96.4 1.4 collective-permute-start.21
  96.8 2.1 %collective-permute-start.22 = (bf16[160,512]{1,0:T(8,128)(2,1)S(1)}, bf16[160,512]{1,0:T(8,128)(2,1)S(1)}, u32[]{:S(2)}, u32[]{:S(2)}) collective-permute-start(bf16[160,512]{1,0:T(8,128)(2,1)S(1)} %get-tuple-element.57.rest_1_), channel_id=1, source_target_pairs={{0,1},{1,0},{2,3},{3,2},{4,5},{5,4},{6,7},{7,6},{8,9},{9,8},{10,11... | collective-permute-start | bytes 491528 | tf_op jit(solution)/shard_map/ppermute | solution.py:300
  96.9 2.9 %collective-permute-start.23 = (bf16[160,512]{1,0:T(8,128)(2,1)S(1)}, bf16[160,512]{1,0:T(8,128)(2,1)S(1)}, u32[]{:S(2)}, u32[]{:S(2)}) collective-permute-start(bf16[160,512]{1,0:T(8,128)(2,1)S(1)} %collective-permute-done.19.rest_2_), channel_id=1, source_target_pairs={{0,1},{1,0},{2,3},{3,2},{4,5},{5,4},{6,7},{7,6},{8,9},{9,8},{10,11... | collective-permute-start | bytes 491528 | tf_op jit(solution)/shard_map/ppermute | solution.py:300
  97.3 3.6 %collective-permute-start.24 = (bf16[160,512]{1,0:T(8,128)(2,1)S(1)}, bf16[160,512]{1,0:T(8,128)(2,1)S(1)}, u32[]{:S(2)}, u32[]{:S(2)}) collective-permute-start(bf16[160,512]{1,0:T(8,128)(2,1)S(1)} %collective-permute-done.20.rest_3_), channel_id=1, source_target_pairs={{0,1},{1,0},{2,3},{3,2},{4,5},{5,4},{6,7},{7,6},{8,9},{9,8},{10,11... | collective-permute-start | bytes 491528 | tf_op jit(solution)/shard_map/ppermute | solution.py:300
  97.7 12.2 %collective-permute-start.32 = (bf16[352,256]{1,0:T(8,128)(2,1)S(1)}, bf16[352,256]{1,0:T(8,128)(2,1)S(1)}, u32[]{:S(2)}, u32[]{:S(2)}) collective-permute-start(bf16[352,256]{1,0:T(8,128)(2,1)S(1)} %get-tuple-element.63.rest_0_), channel_id=1, source_target_pairs={{0,4},{4,0},{8,12},{12,8},{16,20},{20,16},{24,28},{28,24},{1,5},{5... | collective-permute-start | bytes 540680 | tf_op jit(solution)/shard_map/ppermute | solution.py:297
  98.9 14.9 %collective-permute-start.36 = (bf16[352,256]{1,0:T(8,128)(2,1)S(1)}, bf16[352,256]{1,0:T(8,128)(2,1)S(1)}, u32[]{:S(2)}, u32[]{:S(2)}) collective-permute-start(bf16[352,256]{1,0:T(8,128)(2,1)S(1)} %collective-permute-done.35.rest_4_), channel_id=1, source_target_pairs={{0,4},{4,0},{8,12},{12,8},{16,20},{20,16},{24,28},{28,24},{1,5},{5... | collective-permute-start | bytes 540680 | tf_op jit(solution)/shard_map/ppermute | solution.py:297
  99.8 17.9 %collective-permute-start.34 = (bf16[352,256]{1,0:T(8,128)(2,1)S(1)}, bf16[352,256]{1,0:T(8,128)(2,1)S(1)}, u32[]{:S(2)}, u32[]{:S(2)}) collective-permute-start(bf16[352,256]{1,0:T(8,128)(2,1)S(1)} %collective-permute-done.33.rest_2_), channel_id=1, source_target_pairs={{0,4},{4,0},{8,12},{12,8},{16,20},{20,16},{24,28},{28,24},{1,5},{5... | collective-permute-start | bytes 540680 | tf_op jit(solution)/shard_map/ppermute | solution.py:297
  100.9 19.6 %collective-permute-start.38 = (bf16[352,256]{1,0:T(8,128)(2,1)S(1)}, bf16[352,256]{1,0:T(8,128)(2,1)S(1)}, u32[]{:S(2)}, u32[]{:S(2)}) collective-permute-start(bf16[352,256]{1,0:T(8,128)(2,1)S(1)} %collective-permute-done.37.rest_6_), channel_id=1, source_target_pairs={{0,4},{4,0},{8,12},{12,8},{16,20},{20,16},{24,28},{28,24},{1,5},{5... | collective-permute-start | bytes 540680 | tf_op jit(solution)/shard_map/ppermute | solution.py:297
  121.2 1.7 %collective-permute-start.42 = (bf16[2,160,512]{2,1,0:T(8,128)(2,1)S(1)}, bf16[2,160,512]{2,1,0:T(8,128)(2,1)S(1)}, u32[]{:S(2)}, u32[]{:S(2)}) collective-permute-start(bf16[2,160,512]{2,1,0:T(8,128)(2,1)S(1)} %get-tuple-element.70), channel_id=1, source_target_pairs={{0,1},{1,0},{2,3},{3,2},{4,5},{5,4},{6,7},{7,6},{8,9},{9,8},{10,11... | collective-permute-start | bytes 983048 | tf_op jit(solution)/shard_map/ppermute | solution.py:300
  122.0 7.9 %collective-permute-start.39 = (bf16[2,160,512]{2,1,0:T(8,128)(2,1)S(1)}, bf16[2,160,512]{2,1,0:T(8,128)(2,1)S(1)}, u32[]{:S(2)}, u32[]{:S(2)}) collective-permute-start(bf16[2,160,512]{2,1,0:T(8,128)(2,1)S(1)} %get-tuple-element.66), channel_id=1, source_target_pairs={{0,1},{1,0},{2,3},{3,2},{4,5},{5,4},{6,7},{7,6},{8,9},{9,8},{10,11... | collective-permute-start | bytes 983048 | tf_op jit(solution)/shard_map/ppermute | solution.py:300
  123.0 11.9 %collective-permute-start.43 = (bf16[160,512]{1,0:T(8,128)(2,1)S(1)}, bf16[160,512]{1,0:T(8,128)(2,1)S(1)}, u32[]{:S(2)}, u32[]{:S(2)}) collective-permute-start(bf16[160,512]{1,0:T(8,128)(2,1)S(1)} %get-tuple-element.72), channel_id=1, source_target_pairs={{0,8},{1,9},{2,10},{3,11},{4,12},{5,13},{6,14},{7,15},{8,0},{9,1},... | collective-permute-start | bytes 491528 | tf_op jit(solution)/shard_map/ppermute | solution.py:308
  130.0 9.5 %collective-permute-start.40 = (bf16[160,512]{1,0:T(8,128)(2,1)S(1)}, bf16[160,512]{1,0:T(8,128)(2,1)S(1)}, u32[]{:S(2)}, u32[]{:S(2)}) collective-permute-start(bf16[160,512]{1,0:T(8,128)(2,1)S(1)} %get-tuple-element.67), channel_id=1, source_target_pairs={{0,2},{1,3},{2,0},{3,1},{4,6},{5,7},{6,4},{7,5},{8,10},{9,11},{10,... | collective-permute-start | bytes 491528 | tf_op jit(solution)/shard_map/ppermute | solution.py:308
  131.5 8.0 %collective-permute-start.41 = (bf16[160,512]{1,0:T(8,128)(2,1)S(1)}, bf16[160,512]{1,0:T(8,128)(2,1)S(1)}, u32[]{:S(2)}, u32[]{:S(2)}) collective-permute-start(bf16[160,512]{1,0:T(8,128)(2,1)S(1)} %get-tuple-element.68), channel_id=1, source_target_pairs={{0,10},{1,11},{2,8},{3,9},{4,14},{5,15},{6,12},{7,13},{8,2},{9,3},... | collective-permute-start | bytes 491528 | tf_op jit(solution)/shard_map/ppermute | solution.py:308
